TPU v7x, 256 devices: a 8x8x2 block of a 8x8x16 slice. The times are simulated.
256 devices in a mesh: grp: 2 (over z), ep: 64 (over y, x), tp: 2 (over core).
Axes of the slice: x: 8, y: 8, z: 2, core: 2. Of those that a mesh axis runs over, the one named last changes fastest.
The devices are a block of a 8x8x16 slice.
Arguments:
- tokens: bfloat16 [8192, 1024], P(('grp', 'ep')), parts along dimension 0, may hold values from -6 to 6
- routes: int32 [8192, 4], P(('grp', 'ep')), parts along dimension 0, may hold values from 0 to 63, all different within a row; in each aligned block of 64 rows (0 to 63, 64 to 127, ...) at most 12 rows name the same one
- gates: float32 [8192, 4], P(('grp', 'ep')), parts along dimension 0, may hold values from 0.05 to 1
- norm_gain: float32 [1024], replicated, may hold values from 0.1 to 1.9
- w_gate: bfloat16 [64, 1024, 1792], P('ep', None, 'tp'), may hold values from -0.1875 to 0.1875
- w_up: bfloat16 [64, 1024, 1792], P('ep', None, 'tp'), may hold values from -0.1875 to 0.1875
- w_down: bfloat16 [64, 1792, 1024], P('ep', 'tp'), may hold values from -0.125 to 0.125
Outputs:
- mixed: bfloat16 [8192, 1024], P(('grp', 'ep')), parts along dimension 0
There are 2 independent parts, one for each index of `grp`. A program takes and returns all parts, laid end to end along the dimension named above; an argument that names none is the same for every part. Nothing has to cross between parts.
Inputs may be any that keep to these rules, and one draw needn't show every extreme that they name: `routes`: within the rows of one index of ep no expert is named more than 12 times; some expert is named exactly 12 times there in some or all of them.
All inputs are finite; a program needn't handle non-finite values.
Results may differ from a plain program's by a relative error of at most 0.0078.
Values may be sent and summed in bfloat16 or wider, within the bound.
No kernel may reach another device: no remote copies, remote signals or barrier semaphores. Data moves between devices by JAX's collectives and lax.ppermute only.
A program may use at most 64 MiB of HBM per device.

v0:
```python
import jax
import jax.numpy as jnp
from jax import lax
from jax.sharding import PartitionSpec as P

EPS = 1e-06


def sent_to_all(x, axis):
    copies = jnp.broadcast_to(x, (lax.axis_size(axis), *x.shape))
    return lax.all_to_all(copies, axis, split_axis=0, concat_axis=0, tiled=True)


def in_order(parts, dim):
    parts = jnp.moveaxis(parts, 0, dim)
    dims = parts.shape
    return parts.reshape(*dims[:dim], dims[dim] * dims[dim + 1], *dims[dim + 2 :])


def collect(x, axis, dim):
    parts = sent_to_all(x, axis)
    return in_order(parts, dim)


def split_up(x, dim, peers):
    before, after = (x.shape[:dim], x.shape[dim + 1 :])
    return jnp.moveaxis(x.reshape(*before, peers, -1, *after), dim, 0)


def sum_at_owner(x, axis, dim):
    peers = lax.axis_size(axis)
    parts = lax.all_to_all(split_up(x, dim, peers), axis, 0, 0, tiled=True)
    return jnp.sum(parts.astype(jnp.float32), axis=0)


def per_device(tokens, routes, gates, norm_gain, w_gate, w_up, w_down):
    tok_rows, width = tokens.shape
    top = routes.shape[1]
    ep_count = lax.axis_size("ep")
    tp_count = lax.axis_size("tp")
    capacity = max(2, min(tok_rows, 3 * tok_rows * top // ep_count))
    share = width // tp_count
    lane = lax.axis_index("tp")
    xf = tokens.astype(jnp.float32)
    normed = (xf * lax.rsqrt(jnp.mean(xf * xf, axis=-1, keepdims=True) + EPS) * norm_gain).astype(
        jnp.bfloat16
    )
    flat = routes.reshape(-1)
    onehot = (flat[:, None] == jnp.arange(ep_count, dtype=jnp.int32)[None, :]).astype(jnp.int32)
    earlier = jnp.cumsum(onehot, axis=0) - onehot
    rank = jnp.sum(earlier * onehot, axis=1)
    slot = flat * capacity + rank
    placing = (jnp.arange(ep_count * capacity, dtype=jnp.int32)[:, None] == slot[None, :]).astype(
        jnp.bfloat16
    )
    repeated = jnp.repeat(normed, top, axis=0)
    outgoing = jnp.dot(placing, repeated, preferred_element_type=jnp.float32).astype(jnp.bfloat16)
    outgoing = outgoing.reshape(ep_count, capacity, width)
    mine = lax.dynamic_slice_in_dim(outgoing, lane * share, share, 2)
    full = collect(lax.all_to_all(mine, "ep", split_axis=0, concat_axis=0, tiled=True), "tp", 2)
    sources = full.shape[0]
    items = full.shape[1]
    rows = full.reshape(sources * items, width)
    gate_act = jnp.dot(rows, w_gate[0], preferred_element_type=jnp.float32)
    up_act = jnp.dot(rows, w_up[0], preferred_element_type=jnp.float32)
    hidden = (jax.nn.silu(gate_act) * up_act).astype(jnp.bfloat16)
    partial_value = jnp.dot(hidden, w_down[0], preferred_element_type=jnp.float32).astype(
        jnp.bfloat16
    )
    summed = sum_at_owner(
        lax.optimization_barrier(partial_value)
        .astype(jnp.float32)
        .reshape(sources, items, width)
        .astype(jnp.bfloat16),
        "tp",
        2,
    )
    results = summed.astype(jnp.bfloat16)
    returned = lax.all_to_all(results, "ep", split_axis=0, concat_axis=0, tiled=True)
    back = returned.reshape(ep_count * capacity, returned.shape[2])
    picked = jnp.take(back, slot, axis=0).reshape(tok_rows, top, back.shape[1])
    mixed = jnp.sum(gates[:, :, None] * picked.astype(jnp.float32), axis=1).astype(jnp.bfloat16)
    mixed = collect(mixed, "tp", 1)
    return mixed


def solution(mesh):
    return jax.shard_map(
        per_device,
        mesh=mesh,
        in_specs=(
            P(("grp", "ep"), None),
            P(("grp", "ep"), None),
            P(("grp", "ep"), None),
            P(),
            P("ep", None, "tp"),
            P("ep", None, "tp"),
            P("ep", "tp", None),
        ),
        out_specs=P(("grp", "ep"), None),
        check_vma=False,
    )
```

profile of v0, /device:TPU:513, one launch (start us, length us, event | category | flops | bytes accessed | tf_op | source)
XLA Modules:
  0.0 136.4 jit_solution(7492944749125615298)
XLA Ops:
  0.0 0.0 copy-start
  0.0 0.9 copy.60
  0.9 0.1 eq.39
  1.0 0.1 reshape.96
  1.1 0.6 reduce-window.6
  1.8 0.2 slice_reduce_fusion
  2.0 0.1 fusion.19
  2.1 1.0 fusion.14
  3.2 1.0 fusion.16
  4.2 0.2 broadcast_in_dim.26
  4.3 0.9 reshape.98
  5.2 1.6 %convolution_convert_fusion = bf16[768,1024]{1,0:T(8,128)(2,1)S(1)} fusion(bf16[256,1024]{1,0:T(8,128)(2,1)} %reshape.98, s32[256]{0:T(256)S(1)} %multiply_add_fusion), kind=kOutput, calls=%fused_computation.9 | convolution fusion | flops 403636224 | bytes 2098176 | tf_op jit(solution)/shard_map/dot_general | solution.py:57
  6.9 1.5 %reshape.99 = bf16[64,12,1024]{2,1,0:T(8,128)(2,1)} reshape(bf16[768,1024]{1,0:T(8,128)(2,1)S(1)} %convolution_convert_fusion) | data formatting | bytes 3145728 | tf_op jit(solution)/shard_map/reshape | solution.py:58
  8.4 1.3 constant_dynamic-slice_fusion
  9.7 44.6 %all_to_all.25 = bf16[64,12,512]{2,1,0:T(8,128)(2,1)S(1)} all-to-all(bf16[64,12,512]{2,1,0:T(8,128)(2,1)S(1)} %constant_dynamic-slice_fusion), channel_id=1, replica_groups=mesh['grp'=2,'ep'=64,'tp'=2] {'ep'}, dimensions={0} | all-to-all | bytes 1572864 | tf_op jit(solution)/shard_map/all_to_all | solution.py:60
  54.4 0.4 copy.65
  54.8 0.2 broadcast_in_dim.27
  55.0 11.1 %all_to_all.26 = bf16[2,64,12,512]{3,1,2,0:T(8,128)(2,1)S(1)} all-to-all(bf16[2,64,12,512]{3,1,2,0:T(8,128)(2,1)S(1)} %broadcast_in_dim.27), channel_id=1, replica_groups=mesh['grp'=2,'ep'=64,'tp'=2] {'tp'}, dimensions={0} | all-to-all | bytes 3145728 | tf_op jit(solution)/shard_map/all_to_all | solution.py:11
  66.1 1.6 %copy.66 = bf16[64,12,2,512]{3,2,1,0:T(2,128)(2,1)S(1)} copy(bf16[64,12,2,512]{3,0,1,2:T(8,128)(2,1)S(1)} %bitcast.49) | data formatting | bytes 3145728 | tf_op jit(solution)/shard_map/transpose | solution.py:15
  67.7 0.0 copy-start.3
  67.7 0.4 copy.73
  68.1 1.1 copy-done.3
  69.2 3.4 %fusion.2 = f32[768,896]{1,0:T(8,128)} fusion(bf16[768,1024]{1,0:T(8,128)(2,1)S(1)} %bitcast.52, bf16[1,1024,896]{2,1,0:T(8,128)(2,1)S(1)} %copy-done.3), kind=kOutput, calls=%fused_computation.4 | convolution fusion | flops 1409286144 | bytes 6160384 | tf_op jit(solution)/shard_map/dot_general | solution.py:65
  72.6 0.0 copy-done
  72.6 7.0 %fusion.6 = bf16[768,1024]{1,0:T(8,128)(2,1)} fusion(bf16[1,896,1024]{2,1,0:T(8,128)(2,1)S(1)} %copy-done, f32[768,896]{1,0:T(8,128)} %fusion.2, bf16[768,1024]{1,0:T(8,128)(2,1)S(1)} %bitcast.53, bf16[1,1024,896]{2,1,0:T(8,128)(2,1)} %param.11), kind=kOutput, calls=%fused_computation.8 | convolution fusion | flops 2823487488 | bytes 9568256 | tf_op jit(solution)/shard_map/dot_general | solution.py:67
  79.6 2.9 %convert_element_type.44 = bf16[64,12,2,512]{3,2,1,0:T(2,128)(2,1)S(1)} reshape(bf16[768,1024]{1,0:T(8,128)(2,1)} %fusion.6) | data formatting | bytes 3145728 | tf_op jit(solution)/shard_map/convert_element_type | solution.py:74
  82.5 0.5 copy.76
  83.0 5.1 %all_to_all.27 = bf16[2,64,12,512]{3,1,2,0:T(8,128)(2,1)S(1)} all-to-all(bf16[2,64,12,512]{3,1,2,0:T(8,128)(2,1)S(1)} %bitcast.51), channel_id=1, replica_groups=mesh['grp'=2,'ep'=64,'tp'=2] {'tp'}, dimensions={0} | all-to-all | bytes 3145728 | tf_op jit(solution)/shard_map/all_to_all | solution.py:32
  88.1 1.4 %reduce_sum.46 = bf16[64,12,512]{2,0,1:T(8,128)(2,1)} reduce(bf16[2,64,12,512]{3,1,2,0:T(8,128)(2,1)S(1)} %all_to_all.27, bf16[]{:T(256)} %constant.41.clone.1), dimensions={0}, to_apply=%region_4.5 | reduce | flops 393216 | bytes 2359298 | tf_op jit(solution)/shard_map/reduce_sum | solution.py:33
  89.5 0.0 copy-start.1
  89.5 0.0 copy-start.2
  89.5 2.6 %copy.68 = bf16[64,12,512]{2,1,0:T(8,128)(2,1)} copy(bf16[64,12,512]{2,0,1:T(8,128)(2,1)} %reduce_sum.46) | data formatting | bytes 1572864 | tf_op jit(solution)/shard_map/reduce_sum | solution.py:33
  92.1 7.7 %all-to-all-start.3 = ((bf16[64,12,512]{2,1,0:T(8,128)(2,1)}), bf16[64,12,512]{2,1,0:T(8,128)(2,1)}, u32[]{:S(2)}, u32[]{:S(2)}) async-start(bf16[64,12,512]{2,1,0:T(8,128)(2,1)} %copy.68), calls=%async_computation.3 | async-start | bytes 2097152 | tf_op jit(solution)/shard_map/all_to_all | solution.py:79
  99.8 0.1 reduce_sum.44
  99.9 0.0 copy-done.1
  99.9 0.1 copy.69
  100.0 0.1 mul.81
  100.1 0.1 copy.63
  100.2 0.1 copy.64
  100.3 0.0 copy-done.2
  100.3 0.1 copy.59
  100.5 26.1 %all-to-all-done.3 = bf16[64,12,512]{2,1,0:T(8,128)(2,1)} async-done(((bf16[64,12,512]{2,1,0:T(8,128)(2,1)}), bf16[64,12,512]{2,1,0:T(8,128)(2,1)}, u32[]{:S(2)}, u32[]{:S(2)}) %all-to-all-start.3) | async-done | bytes 786464 | tf_op jit(solution)/shard_map/all_to_all | solution.py:79
  126.5 1.3 reshape.100
  127.8 1.2 gather_fusion
  129.0 0.1 gather.7
  129.0 0.5 multiply_reduce_fusion
  129.5 6.2 %all_to_all.28 = bf16[2,64,512]{2,1,0:T(8,128)(2,1)S(1)} all-to-all(bf16[2,64,512]{2,1,0:T(8,128)(2,1)S(1)} %broadcast_in_dim.29), channel_id=1, replica_groups=mesh['grp'=2,'ep'=64,'tp'=2] {'tp'}, dimensions={0} | all-to-all | bytes 262144 | tf_op jit(solution)/shard_map/all_to_all | solution.py:11
  135.7 0.7 copy.72
  (10 shorter events, 0.1 us)
Async XLA Ops:
  0.0 72.6 %copy-start = (bf16[1,896,1024]{2,1,0:T(8,128)(2,1)S(1)}, bf16[1,896,1024]{2,1,0:T(8,128)(2,1)}, u32[]{:S(2)}) copy-start(bf16[1,896,1024]{2,1,0:T(8,128)(2,1)} %param.13) | copy-start | bytes 5505028
  67.7 1.5 %copy-start.3 = (bf16[1,1024,896]{2,1,0:T(8,128)(2,1)S(1)}, bf16[1,1024,896]{2,1,0:T(8,128)(2,1)}, u32[]{:S(2)}) copy-start(bf16[1,1024,896]{2,1,0:T(8,128)(2,1)} %param.12) | copy-start | bytes 5505028
  89.5 10.4 %copy-start.1 = (s32[64,4]{0,1:T(4,128)S(1)}, s32[64,4]{0,1:T(4,128)}, u32[]{:S(2)}) copy-start(s32[64,4]{0,1:T(4,128)} %param.8) | copy-start | bytes 3076
  89.5 10.8 %copy-start.2 = (f32[64,4]{0,1:T(4,128)S(1)}, f32[64,4]{0,1:T(4,128)}, u32[]{:S(2)}) copy-start(f32[64,4]{0,1:T(4,128)} %param.9) | copy-start | bytes 3076
  92.1 34.4 %all-to-all-start.3 = ((bf16[64,12,512]{2,1,0:T(8,128)(2,1)}), bf16[64,12,512]{2,1,0:T(8,128)(2,1)}, u32[]{:S(2)}, u32[]{:S(2)}) async-start(bf16[64,12,512]{2,1,0:T(8,128)(2,1)} %copy.68), calls=%async_computation.3 | async-start | bytes 2097152 | tf_op jit(solution)/shard_map/all_to_all | solution.py:79
where the time goes:
time: 137 us; the launch traced here: 136 us
  blocking collectives  67.1 us (49%)
  waiting for transfers between devices  26.1 us (19%)
  local copies, waits for them, and re-layouts  18.7 us (14%)
  matrix products  12 us (9%)
  starting transfers between devices  7.68 us (6%)
  other arithmetic  4.75 us (3%)
    all_to_all x1, blocking collectives, per_device(): lax.all_to_all(mine, 'ep', split_axis=0, concat_axis=0, tiled=True)  44.6 us
    all_to_all x1, waiting for transfers between devices, per_device(): lax.all_to_all(results, 'ep', split_axis=0, concat_axis=0, tiled=True)  26.1 us
    all_to_all x2, blocking collectives, sent_to_all(): return lax.all_to_all(copies, axis, split_axis=0, concat_axis=0, tiled=True)  17.3 us
    all_to_all x1, starting transfers between devices, per_device(): lax.all_to_all(results, 'ep', split_axis=0, concat_axis=0, tiled=True)  7.68 us
    dot_general x1, matrix products, per_device(): jnp.dot(hidden, w_down[0], preferred_element_type=jnp.float32)  7.03 us
    all_to_all x1, blocking collectives, sum_at_owner(): parts = lax.all_to_all(split_up(x, dim, peers), axis, 0, 0, tiled=True)  5.1 us
    convert_element_type x2, local copies, waits for them, and re-layouts, per_device(): summed = sum_at_owner(lax.optimization_barrier(partial_value).astype(jnp....  3.36 us
    dot_general x1, matrix products, per_device(): up_act = jnp.dot(rows, w_up[0], preferred_element_type=jnp.float32)  3.35 us
  transfers between devices with their start and end apart: 1, of which 1 were waited for; matrix products, arithmetic and copies ran while one was open for 0% of the time, Pallas kernels for 0%

commit v1 on v0

v1 whole, which is shorter than its diff:
```python
import functools

import jax
import jax.numpy as jnp
from jax import lax
from jax.experimental import pallas as pl
from jax.experimental.pallas import tpu as pltpu
from jax.sharding import PartitionSpec as P

EPS = 1e-06
BF = jnp.bfloat16
F32 = jnp.float32
VMEM = pl.BlockSpec(memory_space=pltpu.VMEM)
SMEM = pl.BlockSpec(memory_space=pltpu.SMEM)
LIMIT = 24 * 1024 * 1024


def dot(a, b):
    return jnp.dot(a, b, preferred_element_type=F32)


def iota(shape, dim):
    return lax.broadcasted_iota(jnp.int32, shape, dim)


def call(body, out_shape, n_smem, n_in, scratch=(), flops=0):
    return pl.pallas_call(
        body,
        out_shape=out_shape,
        in_specs=[SMEM] * n_smem + [VMEM] * n_in,
        out_specs=jax.tree.map(lambda _: VMEM, out_shape),
        scratch_shapes=list(scratch),
        compiler_params=pltpu.CompilerParams(vmem_limit_bytes=LIMIT),
        cost_estimate=pl.CostEstimate(flops=flops, bytes_accessed=0, transcendentals=0),
    )


def div_const(x, n):
    mul = -(-(1 << 17) // n)
    return (x * mul) >> 17


def prep_body(lane_ref, tok_ref, gain_ref, rt_ref, out_ref, half_ref, *, experts, cap):
    rows, width = tok_ref.shape
    share = width // 2
    q = share // 2
    xf = tok_ref[...].astype(F32)
    var = jnp.mean(xf * xf, axis=-1, keepdims=True)
    normed = (xf * lax.rsqrt(var + EPS) * gain_ref[...]).astype(BF)
    for c in range(2):
        for h in range(2):
            half_ref[c, h * rows : (h + 1) * rows, :] = normed[:, c * share + h * q : c * share + (h + 1) * q]
    stacked = half_ref[lane_ref[0]]
    wide = 2 * rows
    rt = rt_ref[...]
    e_of = iota((experts, wide), 0)
    chosen = jnp.zeros((experts, wide), F32)
    for k in range(rt.shape[0]):
        chosen = chosen + (e_of == rt[k : k + 1, :]).astype(F32)
    t_of = iota((wide, wide), 1)
    before = iota((wide, wide), 0)
    upper = jnp.where(before < jnp.where(t_of >= rows, t_of - rows, t_of), 1.0, 0.0)
    upper = jnp.where(before < rows, upper, 0.0).astype(BF)
    rank = dot(chosen.astype(BF), upper)
    place = jnp.where(chosen > 0, rank, -1.0).astype(BF)
    group = 8
    block = group * 2 * cap
    r = iota((block, wide), 0)
    e_in = div_const(r, 2 * cap)
    left = r - e_in * (2 * cap)
    h_in = (left >= cap).astype(jnp.int32)
    slot = (left - h_in * cap).astype(F32)
    right_half = h_in == (iota((block, wide), 1) >= rows).astype(jnp.int32)
    e_row = div_const(iota((block, experts), 0), 2 * cap)
    e_col = iota((block, experts), 1)
    for b in range(experts // group):
        rep = (e_col == e_row + b * group).astype(F32).astype(BF)
        ranks = dot(rep, place)
        one = jnp.where((ranks == slot) & right_half, 1.0, 0.0).astype(BF)
        out_ref[b * block : (b + 1) * block, :] = dot(one, stacked).astype(BF)


def sort_matrix(cap, group, transposed):
    n = group * 2 * cap
    half = group * cap
    qdim, pdim = (1, 0) if transposed else (0, 1)
    qq = iota((n, n), qdim)
    h = (qq >= half).astype(jnp.int32)
    i = qq - h * half
    b = div_const(i, cap)
    src = b * (2 * cap) + h * cap + (i - b * cap)
    return jnp.where(iota((n, n), pdim) == src, 1.0, 0.0).astype(BF)


def unpack(x_ref, rows_ref, cap, group):
    n = group * 2 * cap
    half = n // 2
    q = x_ref.shape[1]
    perm = sort_matrix(cap, group, False)
    for b in range(x_ref.shape[0] // n):
        got = dot(perm, x_ref[b * n : (b + 1) * n, :]).astype(BF)
        for h in range(2):
            rows_ref[b * half : (b + 1) * half, h * q : (h + 1) * q] = got[h * half : (h + 1) * half, :]


def pack(y, out_ref, cap, group):
    n = group * 2 * cap
    half = n // 2
    q = y.shape[1] // 2
    perm = sort_matrix(cap, group, True)
    for b in range(y.shape[0] // half):
        part = y[b * half : (b + 1) * half]
        stacked = jnp.concatenate([part[:, :q], part[:, q:]], axis=0)
        out_ref[b * n : (b + 1) * n, :] = dot(perm, stacked).astype(BF)


def first_body(lane_ref, x_ref, wg_ref, wu_ref, acc_ref, rows_ref, *, cap, group):
    share = rows_ref.shape[1]
    unpack(x_ref, rows_ref, cap, group)
    start = pl.multiple_of(lane_ref[0] * share, share)
    rows = rows_ref[...]
    for n in range(acc_ref.shape[0]):
        cols = slice(n * 128, (n + 1) * 128)
        w = jnp.concatenate([wg_ref[pl.ds(start, share), cols], wu_ref[pl.ds(start, share), cols]], axis=1)
        acc_ref[n] = dot(rows, w)


def second_body(lane_ref, x_ref, wg_ref, wu_ref, wd_ref, acc_ref, hid_ref, out_ref, rows_ref, *, cap, group):
    share = rows_ref.shape[1]
    unpack(x_ref, rows_ref, cap, group)
    start = pl.multiple_of((1 - lane_ref[0]) * share, share)
    rows = rows_ref[...]
    for n in range(acc_ref.shape[0]):
        cols = slice(n * 128, (n + 1) * 128)
        w = jnp.concatenate([wg_ref[pl.ds(start, share), cols], wu_ref[pl.ds(start, share), cols]], axis=1)
        both = acc_ref[n] + dot(rows, w)
        g, u = both[:, :128], both[:, 128:]
        hid_ref[:, cols] = (g / (1.0 + jnp.exp(-g)) * u).astype(BF)
    y = dot(hid_ref[...], wd_ref[:, pl.ds(start, share)]).astype(BF)
    pack(y, out_ref, cap, group)


def third_body(lane_ref, hid_ref, wd_ref, rt_ref, gt_ref, out_ref, mix_ref, *, cap, group, experts):
    share = wd_ref.shape[1] // 2
    start = pl.multiple_of(lane_ref[0] * share, share)
    y = dot(hid_ref[...], wd_ref[:, pl.ds(start, share)]).astype(BF)
    pack(y, out_ref, cap, group)
    toks, top = rt_ref.shape
    e_of = iota((toks, experts), 1)
    chosen = jnp.zeros((toks, experts), F32)
    gate = jnp.zeros((toks, experts), F32)
    for k in range(top):
        hit = e_of == rt_ref[:, k : k + 1]
        chosen = chosen + hit.astype(F32)
        gate = gate + jnp.where(hit, gt_ref[:, k : k + 1], 0.0)
    lower = (iota((toks, toks), 1) < iota((toks, toks), 0)).astype(F32).astype(BF)
    rank = dot(lower, chosen.astype(BF))
    place = jnp.where(chosen > 0, rank, -1.0).astype(BF)
    g1 = gate.astype(BF)
    rest = gate - g1.astype(F32)
    g2 = rest.astype(BF)
    g3 = (rest - g2.astype(F32)).astype(BF)
    tall = jnp.concatenate([place, g1, g2, g3], axis=0)
    n = 2 * cap * experts
    r = iota((1, n), 1)
    e_r = div_const(r, 2 * cap)
    left = r - e_r * (2 * cap)
    h_r = left >= cap
    slot = jnp.where(h_r, left - cap, left).astype(F32)
    rep = (iota((experts, n), 0) == e_r).astype(F32).astype(BF)
    spread = dot(tall, rep)
    here = spread[:toks] == slot
    for h in range(2):
        ok = here & (h_r if h else jnp.logical_not(h_r))
        for i in range(3):
            piece = spread[(1 + i) * toks : (2 + i) * toks]
            at = (h * 3 + i) * toks
            mix_ref[at : at + toks, :] = jnp.where(ok, piece, 0.0).astype(BF)


def last_body(mix_ref, back_ref, out_ref):
    toks = out_ref.shape[0]
    q = back_ref.shape[1]
    s = dot(mix_ref[...], back_ref[...])
    for h in range(2):
        at = 3 * h * toks
        total = s[at : at + toks] + s[at + toks : at + 2 * toks] + s[at + 2 * toks : at + 3 * toks]
        out_ref[:, h * q : (h + 1) * q] = total.astype(BF)


def per_device(tokens, routes, gates, norm_gain, w_gate, w_up, w_down):
    toks, width = tokens.shape
    top = routes.shape[1]
    experts = lax.axis_size("ep")
    cap = max(2, min(toks, 3 * toks * top // experts))
    share = width // 2
    q = share // 2
    ff = w_gate.shape[2]
    items = experts * cap
    group = 8
    swap = lambda v: lax.ppermute(v, "tp", [(0, 1), (1, 0)])
    lane = lax.axis_index("tp").astype(jnp.int32)
    lanes = lane.reshape(1)
    rt = routes.T
    rt2 = jnp.concatenate([rt, rt], axis=1)
    struct = jax.ShapeDtypeStruct
    wide = struct((2 * items, q), BF)

    outgoing = call(
        functools.partial(prep_body, experts=experts, cap=cap), wide, 1, 3,
        [pltpu.VMEM((2, 2 * toks, q), BF)], flops=2 * 2 * items * 2 * toks * q,
    )(lanes, tokens, norm_gain.reshape(1, width), rt2)
    exchange = lambda v: lax.all_to_all(
        v.reshape(experts, 2 * cap, q), "ep", split_axis=0, concat_axis=0, tiled=True
    ).reshape(2 * items, q)
    mine = exchange(outgoing)
    other = swap(mine)
    wg, wu, wd = w_gate[0], w_up[0], w_down[0]
    blocks = ff // 128
    acc = call(
        functools.partial(first_body, cap=cap, group=group), struct((blocks, items, 256), F32), 1, 3,
        [pltpu.VMEM((items, share), BF)], flops=2 * items * share * 2 * ff,
    )(lanes, mine, wg, wu)
    hidden, sent = call(
        functools.partial(second_body, cap=cap, group=group), (struct((items, ff), BF), wide), 1, 5,
        [pltpu.VMEM((items, share), BF)], flops=2 * items * share * 3 * ff,
    )(lanes, other, wg, wu, wd, acc)
    got = swap(sent)
    kept, table = call(
        functools.partial(third_body, cap=cap, group=group, experts=experts),
        (wide, struct((6 * toks, 2 * items), BF)), 1, 4, flops=2 * items * share * ff,
    )(lanes, hidden, wd, routes, gates)
    results = (kept.astype(F32) + got.astype(F32)).astype(BF)
    back = exchange(results)
    part = call(last_body, struct((toks, share), BF), 0, 2, flops=2 * 6 * toks * 2 * items * q)(table, back)
    rest = swap(part)
    first = lane == 0
    return jnp.concatenate([jnp.where(first, part, rest), jnp.where(first, rest, part)], axis=1)


def solution(mesh):
    return jax.shard_map(
        per_device,
        mesh=mesh,
        in_specs=(
            P(("grp", "ep"), None),
            P(("grp", "ep"), None),
            P(("grp", "ep"), None),
            P(),
            P("ep", None, "tp"),
            P("ep", None, "tp"),
            P("ep", "tp", None),
        ),
        out_specs=P(("grp", "ep"), None),
        check_vma=False,
    )
```

time: 137 us -> 93.3 us (0.68)
  waiting for transfers between devices: 26.1 us -> 0.91 us
  local copies, waits for them, and re-layouts: 18.7 us -> 4.8 us
  matrix products: 12 us -> 0 us
  Pallas kernels: 0 us -> 9.13 us
  other arithmetic: 4.75 us -> 1.81 us
  starting transfers between devices: 7.68 us -> 9.59 us
    all_to_all x1 -> x0, waiting for transfers between devices: 26.1 us -> none  [per_device(): lax.all_to_all(results, 'ep', split_axis=0, concat_axis=0, tiled=True)]
    dot_general x3 -> x0, matrix products: 12 us -> none  [the longest x1 7.03 us: per_device(): jnp.dot(hidden, w_down[0], preferred_element_type=jnp.float32)]
    ppermute x0 -> x3, starting transfers between devices: none -> 9.59 us  [per_device(): swap = lambda v: lax.ppermute(v, 'tp', [(0, 1), (1, 0)])]
    pallas_call x0 -> x5, Pallas kernels: none -> 9.13 us  [the longest x1 4.25 us: per_device(): call(functools.partial(second_body, cap=cap, group=group), (struct((items...]
    all_to_all x1 -> x0, starting transfers between devices: 7.68 us -> none  [per_device(): lax.all_to_all(results, 'ep', split_axis=0, concat_axis=0, tiled=True)]
    reshape x5 -> x0, local copies, waits for them, and re-layouts: 4.52 us -> none  [the longest x1 1.54 us: per_device(): outgoing = outgoing.reshape(ep_count, capacity, width)]
    convert_element_type x2 -> x0, local copies, waits for them, and re-layouts: 3.36 us -> none  [per_device(): summed = sum_at_owner(lax.optimization_barrier(partial_value).astype(jnp....]
    reduce_sum x4 -> x0, other arithmetic: 3.04 us -> none  [the longest x1 1.44 us: sum_at_owner(): return jnp.sum(parts.astype(jnp.float32), axis=0)]
  transfers between devices with their start and end apart: 1 -> 3, of which waited for: 1 -> 1; matrix products, arithmetic and copies ran while one was open for 0% -> 0% of each run, Pallas kernels for 0% -> 4%
where the time goes in v1:
time: 93.3 us; the launch traced here: 93.1 us
  blocking collectives  66.7 us (71%)
  starting transfers between devices  9.59 us (10%)
  Pallas kernels  9.13 us (10%)
  local copies, waits for them, and re-layouts  4.8 us (5%)
  other arithmetic  1.81 us (2%)
    all_to_all x2, blocking collectives, per_device(): lax.all_to_all(v.reshape(experts, 2 * cap, q), 'ep', split_axis=0, concat...  66.7 us
    ppermute x3, starting transfers between devices, per_device(): swap = lambda v: lax.ppermute(v, 'tp', [(0, 1), (1, 0)])  9.59 us
    unnamed x18, local copies, waits for them, and re-layouts  4.8 us
    pallas_call x1, Pallas kernels, per_device(): call(functools.partial(second_body, cap=cap, group=group), (struct((items...  4.25 us
  transfers between devices with their start and end apart: 3, of which 1 were waited for; matrix products, arithmetic and copies ran while one was open for 0% of the time, Pallas kernels for 4%

profile of v1, /device:TPU:513, one launch (start us, length us, event | category | flops | bytes accessed | tf_op | source)
XLA Modules:
  0.0 93.1 jit_solution(8477741310363245387)
XLA Ops:
  0.0 0.0 copy-start
  0.0 0.9 pad_add_fusion.rt_ref
  0.9 0.0 copy-start.4
  0.9 0.9 copy-done.4
  1.8 0.0 copy-start.5
  1.8 0.7 copy-done.5
  2.5 1.0 %shard_map.73 = bf16[1536,256]{1,0:T(8,128)(2,1)S(1)} custom-call(s32[1]{0:T(128)} %bitcast.lane_ref, bf16[64,1024]{1,0:T(8,128)(2,1)S(1)} %copy-done.4, f32[1,1024]{1,0:T(1,128)S(1)} %bitcast.20, s32[4,128]{1,0:T(4,128)S(1)} %pad_add_fusion.rt_ref), custom_call_target="tpu_custom_call" | custom-call | flops 100663296 | tf_op jit(solution)/shard_map/pallas_call | solution.py:209
  3.5 38.9 %all_to_all.10 = bf16[64,24,256]{2,1,0:T(8,128)(2,1)S(1)} all-to-all(bf16[64,24,256]{2,1,0:T(8,128)(2,1)S(1)} %bitcast.18), channel_id=1, replica_groups=mesh['grp'=2,'ep'=64,'tp'=2] {'ep'}, dimensions={0} | all-to-all | bytes 1572864 | tf_op jit(solution)/shard_map/all_to_all | solution.py:213
  42.4 7.1 %collective-permute-start = (bf16[1536,256]{1,0:T(8,128)(2,1)S(1)}, bf16[1536,256]{1,0:T(8,128)(2,1)S(1)}, u32[]{:S(2)}, u32[]{:S(2)}) collective-permute-start(bf16[1536,256]{1,0:T(8,128)(2,1)S(1)} %bitcast.16), channel_id=1, source_target_pairs={{0,1},{1,0},{2,3},{3,2},{4,5},{5,4},{6,7},{7,6},{8,9},{9,8},{10,11... | collective-permute-start | bytes 2359304 | tf_op jit(solution)/shard_map/ppermute | solution.py:201
  49.5 0.0 copy-done
  49.5 0.0 copy-start.1
  49.5 1.5 %copy-done.1 = bf16[1,1024,896]{2,1,0:T(8,128)(2,1)S(1)} copy-done((bf16[1,1024,896]{2,1,0:T(8,128)(2,1)S(1)}, bf16[1,1024,896]{2,1,0:T(8,128)(2,1)}, u32[]{:S(2)}) %copy-start.1) | copy-done | bytes 1835032
  51.0 0.0 copy-start.2
  51.0 1.8 %shard_map.74.acc_ref = f32[7,768,256]{2,1,0:T(8,128)S(1)} custom-call(s32[1]{0:T(128)} %bitcast.lane_ref, bf16[1536,256]{1,0:T(8,128)(2,1)S(1)} %bitcast.17, bf16[1024,896]{1,0:T(8,128)(2,1)S(1)} %bitcast.10, bf16[1024,896]{1,0:T(8,128)(2,1)S(1)} %bitcast.12), custom_call_target="tpu_custom_call" | custom-call | flops 1409286144 | tf_op jit(solution)/shard_map/pallas_call | solution.py:220
  52.8 0.0 collective-permute-done.x_ref
  52.8 0.0 copy-done.2
  52.8 0.0 copy-start.6
  52.8 0.0 copy-start.7
  52.8 4.3 %shard_map.75 = (bf16[768,896]{1,0:T(8,128)(2,1)S(1)}, bf16[1536,256]{1,0:T(8,128)(2,1)}) custom-call(s32[1]{0:T(128)} %bitcast.lane_ref, bf16[1536,256]{1,0:T(8,128)(2,1)S(1)} %collective-permute-done.x_ref, bf16[1024,896]{1,0:T(8,128)(2,1)S(1)} %bitcast.11, bf16[1024,896]{1,0:T(8,128)(2,1)S(1)} %bitcast.13, bf16[896,1024]{1,0:T(8,128)(2,1)S(1)} %bitcast.14, ...), custom_call_target="tpu_custom_call" | custom-call | flops 2113929216 | tf_op jit(solution)/shard_map/pallas_call | solution.py:224
  57.1 0.0 collective-permute-start.1
  57.1 0.0 copy-done.6
  57.1 0.1 copy.8.rt_ref
  57.2 0.0 copy-done.7
  57.2 0.1 copy.9.gt_ref
  57.3 0.0 copy-start.3
  57.3 1.5 %copy-done.3 = bf16[1,896,1024]{2,1,0:T(8,128)(2,1)S(1)} copy-done((bf16[1,896,1024]{2,1,0:T(8,128)(2,1)S(1)}, bf16[1,896,1024]{2,1,0:T(8,128)(2,1)}, u32[]{:S(2)}) %copy-start.3) | copy-done | bytes 1835032
  58.8 1.6 %shard_map.76 = (bf16[1536,256]{1,0:T(8,128)(2,1)S(1)}, bf16[384,1536]{1,0:T(8,128)(2,1)S(1)}) custom-call(s32[1]{0:T(128)} %bitcast.lane_ref, bf16[768,896]{1,0:T(8,128)(2,1)S(1)} %get-tuple-element.9.hid_ref, bf16[896,1024]{1,0:T(8,128)(2,1)S(1)} %bitcast.15, s32[64,4]{1,0:T(8,128)S(1)} %copy.8.rt_ref, f32[64,4]{1,0:T(8,128)S(1)} %copy.9.gt_ref), custom_call_target="tpu_custom_call" | custom-call | flops 704643072 | tf_op jit(solution)/shard_map/pallas_call | solution.py:229
  60.4 0.0 collective-permute-done.1
  60.4 0.2 add_convert_fusion
  60.7 27.8 %all_to_all.11 = bf16[64,24,256]{2,1,0:T(8,128)(2,1)S(1)} all-to-all(bf16[64,24,256]{2,1,0:T(8,128)(2,1)S(1)} %bitcast.21), channel_id=1, replica_groups=mesh['grp'=2,'ep'=64,'tp'=2] {'ep'}, dimensions={0} | all-to-all | bytes 1572864 | tf_op jit(solution)/shard_map/all_to_all | solution.py:213
  88.5 0.5 shard_map.77
  89.0 2.5 %collective-permute-start.2 = (bf16[64,512]{1,0:T(8,128)(2,1)S(1)}, bf16[64,512]{1,0:T(8,128)(2,1)S(1)}, u32[]{:S(2)}, u32[]{:S(2)}) collective-permute-start(bf16[64,512]{1,0:T(8,128)(2,1)S(1)} %shard_map.77), channel_id=1, source_target_pairs={{0,1},{1,0},{2,3},{3,2},{4,5},{5,4},{6,7},{7,6},{8,9},{9,8},{10,11... | collective-permute-start | bytes 196616 | tf_op jit(solution)/shard_map/ppermute | solution.py:201
  91.5 0.9 collective-permute-done.2
  92.4 0.7 pad_maximum_fusion
  (1 shorter events, 0.0 us)
Async XLA Ops:
  0.0 49.5 %copy-start = (bf16[1,1024,896]{2,1,0:T(8,128)(2,1)S(1)}, bf16[1,1024,896]{2,1,0:T(8,128)(2,1)}, u32[]{:S(2)}) copy-start(bf16[1,1024,896]{2,1,0:T(8,128)(2,1)} %param.11) | copy-start | bytes 5505028
  0.9 0.9 copy-start.4
  1.8 0.7 copy-start.5
  42.4 10.4 %collective-permute-start = (bf16[1536,256]{1,0:T(8,128)(2,1)S(1)}, bf16[1536,256]{1,0:T(8,128)(2,1)S(1)}, u32[]{:S(2)}, u32[]{:S(2)}) collective-permute-start(bf16[1536,256]{1,0:T(8,128)(2,1)S(1)} %bitcast.16), channel_id=1, source_target_pairs={{0,1},{1,0},{2,3},{3,2},{4,5},{5,4},{6,7},{7,6},{8,9},{9,8},{10,11... | collective-permute-start | bytes 2359304 | tf_op jit(solution)/shard_map/ppermute | solution.py:201
  49.5 1.5 %copy-start.1 = (bf16[1,1024,896]{2,1,0:T(8,128)(2,1)S(1)}, bf16[1,1024,896]{2,1,0:T(8,128)(2,1)}, u32[]{:S(2)}) copy-start(bf16[1,1024,896]{2,1,0:T(8,128)(2,1)} %param.12) | copy-start | bytes 5505028
  51.0 1.8 %copy-start.2 = (bf16[1,896,1024]{2,1,0:T(8,128)(2,1)S(1)}, bf16[1,896,1024]{2,1,0:T(8,128)(2,1)}, u32[]{:S(2)}) copy-start(bf16[1,896,1024]{2,1,0:T(8,128)(2,1)} %param.13) | copy-start | bytes 5505028
  52.8 4.3 %copy-start.6 = (s32[64,4]{0,1:T(4,128)S(1)}, s32[64,4]{0,1:T(4,128)}, u32[]{:S(2)}) copy-start(s32[64,4]{0,1:T(4,128)} %param.8) | copy-start | bytes 3076
  52.8 4.4 %copy-start.7 = (f32[64,4]{0,1:T(4,128)S(1)}, f32[64,4]{0,1:T(4,128)}, u32[]{:S(2)}) copy-start(f32[64,4]{0,1:T(4,128)} %param.9) | copy-start | bytes 3076
  57.1 3.3 %collective-permute-start.1 = (bf16[1536,256]{1,0:T(8,128)(2,1)}, bf16[1536,256]{1,0:T(8,128)(2,1)S(1)}, u32[]{:S(2)}, u32[]{:S(2)}) collective-permute-start(bf16[1536,256]{1,0:T(8,128)(2,1)} %get-tuple-element.12), channel_id=1, source_target_pairs={{0,1},{1,0},{2,3},{3,2},{4,5},{5,4},{6,7},{7,6},{8,9},{9,8},{10,11... | collective-permute-start | bytes 2359304 | tf_op jit(solution)/shard_map/ppermute | solution.py:201
  57.3 1.5 %copy-start.3 = (bf16[1,896,1024]{2,1,0:T(8,128)(2,1)S(1)}, bf16[1,896,1024]{2,1,0:T(8,128)(2,1)}, u32[]{:S(2)}) copy-start(bf16[1,896,1024]{2,1,0:T(8,128)(2,1)} %param.13) | copy-start | bytes 5505028
  89.0 3.4 %collective-permute-start.2 = (bf16[64,512]{1,0:T(8,128)(2,1)S(1)}, bf16[64,512]{1,0:T(8,128)(2,1)S(1)}, u32[]{:S(2)}, u32[]{:S(2)}) collective-permute-start(bf16[64,512]{1,0:T(8,128)(2,1)S(1)} %shard_map.77), channel_id=1, source_target_pairs={{0,1},{1,0},{2,3},{3,2},{4,5},{5,4},{6,7},{7,6},{8,9},{9,8},{10,11... | collective-permute-start | bytes 196616 | tf_op jit(solution)/shard_map/ppermute | solution.py:201

commit v2 on v0

v2 whole, which is shorter than its diff:
```python
import functools

import jax
import jax.numpy as jnp
from jax import lax
from jax.experimental import pallas as pl
from jax.experimental.pallas import tpu as pltpu
from jax.sharding import PartitionSpec as P

EPS = 1e-06
BF = jnp.bfloat16
F32 = jnp.float32
VMEM = pl.BlockSpec(memory_space=pltpu.VMEM)
SMEM = pl.BlockSpec(memory_space=pltpu.SMEM)
HBM = pl.BlockSpec(memory_space=pltpu.HBM)
LIMIT = 16 * 1024 * 1024
QUARTERS = 4
GROUP = 8


def dot(a, b):
    return jnp.dot(a, b, preferred_element_type=F32)


def iota(shape, dim):
    return lax.broadcasted_iota(jnp.int32, shape, dim)


def div_const(x, n):
    return (x * (-(-(1 << 17) // n))) >> 17


def bf(mask):
    return jnp.where(mask, 1.0, 0.0).astype(BF)


def call(body, outs, in_specs, scratch=(), flops=0):
    return pl.pallas_call(
        body,
        out_shape=outs,
        in_specs=in_specs,
        out_specs=jax.tree.map(lambda _: VMEM, outs),
        scratch_shapes=list(scratch),
        compiler_params=pltpu.CompilerParams(vmem_limit_bytes=LIMIT),
        cost_estimate=pl.CostEstimate(flops=flops, bytes_accessed=0, transcendentals=0),
    )


def prep_body(
    lane_ref, tok_hbm, gain_hbm, rt_hbm, wg_hbm, wu_hbm, wd_hbm,
    out_ref, wg_ref, wu_ref, wd_ref,
    tok_ref, gain_ref, rt_ref, stack_ref, sems, *, experts, slots,
):
    pairs = (
        (tok_hbm, tok_ref), (gain_hbm, gain_ref), (rt_hbm, rt_ref),
        (wg_hbm, wg_ref), (wu_hbm, wu_ref), (wd_hbm, wd_ref),
    )
    copies = [pltpu.make_async_copy(a, b, sems.at[i]) for i, (a, b) in enumerate(pairs)]
    for c in copies:
        c.start()
    for c in copies[:3]:
        c.wait()
    rows, width = tok_ref.shape
    q = width // QUARTERS
    xf = tok_ref[...].astype(F32)
    var = jnp.mean(xf * xf, axis=-1, keepdims=True)
    normed = (xf * lax.rsqrt(var + EPS) * gain_ref[...]).astype(BF)
    for h in range(QUARTERS):
        stack_ref[h * rows : (h + 1) * rows, :] = normed[:, h * q : (h + 1) * q]
    rt = rt_ref[...]
    e_of = iota((experts, rows), 0)
    chosen = jnp.zeros((experts, rows), F32)
    for k in range(rt.shape[0]):
        chosen = chosen + (e_of == rt[k : k + 1, :]).astype(F32)
    upper = bf(iota((rows, rows), 0) < iota((rows, rows), 1))
    rel = dot(chosen.astype(BF), upper) - (lane_ref[0] * slots).astype(F32)
    place = jnp.where((chosen > 0) & (rel >= 0) & (rel < slots), rel, -1.0).astype(BF)
    wide = QUARTERS * rows
    t2 = iota((rows, wide), 1)
    quarter = div_const(t2, rows)
    spread = dot(place, bf(t2 - quarter * rows == iota((rows, wide), 0)))
    quarter = div_const(iota((experts, wide), 1), rows).astype(F32)
    code = jnp.where(spread >= 0, spread + 16.0 * quarter, -1.0).astype(BF)
    message = QUARTERS * slots
    block = GROUP * message
    r = iota((block, wide), 0)
    left = r - div_const(r, message) * message
    part = div_const(left, slots)
    want = (left + part * (16 - slots)).astype(F32)
    e_row = div_const(iota((block, experts), 0), message)
    e_col = iota((block, experts), 1)
    stacked = stack_ref[...]
    for b in range(experts // GROUP):
        one = bf(dot(bf(e_col == e_row + b * GROUP), code) == want)
        out_ref[b * block : (b + 1) * block, :] = dot(one, stacked).astype(BF)
    for c in copies[3:]:
        c.wait()


def sort_matrix(slots, transposed):
    message = QUARTERS * slots
    n = GROUP * message
    each = GROUP * slots
    qdim, pdim = (1, 0) if transposed else (0, 1)
    qq = iota((n, n), qdim)
    h = div_const(qq, each)
    i = qq - h * each
    b = div_const(i, slots)
    src = b * (message - slots) + h * slots + i
    return bf(iota((n, n), pdim) == src)


def unpack(x_ref, rows_ref, slots):
    n = GROUP * QUARTERS * slots
    each = GROUP * slots
    q = x_ref.shape[1]
    perm = sort_matrix(slots, False)
    for b in range(x_ref.shape[0] // n):
        got = dot(perm, x_ref[b * n : (b + 1) * n, :]).astype(BF)
        for h in range(QUARTERS):
            rows_ref[b * each : (b + 1) * each, h * q : (h + 1) * q] = got[h * each : (h + 1) * each, :]


def pack(y, out_ref, slots):
    n = GROUP * QUARTERS * slots
    each = GROUP * slots
    q = out_ref.shape[1]
    perm = sort_matrix(slots, True)
    for b in range(y.shape[0] // each):
        part = y[b * each : (b + 1) * each]
        stacked = jnp.concatenate([part[:, h * q : (h + 1) * q] for h in range(QUARTERS)], axis=0)
        out_ref[b * n : (b + 1) * n, :] = dot(perm, stacked).astype(BF)


def ffn_body(x_ref, wg_ref, wu_ref, wd_ref, out_ref, rows_ref, hid_ref, *, slots):
    unpack(x_ref, rows_ref, slots)
    rows = rows_ref[...]
    for n in range(hid_ref.shape[1] // 128):
        cols = slice(n * 128, (n + 1) * 128)
        both = dot(rows, jnp.concatenate([wg_ref[:, cols], wu_ref[:, cols]], axis=1))
        g, u = both[:, :128], both[:, 128:]
        hid_ref[:, cols] = ((0.5 * g) * (1.0 + jnp.tanh(0.5 * g)) * u).astype(BF)
    y = dot(hid_ref[...], wd_ref[...]).astype(BF)
    pack(y, out_ref, slots)


def table_body(lane_ref, rt_ref, gt_ref, mix_ref, *, slots, experts):
    toks, top = rt_ref.shape
    e_of = iota((toks, experts), 1)
    chosen = jnp.zeros((toks, experts), F32)
    gate = jnp.zeros((toks, experts), F32)
    for k in range(top):
        hit = e_of == rt_ref[:, k : k + 1]
        chosen = chosen + hit.astype(F32)
        gate = gate + jnp.where(hit, gt_ref[:, k : k + 1], 0.0)
    lower = bf(iota((toks, toks), 1) < iota((toks, toks), 0))
    rel = dot(lower, chosen.astype(BF)) - ((1 - lane_ref[0]) * slots).astype(F32)
    place = jnp.where((chosen > 0) & (rel >= 0) & (rel < slots), rel, -1.0).astype(BF)
    g1 = gate.astype(BF)
    rest = gate - g1.astype(F32)
    g2 = rest.astype(BF)
    g3 = (rest - g2.astype(F32)).astype(BF)
    n = slots * experts
    r = iota((1, n), 1)
    e_r = div_const(r, slots)
    slot = (r - e_r * slots).astype(F32)
    rep = bf(iota((experts, n), 0) == e_r)
    here = dot(place, rep) == slot
    for i, piece in enumerate((g1, g2, g3)):
        mix_ref[i * toks : (i + 1) * toks, :] = jnp.where(here, dot(piece, rep), 0.0).astype(BF)


def add_body(a_ref, b_ref, out_ref):
    out_ref[...] = (a_ref[...].astype(F32) + b_ref[...].astype(F32)).astype(BF)


def last_body(mix_ref, back_ref, out_ref, rows_ref, *, slots):
    toks = out_ref.shape[0]
    unpack(back_ref, rows_ref, slots)
    s = dot(mix_ref[...], rows_ref[...])
    out_ref[...] = s[:toks] + s[toks : 2 * toks] + s[2 * toks :]


def per_device(tokens, routes, gates, norm_gain, w_gate, w_up, w_down):
    toks, width = tokens.shape
    top = routes.shape[1]
    experts = lax.axis_size("ep")
    cap = max(2, min(toks, 3 * toks * top // experts))
    slots = -(-cap // 2)
    q = width // QUARTERS
    ff = w_gate.shape[2]
    items = experts * slots
    wide = pltpu.VMEM((QUARTERS * items, q), BF)
    swap = lambda v: lax.ppermute(v, "tp", [(0, 1), (1, 0)])
    lanes = lax.axis_index("tp").astype(jnp.int32).reshape(1)
    wg, wu, wd = w_gate[0], w_up[0], w_down[0]

    outgoing, wg, wu, wd = call(
        functools.partial(prep_body, experts=experts, slots=slots),
        (wide, pltpu.VMEM(wg.shape, BF), pltpu.VMEM(wu.shape, BF), pltpu.VMEM(wd.shape, BF)),
        [SMEM] + [HBM] * 6,
        [
            pltpu.VMEM((toks, width), BF),
            pltpu.VMEM((1, width), F32),
            pltpu.VMEM((top, toks), jnp.int32),
            pltpu.VMEM((QUARTERS * toks, q), BF),
            pltpu.SemaphoreType.DMA((6,)),
        ],
        flops=2 * QUARTERS * items * QUARTERS * toks * q,
    )(lanes, *[pltpu.with_memory_space_constraint(v, pltpu.HBM) for v in (tokens, norm_gain.reshape(1, width), routes.T, wg, wu, wd)])
    exchange = lambda v: lax.all_to_all(
        v.reshape(experts, QUARTERS * slots, q), "ep", split_axis=0, concat_axis=0, tiled=True
    ).reshape(QUARTERS * items, q)
    ffn = call(
        functools.partial(ffn_body, slots=slots), wide, [VMEM] * 4,
        [pltpu.VMEM((items, width), BF), pltpu.VMEM((items, ff), BF)], flops=2 * items * width * 3 * ff,
    )
    mine = exchange(outgoing)
    other = swap(mine)
    got = swap(ffn(mine, wg, wu, wd))
    kept = ffn(other, wg, wu, wd)
    table = call(
        functools.partial(table_body, slots=slots, experts=experts), pltpu.VMEM((3 * toks, items), BF),
        [SMEM, VMEM, VMEM], flops=2 * 4 * toks * experts * items,
    )(lanes, routes, gates)
    back = exchange(call(add_body, wide, [VMEM] * 2, flops=QUARTERS * items * q)(kept, got))
    part = call(
        functools.partial(last_body, slots=slots), pltpu.VMEM((toks, width), F32), [VMEM] * 2,
        [pltpu.VMEM((items, width), BF)], flops=2 * 3 * toks * items * width,
    )(table, back)
    return (part + swap(part)).astype(BF)


def solution(mesh):
    return jax.shard_map(
        per_device,
        mesh=mesh,
        in_specs=(
            P(("grp", "ep"), None),
            P(("grp", "ep"), None),
            P(("grp", "ep"), None),
            P(),
            P("ep", None, "tp"),
            P("ep", None, "tp"),
            P("ep", "tp", None),
        ),
        out_specs=P(("grp", "ep"), None),
        check_vma=False,
    )
```

time: 137 us -> 89.9 us (0.66)
  blocking collectives: 67.1 us -> 38.9 us
  local copies, waits for them, and re-layouts: 18.7 us -> 0.2 us
  matrix products: 12 us -> 0 us
  Pallas kernels: 0 us -> 11.4 us
  starting transfers between devices: 7.68 us -> 16.8 us
  waiting for transfers between devices: 26.1 us -> 21.5 us
  other arithmetic: 4.75 us -> 0.69 us
    all_to_all x4 -> x1, blocking collectives: 67.1 us -> 38.9 us  [per_device(): lax.all_to_all(v.reshape(experts, QUARTERS * slots, q), 'ep', split_axis=...]
    dot_general x3 -> x0, matrix products: 12 us -> none  [the longest x1 7.03 us: per_device(): jnp.dot(hidden, w_down[0], preferred_element_type=jnp.float32)]
    pallas_call x0 -> x6, Pallas kernels: none -> 11.4 us  [the longest x1 3.29 us: per_device(): got = swap(ffn(mine, wg, wu, wd))]
    ppermute x0 -> x3, starting transfers between devices: none -> 9.73 us  [per_device(): swap = lambda v: lax.ppermute(v, 'tp', [(0, 1), (1, 0)])]
    all_to_all x1, waiting for transfers between devices: 26.1 us -> 20.3 us  [per_device(): lax.all_to_all(v.reshape(experts, QUARTERS * slots, q), 'ep', split_axis=...]
    reshape x5 -> x0, local copies, waits for them, and re-layouts: 4.52 us -> none  [the longest x1 1.54 us: per_device(): outgoing = outgoing.reshape(ep_count, capacity, width)]
    convert_element_type x2 -> x0, local copies, waits for them, and re-layouts: 3.36 us -> none  [per_device(): summed = sum_at_owner(lax.optimization_barrier(partial_value).astype(jnp....]
    reduce_sum x4 -> x0, other arithmetic: 3.04 us -> none  [the longest x1 1.44 us: sum_at_owner(): return jnp.sum(parts.astype(jnp.float32), axis=0)]
  transfers between devices with their start and end apart: 1 -> 4, of which waited for: 1 -> 2; matrix products, arithmetic and copies ran while one was open for 0% -> 0% of each run, Pallas kernels for 0% -> 8%
where the time goes in v2:
time: 89.9 us; the launch traced here: 89.6 us
  blocking collectives  38.9 us (43%)
  waiting for transfers between devices  21.5 us (24%)
  starting transfers between devices  16.8 us (19%)
  Pallas kernels  11.4 us (13%)
    all_to_all x1, blocking collectives, per_device(): lax.all_to_all(v.reshape(experts, QUARTERS * slots, q), 'ep', split_axis=...  38.9 us
    all_to_all x1, waiting for transfers between devices, per_device(): lax.all_to_all(v.reshape(experts, QUARTERS * slots, q), 'ep', split_axis=...  20.3 us
    ppermute x3, starting transfers between devices, per_device(): swap = lambda v: lax.ppermute(v, 'tp', [(0, 1), (1, 0)])  9.73 us
    all_to_all x1, starting transfers between devices, per_device(): lax.all_to_all(v.reshape(experts, QUARTERS * slots, q), 'ep', split_axis=...  7.11 us
    pallas_call x1, Pallas kernels, per_device(): got = swap(ffn(mine, wg, wu, wd))  3.29 us
    pallas_call x1, Pallas kernels, per_device(): kept = ffn(other, wg, wu, wd)  3.29 us
    pallas_call x1, Pallas kernels, per_device(): call(functools.partial(prep_body, experts=experts, slots=slots), (wide, p...  2.76 us
  transfers between devices with their start and end apart: 4, of which 2 were waited for; matrix products, arithmetic and copies ran while one was open for 0% of the time, Pallas kernels for 8%

profile of v2, /device:TPU:513, one launch (start us, length us, event | category | flops | bytes accessed | tf_op | source)
XLA Modules:
  0.0 89.6 jit_solution(3725974487457172826)
XLA Ops:
  0.0 2.8 %shard_map.74 = (bf16[1536,256]{1,0:T(8,128)(2,1)S(1)}, bf16[1024,896]{1,0:T(8,128)(2,1)S(1)}, bf16[1024,896]{1,0:T(8,128)(2,1)S(1)}, bf16[896,1024]{1,0:T(8,128)(2,1)S(1)}) custom-call(s32[1]{0:T(128)} %bitcast.lane_ref, bf16[64,1024]{1,0:T(8,128)(2,1)} %tok_hbm.1, f32[1,1024]{1,0:T(1,128)} %bitcast.18, s32[4,64]{1,0:T(4,128)} %bitcast.17, ...), custom_call_target="tpu_custom_call" | custom-call | flops 201326592 | tf_op jit(solution)/shard_map/pallas_call | solution.py:198
  2.8 38.9 %all_to_all.10 = bf16[64,24,256]{2,1,0:T(8,128)(2,1)S(1)} all-to-all(bf16[64,24,256]{2,1,0:T(8,128)(2,1)S(1)} %bitcast.13), channel_id=1, replica_groups=mesh['grp'=2,'ep'=64,'tp'=2] {'ep'}, dimensions={0} | all-to-all | bytes 1572864 | tf_op jit(solution)/shard_map/all_to_all | solution.py:211
  41.7 7.1 %collective-permute-start = (bf16[1536,256]{1,0:T(8,128)(2,1)S(1)}, bf16[1536,256]{1,0:T(8,128)(2,1)S(1)}, u32[]{:S(2)}, u32[]{:S(2)}) collective-permute-start(bf16[1536,256]{1,0:T(8,128)(2,1)S(1)} %bitcast.11), channel_id=1, source_target_pairs={{0,1},{1,0},{2,3},{3,2},{4,5},{5,4},{6,7},{7,6},{8,9},{9,8},{10,11... | collective-permute-start | bytes 2359304 | tf_op jit(solution)/shard_map/ppermute | solution.py:194
  48.8 3.3 %shard_map.76 = bf16[1536,256]{1,0:T(8,128)(2,1)S(1)} custom-call(bf16[1536,256]{1,0:T(8,128)(2,1)S(1)} %bitcast.12, bf16[1024,896]{1,0:T(8,128)(2,1)S(1)} %get-tuple-element.10.wg_ref, bf16[1024,896]{1,0:T(8,128)(2,1)S(1)} %get-tuple-element.11.wu_ref, bf16[896,1024]{1,0:T(8,128)(2,1)S(1)} %get-tuple-element.12.wd_ref), custom_call_target="tpu_custom_call" | custom-call | flops 2113929216 | tf_op jit(solution)/shard_map/pallas_call | solution.py:220
  52.1 0.1 collective-permute-start.1
  52.2 0.0 collective-permute-done.x_ref
  52.2 3.3 %shard_map.75.a_ref = bf16[1536,256]{1,0:T(8,128)(2,1)S(1)} custom-call(bf16[1536,256]{1,0:T(8,128)(2,1)S(1)} %collective-permute-done.x_ref, bf16[1024,896]{1,0:T(8,128)(2,1)S(1)} %get-tuple-element.10.wg_ref, bf16[1024,896]{1,0:T(8,128)(2,1)S(1)} %get-tuple-element.11.wu_ref, bf16[896,1024]{1,0:T(8,128)(2,1)S(1)} %get-tuple-element.12.wd_ref), custom_call_target="tpu_custom_call" | custom-call | flops 2113929216 | tf_op jit(solution)/shard_map/pallas_call | solution.py:221
  55.5 0.0 copy-start
  55.5 0.0 copy-start.1
  55.5 0.0 collective-permute-done.1.b_ref
  55.5 1.1 %shard_map.77 = bf16[1536,256]{1,0:T(8,128)(2,1)} custom-call(bf16[1536,256]{1,0:T(8,128)(2,1)S(1)} %shard_map.75.a_ref, bf16[1536,256]{1,0:T(8,128)(2,1)S(1)} %collective-permute-done.1.b_ref), custom_call_target="tpu_custom_call" | custom-call | flops 393216 | tf_op jit(solution)/shard_map/pallas_call | solution.py:226
  56.6 7.1 %all-to-all-start.1 = ((bf16[64,24,256]{2,1,0:T(8,128)(2,1)}), bf16[64,24,256]{2,1,0:T(8,128)(2,1)S(1)}, u32[]{:S(2)}, u32[]{:S(2)}) async-start(bf16[64,24,256]{2,1,0:T(8,128)(2,1)} %bitcast.8), calls=%async_computation.1 | async-start | bytes 1572864 | tf_op jit(solution)/shard_map/all_to_all | solution.py:211
  63.7 0.0 copy-done
  63.7 0.1 copy.8.rt_ref
  63.8 0.0 copy-done.1
  63.8 0.1 copy.9.gt_ref
  63.9 0.4 shard_map.73.mix_ref
  64.4 20.3 %all-to-all-done.1 = bf16[64,24,256]{2,1,0:T(8,128)(2,1)S(1)} async-done(((bf16[64,24,256]{2,1,0:T(8,128)(2,1)}), bf16[64,24,256]{2,1,0:T(8,128)(2,1)S(1)}, u32[]{:S(2)}, u32[]{:S(2)}) %all-to-all-start.1) | async-done | bytes 786464 | tf_op jit(solution)/shard_map/all_to_all | solution.py:211
  84.7 0.6 shard_map.78
  85.3 2.5 %collective-permute-start.2 = (f32[64,1024]{1,0:T(8,128)S(1)}, f32[64,1024]{1,0:T(8,128)S(1)}, u32[]{:S(2)}, u32[]{:S(2)}) collective-permute-start(f32[64,1024]{1,0:T(8,128)S(1)} %shard_map.78), channel_id=1, source_target_pairs={{0,1},{1,0},{2,3},{3,2},{4,5},{5,4},{6,7},{7,6},{8,9},{9,8},{10,11... | collective-permute-start | bytes 786440 | tf_op jit(solution)/shard_map/ppermute | solution.py:194
  87.8 1.2 %collective-permute-done.2 = f32[64,1024]{1,0:T(8,128)S(1)} collective-permute-done((f32[64,1024]{1,0:T(8,128)S(1)}, f32[64,1024]{1,0:T(8,128)S(1)}, u32[]{:S(2)}, u32[]{:S(2)}) %collective-permute-start.2) | collective-permute-done | bytes 262176 | tf_op jit(solution)/shard_map/ppermute | solution.py:194
  89.0 0.7 add_convert_fusion
Async XLA Ops:
  41.7 10.5 %collective-permute-start = (bf16[1536,256]{1,0:T(8,128)(2,1)S(1)}, bf16[1536,256]{1,0:T(8,128)(2,1)S(1)}, u32[]{:S(2)}, u32[]{:S(2)}) collective-permute-start(bf16[1536,256]{1,0:T(8,128)(2,1)S(1)} %bitcast.11), channel_id=1, source_target_pairs={{0,1},{1,0},{2,3},{3,2},{4,5},{5,4},{6,7},{7,6},{8,9},{9,8},{10,11... | collective-permute-start | bytes 2359304 | tf_op jit(solution)/shard_map/ppermute | solution.py:194
  52.1 3.5 %collective-permute-start.1 = (bf16[1536,256]{1,0:T(8,128)(2,1)S(1)}, bf16[1536,256]{1,0:T(8,128)(2,1)S(1)}, u32[]{:S(2)}, u32[]{:S(2)}) collective-permute-start(bf16[1536,256]{1,0:T(8,128)(2,1)S(1)} %shard_map.76), channel_id=1, source_target_pairs={{0,1},{1,0},{2,3},{3,2},{4,5},{5,4},{6,7},{7,6},{8,9},{9,8},{10,11... | collective-permute-start | bytes 2359304 | tf_op jit(solution)/shard_map/ppermute | solution.py:194
  55.5 8.2 %copy-start = (s32[64,4]{0,1:T(4,128)S(1)}, s32[64,4]{0,1:T(4,128)}, u32[]{:S(2)}) copy-start(s32[64,4]{0,1:T(4,128)} %param.8) | copy-start | bytes 3076
  55.5 8.3 %copy-start.1 = (f32[64,4]{0,1:T(4,128)S(1)}, f32[64,4]{0,1:T(4,128)}, u32[]{:S(2)}) copy-start(f32[64,4]{0,1:T(4,128)} %param.9) | copy-start | bytes 3076
  56.6 28.1 %all-to-all-start.1 = ((bf16[64,24,256]{2,1,0:T(8,128)(2,1)}), bf16[64,24,256]{2,1,0:T(8,128)(2,1)S(1)}, u32[]{:S(2)}, u32[]{:S(2)}) async-start(bf16[64,24,256]{2,1,0:T(8,128)(2,1)} %bitcast.8), calls=%async_computation.1 | async-start | bytes 1572864 | tf_op jit(solution)/shard_map/all_to_all | solution.py:211
  85.3 3.7 %collective-permute-start.2 = (f32[64,1024]{1,0:T(8,128)S(1)}, f32[64,1024]{1,0:T(8,128)S(1)}, u32[]{:S(2)}, u32[]{:S(2)}) collective-permute-start(f32[64,1024]{1,0:T(8,128)S(1)} %shard_map.78), channel_id=1, source_target_pairs={{0,1},{1,0},{2,3},{3,2},{4,5},{5,4},{6,7},{7,6},{8,9},{9,8},{10,11... | collective-permute-start | bytes 786440 | tf_op jit(solution)/shard_map/ppermute | solution.py:194

commit v3 on v2

--- a/solution.py
+++ b/solution.py
@@ -46,18 +46,26 @@
     )
 
 
-def prep_body(
-    lane_ref, tok_hbm, gain_hbm, rt_hbm, wg_hbm, wu_hbm, wd_hbm,
-    out_ref, wg_ref, wu_ref, wd_ref,
-    tok_ref, gain_ref, rt_ref, stack_ref, sems, *, experts, slots,
-):
-    pairs = (
-        (tok_hbm, tok_ref), (gain_hbm, gain_ref), (rt_hbm, rt_ref),
-        (wg_hbm, wg_ref), (wu_hbm, wu_ref), (wd_hbm, wd_ref),
-    )
+def start_all(pairs, sems):
     copies = [pltpu.make_async_copy(a, b, sems.at[i]) for i, (a, b) in enumerate(pairs)]
     for c in copies:
         c.start()
+    return copies
+
+
+def prep_body(
+    lane_ref, tok_hbm, gain_hbm, rt_hbm, wg_hbm, wu_hbm,
+    out_ref, wg_ref, wu_ref,
+    tok_ref, gain_ref, rt_ref, stack_ref, sems, *, experts, slots,
+):
+    early = wg_ref.shape[1]
+    copies = start_all(
+        (
+            (rt_hbm, rt_ref), (tok_hbm, tok_ref), (gain_hbm, gain_ref),
+            (wg_hbm.at[:, :early], wg_ref), (wu_hbm.at[:, :early], wu_ref),
+        ),
+        sems,
+    )
     for c in copies[:3]:
         c.wait()
     rows, width = tok_ref.shape
@@ -132,30 +140,67 @@
         out_ref[b * n : (b + 1) * n, :] = dot(perm, stacked).astype(BF)
 
 
-def ffn_body(x_ref, wg_ref, wu_ref, wd_ref, out_ref, rows_ref, hid_ref, *, slots):
+def columns(first_ref, second_ref, n):
+    at = n * 128
+    ref, at = (first_ref, at) if at < first_ref.shape[1] else (second_ref, at - first_ref.shape[1])
+    return ref[:, at : at + 128]
+
+
+def hidden_units(rows, wg1_ref, wu1_ref, wg2_ref, wu2_ref, hid_ref, ready):
+    for n in range(hid_ref.shape[1] // 128):
+        ready(n)
+        w = jnp.concatenate([columns(wg1_ref, wg2_ref, n), columns(wu1_ref, wu2_ref, n)], axis=1)
+        both = dot(rows, w)
+        g, u = both[:, :128], both[:, 128:]
+        hid_ref[:, n * 128 : (n + 1) * 128] = ((0.5 * g) * (1.0 + jnp.tanh(0.5 * g)) * u).astype(BF)
+
+
+def own_body(
+    lane_ref, x_ref, wg1_ref, wu1_ref, wg_hbm, wu_hbm, wd_hbm, rt_hbm, gt_hbm,
+    out_ref, wg2_ref, wu2_ref, wd_ref, mix_ref,
+    rows_ref, hid_ref, rt_ref, gt_ref, sems, *, slots, experts,
+):
+    early, late = wg1_ref.shape[1], wg2_ref.shape[1]
+    pairs = []
+    for at in range(0, late, 128):
+        for hbm, ref in ((wg_hbm, wg2_ref), (wu_hbm, wu2_ref)):
+            pairs.append((hbm.at[:, early + at : early + at + 128], ref.at[:, at : at + 128]))
+    pairs += [(wd_hbm, wd_ref), (rt_hbm, rt_ref), (gt_hbm, gt_ref)]
+    copies = start_all(pairs, sems)
+
+    def ready(n):
+        k = n - early // 128
+        if k >= 0:
+            copies[2 * k].wait()
+            copies[2 * k + 1].wait()
+
     unpack(x_ref, rows_ref, slots)
-    rows = rows_ref[...]
-    for n in range(hid_ref.shape[1] // 128):
-        cols = slice(n * 128, (n + 1) * 128)
-        both = dot(rows, jnp.concatenate([wg_ref[:, cols], wu_ref[:, cols]], axis=1))
-        g, u = both[:, :128], both[:, 128:]
-        hid_ref[:, cols] = ((0.5 * g) * (1.0 + jnp.tanh(0.5 * g)) * u).astype(BF)
-    y = dot(hid_ref[...], wd_ref[...]).astype(BF)
-    pack(y, out_ref, slots)
-
-
-def table_body(lane_ref, rt_ref, gt_ref, mix_ref, *, slots, experts):
-    toks, top = rt_ref.shape
-    e_of = iota((toks, experts), 1)
-    chosen = jnp.zeros((toks, experts), F32)
-    gate = jnp.zeros((toks, experts), F32)
+    hidden_units(rows_ref[...], wg1_ref, wu1_ref, wg2_ref, wu2_ref, hid_ref, ready)
+    for c in copies[-3:]:
+        c.wait()
+    out_ref[...] = dot(hid_ref[...], wd_ref[...]).astype(BF)
+    table(lane_ref, rt_ref[...], gt_ref[...], mix_ref, slots, experts)
+
+
+def other_body(x_ref, wg1_ref, wu1_ref, wg2_ref, wu2_ref, wd_ref, out_ref, rows_ref, hid_ref, *, slots):
+    unpack(x_ref, rows_ref, slots)
+    hidden_units(rows_ref[...], wg1_ref, wu1_ref, wg2_ref, wu2_ref, hid_ref, lambda n: None)
+    out_ref[...] = dot(hid_ref[...], wd_ref[...]).astype(BF)
+
+
+def table(lane_ref, rt, gt, mix_ref, slots, experts):
+    top, toks = rt.shape
+    e_of = iota((experts, toks), 0)
+    chosen = jnp.zeros((experts, toks), F32)
+    gate = jnp.zeros((experts, toks), F32)
     for k in range(top):
-        hit = e_of == rt_ref[:, k : k + 1]
+        hit = e_of == rt[k : k + 1, :]
         chosen = chosen + hit.astype(F32)
-        gate = gate + jnp.where(hit, gt_ref[:, k : k + 1], 0.0)
-    lower = bf(iota((toks, toks), 1) < iota((toks, toks), 0))
-    rel = dot(lower, chosen.astype(BF)) - ((1 - lane_ref[0]) * slots).astype(F32)
-    place = jnp.where((chosen > 0) & (rel >= 0) & (rel < slots), rel, -1.0).astype(BF)
+        gate = gate + jnp.where(hit, gt[k : k + 1, :], 0.0)
+    upper = bf(iota((toks, toks), 0) < iota((toks, toks), 1))
+    rel = dot(chosen.astype(BF), upper) - ((1 - lane_ref[0]) * slots).astype(F32)
+    place = jnp.where((chosen > 0) & (rel >= 0) & (rel < slots), rel, -1.0).T.astype(BF)
+    gate = gate.T
     g1 = gate.astype(BF)
     rest = gate - g1.astype(F32)
     g2 = rest.astype(BF)
@@ -170,8 +215,8 @@
         mix_ref[i * toks : (i + 1) * toks, :] = jnp.where(here, dot(piece, rep), 0.0).astype(BF)
 
 
-def add_body(a_ref, b_ref, out_ref):
-    out_ref[...] = (a_ref[...].astype(F32) + b_ref[...].astype(F32)).astype(BF)
+def add_body(a_ref, b_ref, out_ref, *, slots):
+    pack((a_ref[...].astype(F32) + b_ref[...].astype(F32)).astype(BF), out_ref, slots)
 
 
 def last_body(mix_ref, back_ref, out_ref, rows_ref, *, slots):
@@ -191,43 +236,60 @@
     ff = w_gate.shape[2]
     items = experts * slots
     wide = pltpu.VMEM((QUARTERS * items, q), BF)
+    tall = pltpu.VMEM((items, width), BF)
+    early = ff // 128 * 3 // 7 * 128
+    late = ff - early
     swap = lambda v: lax.ppermute(v, "tp", [(0, 1), (1, 0)])
     lanes = lax.axis_index("tp").astype(jnp.int32).reshape(1)
+    in_hbm = lambda *vs: [pltpu.with_memory_space_constraint(v, pltpu.HBM) for v in vs]
     wg, wu, wd = w_gate[0], w_up[0], w_down[0]
-
-    outgoing, wg, wu, wd = call(
+    rt = routes.T
+
+    outgoing, wg1, wu1 = call(
         functools.partial(prep_body, experts=experts, slots=slots),
-        (wide, pltpu.VMEM(wg.shape, BF), pltpu.VMEM(wu.shape, BF), pltpu.VMEM(wd.shape, BF)),
-        [SMEM] + [HBM] * 6,
+        (wide, pltpu.VMEM((width, early), BF), pltpu.VMEM((width, early), BF)),
+        [SMEM] + [HBM] * 5,
         [
             pltpu.VMEM((toks, width), BF),
             pltpu.VMEM((1, width), F32),
             pltpu.VMEM((top, toks), jnp.int32),
             pltpu.VMEM((QUARTERS * toks, q), BF),
-            pltpu.SemaphoreType.DMA((6,)),
+            pltpu.SemaphoreType.DMA((5,)),
         ],
         flops=2 * QUARTERS * items * QUARTERS * toks * q,
-    )(lanes, *[pltpu.with_memory_space_constraint(v, pltpu.HBM) for v in (tokens, norm_gain.reshape(1, width), routes.T, wg, wu, wd)])
+    )(lanes, *in_hbm(tokens, norm_gain.reshape(1, width), rt, wg, wu))
     exchange = lambda v: lax.all_to_all(
         v.reshape(experts, QUARTERS * slots, q), "ep", split_axis=0, concat_axis=0, tiled=True
     ).reshape(QUARTERS * items, q)
-    ffn = call(
-        functools.partial(ffn_body, slots=slots), wide, [VMEM] * 4,
-        [pltpu.VMEM((items, width), BF), pltpu.VMEM((items, ff), BF)], flops=2 * items * width * 3 * ff,
-    )
     mine = exchange(outgoing)
     other = swap(mine)
-    got = swap(ffn(mine, wg, wu, wd))
-    kept = ffn(other, wg, wu, wd)
-    table = call(
-        functools.partial(table_body, slots=slots, experts=experts), pltpu.VMEM((3 * toks, items), BF),
-        [SMEM, VMEM, VMEM], flops=2 * 4 * toks * experts * items,
-    )(lanes, routes, gates)
-    back = exchange(call(add_body, wide, [VMEM] * 2, flops=QUARTERS * items * q)(kept, got))
+    work = 2 * items * width * 3 * ff
+    held = [pltpu.VMEM((items, width), BF), pltpu.VMEM((items, ff), BF)]
+    sent, wg2, wu2, wd1, mix = call(
+        functools.partial(own_body, slots=slots, experts=experts),
+        (
+            tall, pltpu.VMEM((width, late), BF), pltpu.VMEM((width, late), BF),
+            pltpu.VMEM(wd.shape, BF), pltpu.VMEM((3 * toks, items), BF),
+        ),
+        [SMEM] + [VMEM] * 3 + [HBM] * 5,
+        [
+            *held,
+            pltpu.VMEM((top, toks), jnp.int32),
+            pltpu.VMEM((top, toks), F32),
+            pltpu.SemaphoreType.DMA((late // 128 * 2 + 3,)),
+        ],
+        flops=work,
+    )(lanes, mine, wg1, wu1, *in_hbm(wg, wu, wd, rt, gates.T))
+    got = swap(sent)
+    kept = call(functools.partial(other_body, slots=slots), tall, [VMEM] * 6, held, flops=work)(
+        other, wg1, wu1, wg2, wu2, wd1
+    )
+    summed = call(functools.partial(add_body, slots=slots), wide, [VMEM] * 2, flops=items * width)(kept, got)
+    back = exchange(summed)
     part = call(
         functools.partial(last_body, slots=slots), pltpu.VMEM((toks, width), F32), [VMEM] * 2,
         [pltpu.VMEM((items, width), BF)], flops=2 * 3 * toks * items * width,
-    )(table, back)
+    )(mix, back)
     return (part + swap(part)).astype(BF)
 
 

time: 89.9 us -> 89.1 us (level)
  blocking collectives: 38.9 us -> 66.7 us
  waiting for transfers between devices: 21.5 us -> 1.17 us
  starting transfers between devices: 16.8 us -> 9.72 us
  Pallas kernels: 11.4 us -> 10.5 us
    all_to_all x1 -> x2, blocking collectives: 38.9 us -> 66.7 us  [per_device(): lax.all_to_all(v.reshape(experts, QUARTERS * slots, q), 'ep', split_axis=...]
    all_to_all x1 -> x0, waiting for transfers between devices: 20.3 us -> none  [per_device(): lax.all_to_all(v.reshape(experts, QUARTERS * slots, q), 'ep', split_axis=...]
    all_to_all x1 -> x0, starting transfers between devices: 7.11 us -> none  [per_device(): lax.all_to_all(v.reshape(experts, QUARTERS * slots, q), 'ep', split_axis=...]
    pallas_call x4 -> x3, Pallas kernels: 8.06 us -> 7.97 us  [the longest x1 4.92 us: per_device(): call(functools.partial(own_body, slots=slots, experts=experts), (tall, pl...]
  transfers between devices with their start and end apart: 4 -> 3, of which waited for: 2 -> 1; matrix products, arithmetic and copies ran while one was open for 0% -> 0% of each run, Pallas kernels for 8% -> 9%
where the time goes in v3:
time: 89.1 us; the launch traced here: 88.9 us
  blocking collectives  66.7 us (75%)
  Pallas kernels  10.5 us (12%)
  starting transfers between devices  9.72 us (11%)
  waiting for transfers between devices  1.17 us (1%)
    all_to_all x2, blocking collectives, per_device(): lax.all_to_all(v.reshape(experts, QUARTERS * slots, q), 'ep', split_axis=...  66.7 us
    ppermute x3, starting transfers between devices, per_device(): swap = lambda v: lax.ppermute(v, 'tp', [(0, 1), (1, 0)])  9.72 us
    pallas_call x1, Pallas kernels, per_device(): call(functools.partial(own_body, slots=slots, experts=experts), (tall, pl...  4.92 us
    pallas_call x1, Pallas kernels, per_device(): call(functools.partial(other_body, slots=slots), tall, [VMEM] * 6, held,...  2.64 us
    pallas_call x1, Pallas kernels, per_device(): call(functools.partial(prep_body, experts=experts, slots=slots), (wide, p...  1.97 us
  transfers between devices with their start and end apart: 3, of which 1 were waited for; matrix products, arithmetic and copies ran while one was open for 0% of the time, Pallas kernels for 9%

profile of v3, /device:TPU:513, one launch (start us, length us, event | category | flops | bytes accessed | tf_op | source)
XLA Modules:
  0.0 88.9 jit_solution(10784383940528560836)
XLA Ops:
  0.0 2.0 %shard_map.73 = (bf16[1536,256]{1,0:T(8,128)(2,1)S(1)}, bf16[1024,384]{1,0:T(8,128)(2,1)S(1)}, bf16[1024,384]{1,0:T(8,128)(2,1)S(1)}) custom-call(s32[1]{0:T(128)} %bitcast.lane_ref, bf16[64,1024]{1,0:T(8,128)(2,1)} %tok_hbm.1, f32[1,1024]{1,0:T(1,128)} %bitcast.23, s32[4,64]{1,0:T(4,128)} %bitcast.21, bf16[1024,896]{1,0:T(8,128)(2,1)} %bitcast.16, ...), custom_call_target="tpu_custom_call" | custom-call | flops 201326592 | tf_op jit(solution)/shard_map/pallas_call | solution.py:248
  2.0 38.9 %all_to_all.10 = bf16[64,24,256]{2,1,0:T(8,128)(2,1)S(1)} all-to-all(bf16[64,24,256]{2,1,0:T(8,128)(2,1)S(1)} %bitcast.15), channel_id=1, replica_groups=mesh['grp'=2,'ep'=64,'tp'=2] {'ep'}, dimensions={0} | all-to-all | bytes 1572864 | tf_op jit(solution)/shard_map/all_to_all | solution.py:261
  40.9 7.1 %collective-permute-start = (bf16[1536,256]{1,0:T(8,128)(2,1)S(1)}, bf16[1536,256]{1,0:T(8,128)(2,1)S(1)}, u32[]{:S(2)}, u32[]{:S(2)}) collective-permute-start(bf16[1536,256]{1,0:T(8,128)(2,1)S(1)} %bitcast.11), channel_id=1, source_target_pairs={{0,1},{1,0},{2,3},{3,2},{4,5},{5,4},{6,7},{7,6},{8,9},{9,8},{10,11... | collective-permute-start | bytes 2359304 | tf_op jit(solution)/shard_map/ppermute | solution.py:242
  48.0 4.9 %shard_map.74 = (bf16[384,1024]{1,0:T(8,128)(2,1)S(1)}, bf16[1024,512]{1,0:T(8,128)(2,1)S(1)}, bf16[1024,512]{1,0:T(8,128)(2,1)S(1)}, bf16[896,1024]{1,0:T(8,128)(2,1)S(1)}, bf16[192,384]{1,0:T(8,128)(2,1)S(1)}) custom-call(s32[1]{0:T(128)} %bitcast.lane_ref, bf16[1536,256]{1,0:T(8,128)(2,1)S(1)} %bitcast.12, ...), custom_call_target="tpu_custom_call" | custom-call | flops 2113929216 | tf_op jit(solution)/shard_map/pallas_call | solution.py:268
  52.9 0.1 collective-permute-start.1
  53.0 0.0 collective-permute-done.x_ref
  53.0 2.6 %shard_map.75.a_ref = bf16[384,1024]{1,0:T(8,128)(2,1)S(1)} custom-call(bf16[1536,256]{1,0:T(8,128)(2,1)S(1)} %collective-permute-done.x_ref, bf16[1024,384]{1,0:T(8,128)(2,1)S(1)} %get-tuple-element.14.wg1_ref, bf16[1024,384]{1,0:T(8,128)(2,1)S(1)} %get-tuple-element.15.wu1_ref, bf16[1024,512]{1,0:T(8,128)(2,1)S(1)} %get-tuple-element.17.wg2_ref, ...), custom_call_target="tpu_custom_call" | custom-call | flops 2113929216 | tf_op jit(solution)/shard_map/pallas_call | solution.py:284
  55.7 0.0 collective-permute-done.1.b_ref
  55.7 0.4 shard_map.76
  56.1 27.8 %all_to_all.11 = bf16[64,24,256]{2,1,0:T(8,128)(2,1)S(1)} all-to-all(bf16[64,24,256]{2,1,0:T(8,128)(2,1)S(1)} %bitcast.14), channel_id=1, replica_groups=mesh['grp'=2,'ep'=64,'tp'=2] {'ep'}, dimensions={0} | all-to-all | bytes 1572864 | tf_op jit(solution)/shard_map/all_to_all | solution.py:261
  84.0 0.6 shard_map.77
  84.6 2.5 %collective-permute-start.2 = (f32[64,1024]{1,0:T(8,128)S(1)}, f32[64,1024]{1,0:T(8,128)S(1)}, u32[]{:S(2)}, u32[]{:S(2)}) collective-permute-start(f32[64,1024]{1,0:T(8,128)S(1)} %shard_map.77), channel_id=1, source_target_pairs={{0,1},{1,0},{2,3},{3,2},{4,5},{5,4},{6,7},{7,6},{8,9},{9,8},{10,11... | collective-permute-start | bytes 786440 | tf_op jit(solution)/shard_map/ppermute | solution.py:242
  87.1 1.2 %collective-permute-done.2 = f32[64,1024]{1,0:T(8,128)S(1)} collective-permute-done((f32[64,1024]{1,0:T(8,128)S(1)}, f32[64,1024]{1,0:T(8,128)S(1)}, u32[]{:S(2)}, u32[]{:S(2)}) %collective-permute-start.2) | collective-permute-done | bytes 262176 | tf_op jit(solution)/shard_map/ppermute | solution.py:242
  88.2 0.7 add_convert_fusion
Async XLA Ops:
  40.9 12.2 %collective-permute-start = (bf16[1536,256]{1,0:T(8,128)(2,1)S(1)}, bf16[1536,256]{1,0:T(8,128)(2,1)S(1)}, u32[]{:S(2)}, u32[]{:S(2)}) collective-permute-start(bf16[1536,256]{1,0:T(8,128)(2,1)S(1)} %bitcast.11), channel_id=1, source_target_pairs={{0,1},{1,0},{2,3},{3,2},{4,5},{5,4},{6,7},{7,6},{8,9},{9,8},{10,11... | collective-permute-start | bytes 2359304 | tf_op jit(solution)/shard_map/ppermute | solution.py:242
  52.9 2.8 %collective-permute-start.1 = (bf16[384,1024]{1,0:T(8,128)(2,1)S(1)}, bf16[384,1024]{1,0:T(8,128)(2,1)S(1)}, u32[]{:S(2)}, u32[]{:S(2)}) collective-permute-start(bf16[384,1024]{1,0:T(8,128)(2,1)S(1)} %get-tuple-element.20), channel_id=1, source_target_pairs={{0,1},{1,0},{2,3},{3,2},{4,5},{5,4},{6,7},{7,6},{8,9},{9,8},{10,11... | collective-permute-start | bytes 2359304 | tf_op jit(solution)/shard_map/ppermute | solution.py:242
  84.6 3.7 %collective-permute-start.2 = (f32[64,1024]{1,0:T(8,128)S(1)}, f32[64,1024]{1,0:T(8,128)S(1)}, u32[]{:S(2)}, u32[]{:S(2)}) collective-permute-start(f32[64,1024]{1,0:T(8,128)S(1)} %shard_map.77), channel_id=1, source_target_pairs={{0,1},{1,0},{2,3},{3,2},{4,5},{5,4},{6,7},{7,6},{8,9},{9,8},{10,11... | collective-permute-start | bytes 786440 | tf_op jit(solution)/shard_map/ppermute | solution.py:242

commit v4 on v3

--- a/solution.py
+++ b/solution.py
@@ -75,20 +75,17 @@
     normed = (xf * lax.rsqrt(var + EPS) * gain_ref[...]).astype(BF)
     for h in range(QUARTERS):
         stack_ref[h * rows : (h + 1) * rows, :] = normed[:, h * q : (h + 1) * q]
-    rt = rt_ref[...]
-    e_of = iota((experts, rows), 0)
-    chosen = jnp.zeros((experts, rows), F32)
+    wide = QUARTERS * rows
+    rt = jnp.concatenate([rt_ref[...]] * QUARTERS, axis=1)
+    e_of = iota((experts, wide), 0)
+    chosen = jnp.zeros((experts, wide), F32)
     for k in range(rt.shape[0]):
         chosen = chosen + (e_of == rt[k : k + 1, :]).astype(F32)
-    upper = bf(iota((rows, rows), 0) < iota((rows, rows), 1))
-    rel = dot(chosen.astype(BF), upper) - (lane_ref[0] * slots).astype(F32)
-    place = jnp.where((chosen > 0) & (rel >= 0) & (rel < slots), rel, -1.0).astype(BF)
-    wide = QUARTERS * rows
     t2 = iota((rows, wide), 1)
-    quarter = div_const(t2, rows)
-    spread = dot(place, bf(t2 - quarter * rows == iota((rows, wide), 0)))
+    upper = bf(iota((rows, wide), 0) < t2 - div_const(t2, rows) * rows)
+    rel = dot(chosen[:, :rows].astype(BF), upper) - (lane_ref[0] * slots).astype(F32)
     quarter = div_const(iota((experts, wide), 1), rows).astype(F32)
-    code = jnp.where(spread >= 0, spread + 16.0 * quarter, -1.0).astype(BF)
+    code = jnp.where((chosen > 0) & (rel >= 0) & (rel < slots), rel + 16.0 * quarter, -1.0).astype(BF)
     message = QUARTERS * slots
     block = GROUP * message
     r = iota((block, wide), 0)
@@ -156,34 +153,31 @@
 
 
 def own_body(
-    lane_ref, x_ref, wg1_ref, wu1_ref, wg_hbm, wu_hbm, wd_hbm, rt_hbm, gt_hbm,
-    out_ref, wg2_ref, wu2_ref, wd_ref, mix_ref,
-    rows_ref, hid_ref, rt_ref, gt_ref, sems, *, slots, experts,
+    x_ref, wg1_ref, wu1_ref, wg_hbm, wu_hbm, wd_hbm,
+    out_ref, wg2_ref, wu2_ref, wd_ref, rows_ref, hid_ref, sems, *, slots,
 ):
-    early, late = wg1_ref.shape[1], wg2_ref.shape[1]
-    pairs = []
-    for at in range(0, late, 128):
-        for hbm, ref in ((wg_hbm, wg2_ref), (wu_hbm, wu2_ref)):
-            pairs.append((hbm.at[:, early + at : early + at + 128], ref.at[:, at : at + 128]))
-    pairs += [(wd_hbm, wd_ref), (rt_hbm, rt_ref), (gt_hbm, gt_ref)]
-    copies = start_all(pairs, sems)
+    early = wg1_ref.shape[1]
+    copies = start_all(
+        ((wg_hbm.at[:, early:], wg2_ref), (wu_hbm.at[:, early:], wu2_ref), (wd_hbm, wd_ref)), sems
+    )
 
     def ready(n):
-        k = n - early // 128
-        if k >= 0:
-            copies[2 * k].wait()
-            copies[2 * k + 1].wait()
+        if n * 128 == early:
+            copies[0].wait()
+            copies[1].wait()
 
     unpack(x_ref, rows_ref, slots)
     hidden_units(rows_ref[...], wg1_ref, wu1_ref, wg2_ref, wu2_ref, hid_ref, ready)
-    for c in copies[-3:]:
-        c.wait()
+    copies[2].wait()
     out_ref[...] = dot(hid_ref[...], wd_ref[...]).astype(BF)
+
+
+def other_body(
+    lane_ref, x_ref, wg1_ref, wu1_ref, wg2_ref, wu2_ref, wd_ref, rt_ref, gt_ref,
+    out_ref, mix_ref, rows_ref, hid_ref, *, slots, experts,
+):
+    unpack(x_ref, rows_ref, slots)
     table(lane_ref, rt_ref[...], gt_ref[...], mix_ref, slots, experts)
-
-
-def other_body(x_ref, wg1_ref, wu1_ref, wg2_ref, wu2_ref, wd_ref, out_ref, rows_ref, hid_ref, *, slots):
-    unpack(x_ref, rows_ref, slots)
     hidden_units(rows_ref[...], wg1_ref, wu1_ref, wg2_ref, wu2_ref, hid_ref, lambda n: None)
     out_ref[...] = dot(hid_ref[...], wd_ref[...]).astype(BF)
 
@@ -237,7 +231,7 @@
     items = experts * slots
     wide = pltpu.VMEM((QUARTERS * items, q), BF)
     tall = pltpu.VMEM((items, width), BF)
-    early = ff // 128 * 3 // 7 * 128
+    early = ff // 128 * 5 // 7 * 128
     late = ff - early
     swap = lambda v: lax.ppermute(v, "tp", [(0, 1), (1, 0)])
     lanes = lax.axis_index("tp").astype(jnp.int32).reshape(1)
@@ -265,25 +259,16 @@
     other = swap(mine)
     work = 2 * items * width * 3 * ff
     held = [pltpu.VMEM((items, width), BF), pltpu.VMEM((items, ff), BF)]
-    sent, wg2, wu2, wd1, mix = call(
-        functools.partial(own_body, slots=slots, experts=experts),
-        (
-            tall, pltpu.VMEM((width, late), BF), pltpu.VMEM((width, late), BF),
-            pltpu.VMEM(wd.shape, BF), pltpu.VMEM((3 * toks, items), BF),
-        ),
-        [SMEM] + [VMEM] * 3 + [HBM] * 5,
-        [
-            *held,
-            pltpu.VMEM((top, toks), jnp.int32),
-            pltpu.VMEM((top, toks), F32),
-            pltpu.SemaphoreType.DMA((late // 128 * 2 + 3,)),
-        ],
-        flops=work,
-    )(lanes, mine, wg1, wu1, *in_hbm(wg, wu, wd, rt, gates.T))
+    sent, wg2, wu2, wd1 = call(
+        functools.partial(own_body, slots=slots),
+        (tall, pltpu.VMEM((width, late), BF), pltpu.VMEM((width, late), BF), pltpu.VMEM(wd.shape, BF)),
+        [VMEM] * 3 + [HBM] * 3, [*held, pltpu.SemaphoreType.DMA((3,))], flops=work,
+    )(mine, wg1, wu1, *in_hbm(wg, wu, wd))
     got = swap(sent)
-    kept = call(functools.partial(other_body, slots=slots), tall, [VMEM] * 6, held, flops=work)(
-        other, wg1, wu1, wg2, wu2, wd1
-    )
+    kept, mix = call(
+        functools.partial(other_body, slots=slots, experts=experts),
+        (tall, pltpu.VMEM((3 * toks, items), BF)), [SMEM] + [VMEM] * 8, held, flops=work,
+    )(lanes, other, wg1, wu1, wg2, wu2, wd1, rt, gates.T)
     summed = call(functools.partial(add_body, slots=slots), wide, [VMEM] * 2, flops=items * width)(kept, got)
     back = exchange(summed)
     part = call(

time: 89.1 us -> 87.5 us (0.982)
  Pallas kernels: 10.5 us -> 8.88 us
    pallas_call x2, Pallas kernels: 7.56 us -> 5.92 us  [the longest x1 3.01 us: per_device(): call(functools.partial(own_body, slots=slots), (tall, pltpu.VMEM((width,...]
  transfers between devices with their start and end apart: 3 -> 3, of which waited for: 1 -> 1; matrix products, arithmetic and copies ran while one was open for 0% -> 0% of each run, Pallas kernels for 9% -> 7%
where the time goes in v4:
time: 87.5 us; the launch traced here: 87.3 us
  blocking collectives  66.8 us (76%)
  starting transfers between devices  9.7 us (11%)
  Pallas kernels  8.88 us (10%)
  waiting for transfers between devices  1.17 us (1%)
    all_to_all x2, blocking collectives, per_device(): lax.all_to_all(v.reshape(experts, QUARTERS * slots, q), 'ep', split_axis=...  66.8 us
    ppermute x3, starting transfers between devices, per_device(): swap = lambda v: lax.ppermute(v, 'tp', [(0, 1), (1, 0)])  9.7 us
    pallas_call x1, Pallas kernels, per_device(): call(functools.partial(own_body, slots=slots), (tall, pltpu.VMEM((width,...  3.01 us
    pallas_call x1, Pallas kernels, per_device(): call(functools.partial(other_body, slots=slots, experts=experts), (tall,...  2.91 us
    pallas_call x1, Pallas kernels, per_device(): call(functools.partial(prep_body, experts=experts, slots=slots), (wide, p...  1.94 us
  transfers between devices with their start and end apart: 3, of which 1 were waited for; matrix products, arithmetic and copies ran while one was open for 0% of the time, Pallas kernels for 7%

profile of v4, /device:TPU:513, one launch (start us, length us, event | category | flops | bytes accessed | tf_op | source)
XLA Modules:
  0.0 87.3 jit_solution(7412848183726414095)
XLA Ops:
  0.0 1.9 %shard_map.73 = (bf16[1536,256]{1,0:T(8,128)(2,1)S(1)}, bf16[1024,640]{1,0:T(8,128)(2,1)S(1)}, bf16[1024,640]{1,0:T(8,128)(2,1)S(1)}) custom-call(s32[1]{0:T(128)} %bitcast.lane_ref, bf16[64,1024]{1,0:T(8,128)(2,1)} %tok_hbm.1, f32[1,1024]{1,0:T(1,128)} %bitcast.24, s32[4,64]{1,0:T(4,128)} %bitcast.16, bf16[1024,896]{1,0:T(8,128)(2,1)} %bitcast.19, ...), custom_call_target="tpu_custom_call" | custom-call | flops 201326592 | tf_op jit(solution)/shard_map/pallas_call | solution.py:242
  2.0 38.9 %all_to_all.10 = bf16[64,24,256]{2,1,0:T(8,128)(2,1)S(1)} all-to-all(bf16[64,24,256]{2,1,0:T(8,128)(2,1)S(1)} %bitcast.15), channel_id=1, replica_groups=mesh['grp'=2,'ep'=64,'tp'=2] {'ep'}, dimensions={0} | all-to-all | bytes 1572864 | tf_op jit(solution)/shard_map/all_to_all | solution.py:255
  40.8 7.1 %collective-permute-start = (bf16[1536,256]{1,0:T(8,128)(2,1)S(1)}, bf16[1536,256]{1,0:T(8,128)(2,1)S(1)}, u32[]{:S(2)}, u32[]{:S(2)}) collective-permute-start(bf16[1536,256]{1,0:T(8,128)(2,1)S(1)} %bitcast.11), channel_id=1, source_target_pairs={{0,1},{1,0},{2,3},{3,2},{4,5},{5,4},{6,7},{7,6},{8,9},{9,8},{10,11... | collective-permute-start | bytes 2359304 | tf_op jit(solution)/shard_map/ppermute | solution.py:236
  47.9 0.0 copy-start
  47.9 0.0 copy-start.1
  47.9 3.0 %shard_map.74 = (bf16[384,1024]{1,0:T(8,128)(2,1)S(1)}, bf16[1024,256]{1,0:T(8,128)(2,1)S(1)}, bf16[1024,256]{1,0:T(8,128)(2,1)S(1)}, bf16[896,1024]{1,0:T(8,128)(2,1)S(1)}) custom-call(bf16[1536,256]{1,0:T(8,128)(2,1)S(1)} %bitcast.12, bf16[1024,640]{1,0:T(8,128)(2,1)S(1)} %get-tuple-element.15.wg1_ref, bf16[1024,640]{1,0:T(8,128)(2,1)S(1)} %get-tuple-element.16.wu1_ref, ...), custom_call_target="tpu_custom_call" | custom-call | flops 2113929216 | tf_op jit(solution)/shard_map/pallas_call | solution.py:262
  51.0 0.1 collective-permute-start.1
  51.1 0.0 collective-permute-done.x_ref
  51.1 0.0 copy-done
  51.1 0.0 copy-done.1
  51.1 2.9 %shard_map.75 = (bf16[384,1024]{1,0:T(8,128)(2,1)S(1)}, bf16[192,384]{1,0:T(8,128)(2,1)S(1)}) custom-call(s32[1]{0:T(128)} %bitcast.lane_ref, bf16[1536,256]{1,0:T(8,128)(2,1)S(1)} %collective-permute-done.x_ref, bf16[1024,640]{1,0:T(8,128)(2,1)S(1)} %get-tuple-element.15.wg1_ref, bf16[1024,640]{1,0:T(8,128)(2,1)S(1)} %get-tuple-element.16.wu1_ref, ...), custom_call_target="tpu_custom_call" | custom-call | flops 2113929216 | tf_op jit(solution)/shard_map/pallas_call | solution.py:268
  54.1 0.0 collective-permute-done.1.b_ref
  54.1 0.4 shard_map.76
  54.5 27.9 %all_to_all.11 = bf16[64,24,256]{2,1,0:T(8,128)(2,1)S(1)} all-to-all(bf16[64,24,256]{2,1,0:T(8,128)(2,1)S(1)} %bitcast.14), channel_id=1, replica_groups=mesh['grp'=2,'ep'=64,'tp'=2] {'ep'}, dimensions={0} | all-to-all | bytes 1572864 | tf_op jit(solution)/shard_map/all_to_all | solution.py:255
  82.4 0.6 shard_map.77
  83.0 2.5 %collective-permute-start.2 = (f32[64,1024]{1,0:T(8,128)S(1)}, f32[64,1024]{1,0:T(8,128)S(1)}, u32[]{:S(2)}, u32[]{:S(2)}) collective-permute-start(f32[64,1024]{1,0:T(8,128)S(1)} %shard_map.77), channel_id=1, source_target_pairs={{0,1},{1,0},{2,3},{3,2},{4,5},{5,4},{6,7},{7,6},{8,9},{9,8},{10,11... | collective-permute-start | bytes 786440 | tf_op jit(solution)/shard_map/ppermute | solution.py:236
  85.5 1.2 %collective-permute-done.2 = f32[64,1024]{1,0:T(8,128)S(1)} collective-permute-done((f32[64,1024]{1,0:T(8,128)S(1)}, f32[64,1024]{1,0:T(8,128)S(1)}, u32[]{:S(2)}, u32[]{:S(2)}) %collective-permute-start.2) | collective-permute-done | bytes 262176 | tf_op jit(solution)/shard_map/ppermute | solution.py:236
  86.6 0.7 add_convert_fusion
Async XLA Ops:
  40.8 10.3 %collective-permute-start = (bf16[1536,256]{1,0:T(8,128)(2,1)S(1)}, bf16[1536,256]{1,0:T(8,128)(2,1)S(1)}, u32[]{:S(2)}, u32[]{:S(2)}) collective-permute-start(bf16[1536,256]{1,0:T(8,128)(2,1)S(1)} %bitcast.11), channel_id=1, source_target_pairs={{0,1},{1,0},{2,3},{3,2},{4,5},{5,4},{6,7},{7,6},{8,9},{9,8},{10,11... | collective-permute-start | bytes 2359304 | tf_op jit(solution)/shard_map/ppermute | solution.py:236
  47.9 3.2 %copy-start = (s32[64,4]{0,1:T(4,128)S(1)}, s32[64,4]{0,1:T(4,128)}, u32[]{:S(2)}) copy-start(s32[64,4]{0,1:T(4,128)} %param.8) | copy-start | bytes 3076
  47.9 3.2 %copy-start.1 = (f32[64,4]{0,1:T(4,128)S(1)}, f32[64,4]{0,1:T(4,128)}, u32[]{:S(2)}) copy-start(f32[64,4]{0,1:T(4,128)} %param.9) | copy-start | bytes 3076
  51.0 3.1 %collective-permute-start.1 = (bf16[384,1024]{1,0:T(8,128)(2,1)S(1)}, bf16[384,1024]{1,0:T(8,128)(2,1)S(1)}, u32[]{:S(2)}, u32[]{:S(2)}) collective-permute-start(bf16[384,1024]{1,0:T(8,128)(2,1)S(1)} %get-tuple-element.22), channel_id=1, source_target_pairs={{0,1},{1,0},{2,3},{3,2},{4,5},{5,4},{6,7},{7,6},{8,9},{9,8},{10,11... | collective-permute-start | bytes 2359304 | tf_op jit(solution)/shard_map/ppermute | solution.py:236
  83.0 3.6 %collective-permute-start.2 = (f32[64,1024]{1,0:T(8,128)S(1)}, f32[64,1024]{1,0:T(8,128)S(1)}, u32[]{:S(2)}, u32[]{:S(2)}) collective-permute-start(f32[64,1024]{1,0:T(8,128)S(1)} %shard_map.77), channel_id=1, source_target_pairs={{0,1},{1,0},{2,3},{3,2},{4,5},{5,4},{6,7},{7,6},{8,9},{9,8},{10,11... | collective-permute-start | bytes 786440 | tf_op jit(solution)/shard_map/ppermute | solution.py:236

commit v5 on v4

v5 whole, which is shorter than its diff:
```python
import functools

import jax
import jax.numpy as jnp
from jax import lax
from jax.experimental import pallas as pl
from jax.experimental.pallas import tpu as pltpu
from jax.sharding import PartitionSpec as P

EPS = 1e-06
BF = jnp.bfloat16
F32 = jnp.float32
VMEM = pl.BlockSpec(memory_space=pltpu.VMEM)
SMEM = pl.BlockSpec(memory_space=pltpu.SMEM)
HBM = pl.BlockSpec(memory_space=pltpu.HBM)
LIMIT = 16 * 1024 * 1024


def dot(a, b):
    return jnp.dot(a, b, preferred_element_type=F32)


def iota(shape, dim):
    return lax.broadcasted_iota(jnp.int32, shape, dim)


def div_const(x, n):
    return (x * (-(-(1 << 17) // n))) >> 17


def bf(mask):
    return jnp.where(mask, 1.0, 0.0).astype(BF)


def flat(ref):
    pairs, two, width = ref.shape
    return ref[...].reshape(pairs * two, width)


def call(body, outs, in_specs, scratch=(), flops=0):
    return pl.pallas_call(
        body,
        out_shape=outs,
        in_specs=in_specs,
        out_specs=jax.tree.map(lambda _: VMEM, outs),
        scratch_shapes=list(scratch),
        compiler_params=pltpu.CompilerParams(vmem_limit_bytes=LIMIT),
        cost_estimate=pl.CostEstimate(flops=flops, bytes_accessed=0, transcendentals=0),
    )


def start_all(pairs, sems):
    copies = [pltpu.make_async_copy(a, b, sems.at[i]) for i, (a, b) in enumerate(pairs)]
    for c in copies:
        c.start()
    return copies


def slot_of(chosen, core, slots):
    toks = chosen.shape[1]
    upper = bf(iota((toks, toks), 0) < iota((toks, toks), 1))
    rel = dot(chosen.astype(BF), upper) - (core * slots).astype(F32)
    return jnp.where((chosen > 0) & (rel >= 0) & (rel < slots), rel, -1.0)


def prep_body(
    lane_ref, tok_hbm, gain_hbm, rt_hbm, wg_hbm, wu_hbm,
    out_ref, wg_ref, wu_ref,
    tok_ref, gain_ref, rt_ref, sems, *, experts, slots,
):
    early = wg_ref.shape[1]
    copies = start_all(
        (
            (rt_hbm, rt_ref), (tok_hbm, tok_ref), (gain_hbm, gain_ref),
            (wg_hbm.at[:, :early], wg_ref), (wu_hbm.at[:, :early], wu_ref),
        ),
        sems,
    )
    for c in copies[:3]:
        c.wait()
    toks = tok_ref.shape[0]
    xf = tok_ref[...].astype(F32)
    var = jnp.mean(xf * xf, axis=-1, keepdims=True)
    normed = (xf * lax.rsqrt(var + EPS) * gain_ref[...]).astype(BF)
    e_of = iota((experts, toks), 0)
    chosen = jnp.zeros((experts, toks), F32)
    for k in range(rt_ref.shape[0]):
        chosen = chosen + (e_of == rt_ref[k : k + 1, :]).astype(F32)
    place = slot_of(chosen, lane_ref[0], slots).astype(BF)
    n = slots * experts
    e_row = div_const(iota((n, experts), 0), slots)
    r = iota((n, toks), 0)
    slot = (r - div_const(r, slots) * slots).astype(F32)
    one = bf(dot(bf(iota((n, experts), 1) == e_row), place) == slot)
    out_ref[...] = dot(one, normed).astype(BF).reshape(out_ref.shape)
    for c in copies[3:]:
        c.wait()


def columns(first_ref, second_ref, n):
    at = n * 128
    ref, at = (first_ref, at) if at < first_ref.shape[1] else (second_ref, at - first_ref.shape[1])
    return ref[:, at : at + 128]


def hidden_units(rows, wg1_ref, wu1_ref, wg2_ref, wu2_ref, hid_ref, ready):
    for n in range(hid_ref.shape[1] // 128):
        ready(n)
        w = jnp.concatenate([columns(wg1_ref, wg2_ref, n), columns(wu1_ref, wu2_ref, n)], axis=1)
        both = dot(rows, w)
        g, u = both[:, :128], both[:, 128:]
        hid_ref[:, n * 128 : (n + 1) * 128] = ((0.5 * g) * (1.0 + jnp.tanh(0.5 * g)) * u).astype(BF)


def own_body(
    x_ref, wg1_ref, wu1_ref, wg_hbm, wu_hbm, wd_hbm, out_ref, wg2_ref, wu2_ref, wd_ref, hid_ref, sems
):
    early = wg1_ref.shape[1]
    copies = start_all(
        ((wg_hbm.at[:, early:], wg2_ref), (wu_hbm.at[:, early:], wu2_ref), (wd_hbm, wd_ref)), sems
    )

    def ready(n):
        if n * 128 == early:
            copies[0].wait()
            copies[1].wait()

    hidden_units(flat(x_ref), wg1_ref, wu1_ref, wg2_ref, wu2_ref, hid_ref, ready)
    copies[2].wait()
    out_ref[...] = dot(hid_ref[...], wd_ref[...]).astype(BF)


def other_body(
    lane_ref, x_ref, wg1_ref, wu1_ref, wg2_ref, wu2_ref, wd_ref, rt_ref, gt_ref,
    out_ref, mix_ref, hid_ref, *, slots, experts,
):
    table(lane_ref, rt_ref[...], gt_ref[...], mix_ref, slots, experts)
    hidden_units(flat(x_ref), wg1_ref, wu1_ref, wg2_ref, wu2_ref, hid_ref, lambda n: None)
    out_ref[...] = dot(hid_ref[...], wd_ref[...]).astype(BF)


def table(lane_ref, rt, gt, mix_ref, slots, experts):
    top, toks = rt.shape
    e_of = iota((experts, toks), 0)
    chosen = jnp.zeros((experts, toks), F32)
    gate = jnp.zeros((experts, toks), F32)
    for k in range(top):
        hit = e_of == rt[k : k + 1, :]
        chosen = chosen + hit.astype(F32)
        gate = gate + jnp.where(hit, gt[k : k + 1, :], 0.0)
    place = slot_of(chosen, 1 - lane_ref[0], slots).T.astype(BF)
    gate = gate.T
    g1 = gate.astype(BF)
    rest = gate - g1.astype(F32)
    g2 = rest.astype(BF)
    g3 = (rest - g2.astype(F32)).astype(BF)
    n = slots * experts
    r = iota((1, n), 1)
    e_r = div_const(r, slots)
    slot = (r - e_r * slots).astype(F32)
    rep = bf(iota((experts, n), 0) == e_r)
    here = dot(place, rep) == slot
    for i, piece in enumerate((g1, g2, g3)):
        mix_ref[i * toks : (i + 1) * toks, :] = jnp.where(here, dot(piece, rep), 0.0).astype(BF)


def add_body(a_ref, b_ref, out_ref):
    total = a_ref[...].astype(F32) + b_ref[...].astype(F32)
    out_ref[...] = total.astype(BF).reshape(out_ref.shape)


def last_body(mix_ref, back_ref, out_ref):
    toks = out_ref.shape[0]
    s = dot(mix_ref[...], flat(back_ref))
    out_ref[...] = s[:toks] + s[toks : 2 * toks] + s[2 * toks :]


def per_device(tokens, routes, gates, norm_gain, w_gate, w_up, w_down):
    toks, width = tokens.shape
    top = routes.shape[1]
    experts = lax.axis_size("ep")
    cap = max(2, min(toks, 3 * toks * top // experts))
    slots = -(-cap // 4) * 2
    ff = w_gate.shape[2]
    items = experts * slots
    pairs = pltpu.VMEM((items // 2, 2, width), BF)
    tall = pltpu.VMEM((items, width), BF)
    early = ff // 128 * 5 // 7 * 128
    late = ff - early
    swap = lambda v: lax.ppermute(v, "tp", [(0, 1), (1, 0)])
    lanes = lax.axis_index("tp").astype(jnp.int32).reshape(1)
    in_hbm = lambda *vs: [pltpu.with_memory_space_constraint(v, pltpu.HBM) for v in vs]
    wg, wu, wd = w_gate[0], w_up[0], w_down[0]
    rt = routes.T

    outgoing, wg1, wu1 = call(
        functools.partial(prep_body, experts=experts, slots=slots),
        (pairs, pltpu.VMEM((width, early), BF), pltpu.VMEM((width, early), BF)),
        [SMEM] + [HBM] * 5,
        [
            pltpu.VMEM((toks, width), BF),
            pltpu.VMEM((1, width), F32),
            pltpu.VMEM((top, toks), jnp.int32),
            pltpu.SemaphoreType.DMA((5,)),
        ],
        flops=2 * items * toks * width,
    )(lanes, *in_hbm(tokens, norm_gain.reshape(1, width), rt, wg, wu))
    exchange = lambda v: lax.all_to_all(
        v.reshape(experts, slots // 2, 2, width), "ep", split_axis=0, concat_axis=0, tiled=True
    ).reshape(v.shape)
    mine = exchange(outgoing)
    other = swap(mine)
    work = 2 * items * width * 3 * ff
    held = pltpu.VMEM((items, ff), BF)
    sent, wg2, wu2, wd1 = call(
        own_body,
        (tall, pltpu.VMEM((width, late), BF), pltpu.VMEM((width, late), BF), pltpu.VMEM(wd.shape, BF)),
        [VMEM] * 3 + [HBM] * 3, [held, pltpu.SemaphoreType.DMA((3,))], flops=work,
    )(mine, wg1, wu1, *in_hbm(wg, wu, wd))
    got = swap(sent)
    kept, mix = call(
        functools.partial(other_body, slots=slots, experts=experts),
        (tall, pltpu.VMEM((3 * toks, items), BF)), [SMEM] + [VMEM] * 8, [held], flops=work,
    )(lanes, other, wg1, wu1, wg2, wu2, wd1, rt, gates.T)
    back = exchange(call(add_body, pairs, [VMEM] * 2, flops=items * width)(kept, got))
    part = call(
        last_body, pltpu.VMEM((toks, width), F32), [VMEM] * 2, flops=2 * 3 * toks * items * width
    )(mix, back)
    return (part + swap(part)).astype(BF)


def solution(mesh):
    return jax.shard_map(
        per_device,
        mesh=mesh,
        in_specs=(
            P(("grp", "ep"), None),
            P(("grp", "ep"), None),
            P(("grp", "ep"), None),
            P(),
            P("ep", None, "tp"),
            P("ep", None, "tp"),
            P("ep", "tp", None),
        ),
        out_specs=P(("grp", "ep"), None),
        check_vma=False,
    )
```

time: 87.5 us -> 86.8 us (level)
  transfers between devices with their start and end apart: 3 -> 3, of which waited for: 1 -> 1; matrix products, arithmetic and copies ran while one was open for 0% -> 0% of each run, Pallas kernels for 7% -> 6%
where the time goes in v5:
time: 86.8 us; the launch traced here: 86.5 us
  blocking collectives  66.8 us (77%)
  starting transfers between devices  9.7 us (11%)
  Pallas kernels  8.11 us (9%)
  waiting for transfers between devices  1.17 us (1%)
    all_to_all x2, blocking collectives, per_device(): lax.all_to_all(v.reshape(experts, slots // 2, 2, width), 'ep', split_axis...  66.8 us
    ppermute x3, starting transfers between devices, per_device(): swap = lambda v: lax.ppermute(v, 'tp', [(0, 1), (1, 0)])  9.7 us
    pallas_call x1, Pallas kernels, per_device(): call(own_body, (tall, pltpu.VMEM((width, late), BF), pltpu.VMEM((width, l...  2.89 us
    pallas_call x1, Pallas kernels, per_device(): call(functools.partial(other_body, slots=slots, experts=experts), (tall,...  2.69 us
    pallas_call x1, Pallas kernels, per_device(): call(functools.partial(prep_body, experts=experts, slots=slots), (pairs,...  1.86 us
  transfers between devices with their start and end apart: 3, of which 1 were waited for; matrix products, arithmetic and copies ran while one was open for 0% of the time, Pallas kernels for 6%

profile of v5, /device:TPU:513, one launch (start us, length us, event | category | flops | bytes accessed | tf_op | source)
XLA Modules:
  0.0 86.5 jit_solution(1564714488716938524)
XLA Ops:
  0.0 1.9 %shard_map.73 = (bf16[192,2,1024]{2,1,0:T(2,128)(2,1)S(1)}, bf16[1024,640]{1,0:T(8,128)(2,1)S(1)}, bf16[1024,640]{1,0:T(8,128)(2,1)S(1)}) custom-call(s32[1]{0:T(128)} %bitcast.lane_ref, bf16[64,1024]{1,0:T(8,128)(2,1)} %tok_hbm.1, f32[1,1024]{1,0:T(1,128)} %bitcast.24, s32[4,64]{1,0:T(4,128)} %bitcast.16, bf16[1024,896]{1,0:T(8,128)(2,1)} %bitcast.19, ...), custom_call_target="tpu_custom_call" | custom-call | flops 50331648 | tf_op jit(solution)/shard_map/pallas_call | solution.py:196
  1.9 38.9 %all_to_all.10 = bf16[64,3,2,1024]{3,2,1,0:T(2,128)(2,1)S(1)} all-to-all(bf16[64,3,2,1024]{3,2,1,0:T(2,128)(2,1)S(1)} %bitcast.15), channel_id=1, replica_groups=mesh['grp'=2,'ep'=64,'tp'=2] {'ep'}, dimensions={0} | all-to-all | bytes 1572864 | tf_op jit(solution)/shard_map/all_to_all | solution.py:208
  40.8 7.1 %collective-permute-start = (bf16[192,2,1024]{2,1,0:T(2,128)(2,1)S(1)}, bf16[192,2,1024]{2,1,0:T(2,128)(2,1)S(1)}, u32[]{:S(2)}, u32[]{:S(2)}) collective-permute-start(bf16[192,2,1024]{2,1,0:T(2,128)(2,1)S(1)} %bitcast.11), channel_id=1, source_target_pairs={{0,1},{1,0},{2,3},{3,2},{4,5},{5,4},{6,7},{7,6},{8,9},{9,8},{10,11... | collective-permute-start | bytes 2359304 | tf_op jit(solution)/shard_map/ppermute | solution.py:190
  47.9 0.0 copy-start
  47.9 0.0 copy-start.1
  47.9 2.9 %shard_map.74 = (bf16[384,1024]{1,0:T(8,128)(2,1)S(1)}, bf16[1024,256]{1,0:T(8,128)(2,1)S(1)}, bf16[1024,256]{1,0:T(8,128)(2,1)S(1)}, bf16[896,1024]{1,0:T(8,128)(2,1)S(1)}) custom-call(bf16[192,2,1024]{2,1,0:T(2,128)(2,1)S(1)} %bitcast.12, bf16[1024,640]{1,0:T(8,128)(2,1)S(1)} %get-tuple-element.15.wg1_ref, ...), custom_call_target="tpu_custom_call" | custom-call | flops 2113929216 | tf_op jit(solution)/shard_map/pallas_call | solution.py:215
  50.8 0.1 collective-permute-start.1
  50.9 0.0 collective-permute-done.x_ref
  50.9 0.0 copy-done
  50.9 0.0 copy-done.1
  50.9 2.7 %shard_map.75 = (bf16[384,1024]{1,0:T(8,128)(2,1)S(1)}, bf16[192,384]{1,0:T(8,128)(2,1)S(1)}) custom-call(s32[1]{0:T(128)} %bitcast.lane_ref, bf16[192,2,1024]{2,1,0:T(2,128)(2,1)S(1)} %collective-permute-done.x_ref, bf16[1024,640]{1,0:T(8,128)(2,1)S(1)} %get-tuple-element.15.wg1_ref, bf16[1024,640]{1,0:T(8,128)(2,1)S(1)} %get-tuple-element.16.wu1_ref, ...), custom_call_target="tpu_custom_call" | custom-call | flops 2113929216 | tf_op jit(solution)/shard_map/pallas_call | solution.py:221
  53.6 0.0 collective-permute-done.1.b_ref
  53.6 0.3 shard_map.76
  53.9 27.9 %all_to_all.11 = bf16[64,3,2,1024]{3,2,1,0:T(2,128)(2,1)S(1)} all-to-all(bf16[64,3,2,1024]{3,2,1,0:T(2,128)(2,1)S(1)} %bitcast.14), channel_id=1, replica_groups=mesh['grp'=2,'ep'=64,'tp'=2] {'ep'}, dimensions={0} | all-to-all | bytes 1572864 | tf_op jit(solution)/shard_map/all_to_all | solution.py:208
  81.8 0.4 shard_map.77
  82.2 2.5 %collective-permute-start.2 = (f32[64,1024]{1,0:T(8,128)S(1)}, f32[64,1024]{1,0:T(8,128)S(1)}, u32[]{:S(2)}, u32[]{:S(2)}) collective-permute-start(f32[64,1024]{1,0:T(8,128)S(1)} %shard_map.77), channel_id=1, source_target_pairs={{0,1},{1,0},{2,3},{3,2},{4,5},{5,4},{6,7},{7,6},{8,9},{9,8},{10,11... | collective-permute-start | bytes 786440 | tf_op jit(solution)/shard_map/ppermute | solution.py:190
  84.7 1.2 %collective-permute-done.2 = f32[64,1024]{1,0:T(8,128)S(1)} collective-permute-done((f32[64,1024]{1,0:T(8,128)S(1)}, f32[64,1024]{1,0:T(8,128)S(1)}, u32[]{:S(2)}, u32[]{:S(2)}) %collective-permute-start.2) | collective-permute-done | bytes 262176 | tf_op jit(solution)/shard_map/ppermute | solution.py:190
  85.8 0.7 add_convert_fusion
Async XLA Ops:
  40.8 10.1 %collective-permute-start = (bf16[192,2,1024]{2,1,0:T(2,128)(2,1)S(1)}, bf16[192,2,1024]{2,1,0:T(2,128)(2,1)S(1)}, u32[]{:S(2)}, u32[]{:S(2)}) collective-permute-start(bf16[192,2,1024]{2,1,0:T(2,128)(2,1)S(1)} %bitcast.11), channel_id=1, source_target_pairs={{0,1},{1,0},{2,3},{3,2},{4,5},{5,4},{6,7},{7,6},{8,9},{9,8},{10,11... | collective-permute-start | bytes 2359304 | tf_op jit(solution)/shard_map/ppermute | solution.py:190
  47.9 3.1 %copy-start = (s32[64,4]{0,1:T(4,128)S(1)}, s32[64,4]{0,1:T(4,128)}, u32[]{:S(2)}) copy-start(s32[64,4]{0,1:T(4,128)} %param.8) | copy-start | bytes 3076
  47.9 3.1 %copy-start.1 = (f32[64,4]{0,1:T(4,128)S(1)}, f32[64,4]{0,1:T(4,128)}, u32[]{:S(2)}) copy-start(f32[64,4]{0,1:T(4,128)} %param.9) | copy-start | bytes 3076
  50.8 2.9 %collective-permute-start.1 = (bf16[384,1024]{1,0:T(8,128)(2,1)S(1)}, bf16[384,1024]{1,0:T(8,128)(2,1)S(1)}, u32[]{:S(2)}, u32[]{:S(2)}) collective-permute-start(bf16[384,1024]{1,0:T(8,128)(2,1)S(1)} %get-tuple-element.22), channel_id=1, source_target_pairs={{0,1},{1,0},{2,3},{3,2},{4,5},{5,4},{6,7},{7,6},{8,9},{9,8},{10,11... | collective-permute-start | bytes 2359304 | tf_op jit(solution)/shard_map/ppermute | solution.py:190
  82.2 3.6 %collective-permute-start.2 = (f32[64,1024]{1,0:T(8,128)S(1)}, f32[64,1024]{1,0:T(8,128)S(1)}, u32[]{:S(2)}, u32[]{:S(2)}) collective-permute-start(f32[64,1024]{1,0:T(8,128)S(1)} %shard_map.77), channel_id=1, source_target_pairs={{0,1},{1,0},{2,3},{3,2},{4,5},{5,4},{6,7},{7,6},{8,9},{9,8},{10,11... | collective-permute-start | bytes 786440 | tf_op jit(solution)/shard_map/ppermute | solution.py:190

commit v6 on v5

--- a/solution.py
+++ b/solution.py
@@ -64,18 +64,9 @@
 
 
 def prep_body(
-    lane_ref, tok_hbm, gain_hbm, rt_hbm, wg_hbm, wu_hbm,
-    out_ref, wg_ref, wu_ref,
-    tok_ref, gain_ref, rt_ref, sems, *, experts, slots,
+    lane_ref, tok_hbm, gain_hbm, rt_hbm, wu_hbm, out_ref, wu_ref, tok_ref, gain_ref, rt_ref, sems, *, experts, slots
 ):
-    early = wg_ref.shape[1]
-    copies = start_all(
-        (
-            (rt_hbm, rt_ref), (tok_hbm, tok_ref), (gain_hbm, gain_ref),
-            (wg_hbm.at[:, :early], wg_ref), (wu_hbm.at[:, :early], wu_ref),
-        ),
-        sems,
-    )
+    copies = start_all(((rt_hbm, rt_ref), (tok_hbm, tok_ref), (gain_hbm, gain_ref), (wu_hbm, wu_ref)), sems)
     for c in copies[:3]:
         c.wait()
     toks = tok_ref.shape[0]
@@ -93,49 +84,29 @@
     slot = (r - div_const(r, slots) * slots).astype(F32)
     one = bf(dot(bf(iota((n, experts), 1) == e_row), place) == slot)
     out_ref[...] = dot(one, normed).astype(BF).reshape(out_ref.shape)
-    for c in copies[3:]:
-        c.wait()
-
-
-def columns(first_ref, second_ref, n):
-    at = n * 128
-    ref, at = (first_ref, at) if at < first_ref.shape[1] else (second_ref, at - first_ref.shape[1])
-    return ref[:, at : at + 128]
-
-
-def hidden_units(rows, wg1_ref, wu1_ref, wg2_ref, wu2_ref, hid_ref, ready):
+    copies[3].wait()
+
+
+def hidden_units(rows, wg_ref, wu_ref, hid_ref):
     for n in range(hid_ref.shape[1] // 128):
-        ready(n)
-        w = jnp.concatenate([columns(wg1_ref, wg2_ref, n), columns(wu1_ref, wu2_ref, n)], axis=1)
-        both = dot(rows, w)
+        cols = slice(n * 128, (n + 1) * 128)
+        both = dot(rows, jnp.concatenate([wg_ref[:, cols], wu_ref[:, cols]], axis=1))
         g, u = both[:, :128], both[:, 128:]
-        hid_ref[:, n * 128 : (n + 1) * 128] = ((0.5 * g) * (1.0 + jnp.tanh(0.5 * g)) * u).astype(BF)
-
-
-def own_body(
-    x_ref, wg1_ref, wu1_ref, wg_hbm, wu_hbm, wd_hbm, out_ref, wg2_ref, wu2_ref, wd_ref, hid_ref, sems
-):
-    early = wg1_ref.shape[1]
-    copies = start_all(
-        ((wg_hbm.at[:, early:], wg2_ref), (wu_hbm.at[:, early:], wu2_ref), (wd_hbm, wd_ref)), sems
-    )
-
-    def ready(n):
-        if n * 128 == early:
-            copies[0].wait()
-            copies[1].wait()
-
-    hidden_units(flat(x_ref), wg1_ref, wu1_ref, wg2_ref, wu2_ref, hid_ref, ready)
-    copies[2].wait()
+        hid_ref[:, cols] = ((0.5 * g) * (1.0 + jnp.tanh(0.5 * g)) * u).astype(BF)
+
+
+def own_body(x_ref, wg_ref, wu_ref, wd_hbm, out_ref, wd_ref, hid_ref, sems):
+    (copy,) = start_all(((wd_hbm, wd_ref),), sems)
+    hidden_units(flat(x_ref), wg_ref, wu_ref, hid_ref)
+    copy.wait()
     out_ref[...] = dot(hid_ref[...], wd_ref[...]).astype(BF)
 
 
 def other_body(
-    lane_ref, x_ref, wg1_ref, wu1_ref, wg2_ref, wu2_ref, wd_ref, rt_ref, gt_ref,
-    out_ref, mix_ref, hid_ref, *, slots, experts,
+    lane_ref, x_ref, wg_ref, wu_ref, wd_ref, rt_ref, gt_ref, out_ref, mix_ref, hid_ref, *, slots, experts
 ):
     table(lane_ref, rt_ref[...], gt_ref[...], mix_ref, slots, experts)
-    hidden_units(flat(x_ref), wg1_ref, wu1_ref, wg2_ref, wu2_ref, hid_ref, lambda n: None)
+    hidden_units(flat(x_ref), wg_ref, wu_ref, hid_ref)
     out_ref[...] = dot(hid_ref[...], wd_ref[...]).astype(BF)
 
 
@@ -185,26 +156,24 @@
     items = experts * slots
     pairs = pltpu.VMEM((items // 2, 2, width), BF)
     tall = pltpu.VMEM((items, width), BF)
-    early = ff // 128 * 5 // 7 * 128
-    late = ff - early
     swap = lambda v: lax.ppermute(v, "tp", [(0, 1), (1, 0)])
     lanes = lax.axis_index("tp").astype(jnp.int32).reshape(1)
     in_hbm = lambda *vs: [pltpu.with_memory_space_constraint(v, pltpu.HBM) for v in vs]
     wg, wu, wd = w_gate[0], w_up[0], w_down[0]
     rt = routes.T
 
-    outgoing, wg1, wu1 = call(
+    outgoing, wu = call(
         functools.partial(prep_body, experts=experts, slots=slots),
-        (pairs, pltpu.VMEM((width, early), BF), pltpu.VMEM((width, early), BF)),
-        [SMEM] + [HBM] * 5,
+        (pairs, pltpu.VMEM(wu.shape, BF)),
+        [SMEM] + [HBM] * 4,
         [
             pltpu.VMEM((toks, width), BF),
             pltpu.VMEM((1, width), F32),
             pltpu.VMEM((top, toks), jnp.int32),
-            pltpu.SemaphoreType.DMA((5,)),
+            pltpu.SemaphoreType.DMA((4,)),
         ],
         flops=2 * items * toks * width,
-    )(lanes, *in_hbm(tokens, norm_gain.reshape(1, width), rt, wg, wu))
+    )(lanes, *in_hbm(tokens, norm_gain.reshape(1, width), rt, wu))
     exchange = lambda v: lax.all_to_all(
         v.reshape(experts, slots // 2, 2, width), "ep", split_axis=0, concat_axis=0, tiled=True
     ).reshape(v.shape)
@@ -212,16 +181,15 @@
     other = swap(mine)
     work = 2 * items * width * 3 * ff
     held = pltpu.VMEM((items, ff), BF)
-    sent, wg2, wu2, wd1 = call(
-        own_body,
-        (tall, pltpu.VMEM((width, late), BF), pltpu.VMEM((width, late), BF), pltpu.VMEM(wd.shape, BF)),
-        [VMEM] * 3 + [HBM] * 3, [held, pltpu.SemaphoreType.DMA((3,))], flops=work,
-    )(mine, wg1, wu1, *in_hbm(wg, wu, wd))
+    sent, wd = call(
+        own_body, (tall, pltpu.VMEM(wd.shape, BF)), [VMEM] * 3 + [HBM],
+        [held, pltpu.SemaphoreType.DMA((1,))], flops=work,
+    )(mine, wg, wu, *in_hbm(wd))
     got = swap(sent)
     kept, mix = call(
         functools.partial(other_body, slots=slots, experts=experts),
-        (tall, pltpu.VMEM((3 * toks, items), BF)), [SMEM] + [VMEM] * 8, [held], flops=work,
-    )(lanes, other, wg1, wu1, wg2, wu2, wd1, rt, gates.T)
+        (tall, pltpu.VMEM((3 * toks, items), BF)), [SMEM] + [VMEM] * 6, [held], flops=work,
+    )(lanes, other, wg, wu, wd, rt, gates.T)
     back = exchange(call(add_body, pairs, [VMEM] * 2, flops=items * width)(kept, got))
     part = call(
         last_body, pltpu.VMEM((toks, width), F32), [VMEM] * 2, flops=2 * 3 * toks * items * width

time: 86.8 us -> 86.5 us (level)
  no operation moved by 1% of the time
where the time goes in v6:
time: 86.5 us; the launch traced here: 86.3 us
  blocking collectives  66.8 us (77%)
  starting transfers between devices  9.71 us (11%)
  Pallas kernels  7.84 us (9%)
  waiting for transfers between devices  1.17 us (1%)
    all_to_all x2, blocking collectives, per_device(): lax.all_to_all(v.reshape(experts, slots // 2, 2, width), 'ep', split_axis...  66.8 us
    ppermute x3, starting transfers between devices, per_device(): swap = lambda v: lax.ppermute(v, 'tp', [(0, 1), (1, 0)])  9.71 us
    pallas_call x1, Pallas kernels, per_device(): call(functools.partial(other_body, slots=slots, experts=experts), (tall,...  2.75 us
    pallas_call x1, Pallas kernels, per_device(): call(own_body, (tall, pltpu.VMEM(wd.shape, BF)), [VMEM] * 3 + [HBM], [hel...  2.67 us
    pallas_call x1, Pallas kernels, per_device(): call(functools.partial(prep_body, experts=experts, slots=slots), (pairs,...  1.76 us
  transfers between devices with their start and end apart: 3, of which 1 were waited for; matrix products, arithmetic and copies ran while one was open for 0% of the time, Pallas kernels for 6%

profile of v6, /device:TPU:513, one launch (start us, length us, event | category | flops | bytes accessed | tf_op | source)
XLA Modules:
  0.0 86.3 jit_solution(17107474642430964997)
XLA Ops:
  0.0 0.0 copy-start.1
  0.0 1.8 %shard_map.73 = (bf16[192,2,1024]{2,1,0:T(2,128)(2,1)S(1)}, bf16[1024,896]{1,0:T(8,128)(2,1)S(1)}) custom-call(s32[1]{0:T(128)} %bitcast.lane_ref, bf16[64,1024]{1,0:T(8,128)(2,1)} %tok_hbm.1, f32[1,1024]{1,0:T(1,128)} %bitcast.22, s32[4,64]{1,0:T(4,128)} %bitcast.16, bf16[1024,896]{1,0:T(8,128)(2,1)} %bitcast.21), custom_call_target="tpu_custom_call" | custom-call | flops 50331648 | tf_op jit(solution)/shard_map/pallas_call | solution.py:165
  1.8 38.9 %all_to_all.10 = bf16[64,3,2,1024]{3,2,1,0:T(2,128)(2,1)S(1)} all-to-all(bf16[64,3,2,1024]{3,2,1,0:T(2,128)(2,1)S(1)} %bitcast.15), channel_id=1, replica_groups=mesh['grp'=2,'ep'=64,'tp'=2] {'ep'}, dimensions={0} | all-to-all | bytes 1572864 | tf_op jit(solution)/shard_map/all_to_all | solution.py:177
  40.7 7.1 %collective-permute-start = (bf16[192,2,1024]{2,1,0:T(2,128)(2,1)S(1)}, bf16[192,2,1024]{2,1,0:T(2,128)(2,1)S(1)}, u32[]{:S(2)}, u32[]{:S(2)}) collective-permute-start(bf16[192,2,1024]{2,1,0:T(2,128)(2,1)S(1)} %bitcast.13), channel_id=1, source_target_pairs={{0,1},{1,0},{2,3},{3,2},{4,5},{5,4},{6,7},{7,6},{8,9},{9,8},{10,11... | collective-permute-start | bytes 2359304 | tf_op jit(solution)/shard_map/ppermute | solution.py:159
  47.8 0.0 copy-done.1
  47.8 0.0 copy-start
  47.8 0.0 copy-start.2
  47.8 2.7 %shard_map.74 = (bf16[384,1024]{1,0:T(8,128)(2,1)S(1)}, bf16[896,1024]{1,0:T(8,128)(2,1)S(1)}) custom-call(bf16[192,2,1024]{2,1,0:T(2,128)(2,1)S(1)} %bitcast.14, bf16[1024,896]{1,0:T(8,128)(2,1)S(1)} %bitcast.18, bf16[1024,896]{1,0:T(8,128)(2,1)S(1)} %get-tuple-element.12.wu_ref, bf16[896,1024]{1,0:T(8,128)(2,1)} %bitcast.23), custom_call_target="tpu_custom_call" | custom-call | flops 2113929216 | tf_op jit(solution)/shard_map/pallas_call | solution.py:184
  50.4 0.1 collective-permute-start.1
  50.6 0.0 collective-permute-done.x_ref
  50.6 0.0 copy-done
  50.6 0.0 copy-done.2
  50.6 2.8 %shard_map.75 = (bf16[384,1024]{1,0:T(8,128)(2,1)S(1)}, bf16[192,384]{1,0:T(8,128)(2,1)S(1)}) custom-call(s32[1]{0:T(128)} %bitcast.lane_ref, bf16[192,2,1024]{2,1,0:T(2,128)(2,1)S(1)} %collective-permute-done.x_ref, bf16[1024,896]{1,0:T(8,128)(2,1)S(1)} %bitcast.19, bf16[1024,896]{1,0:T(8,128)(2,1)S(1)} %get-tuple-element.12.wu_ref, ...), custom_call_target="tpu_custom_call" | custom-call | flops 2113929216 | tf_op jit(solution)/shard_map/pallas_call | solution.py:189
  53.4 0.0 collective-permute-done.1.b_ref
  53.4 0.3 shard_map.76
  53.7 27.9 %all_to_all.11 = bf16[64,3,2,1024]{3,2,1,0:T(2,128)(2,1)S(1)} all-to-all(bf16[64,3,2,1024]{3,2,1,0:T(2,128)(2,1)S(1)} %bitcast.12), channel_id=1, replica_groups=mesh['grp'=2,'ep'=64,'tp'=2] {'ep'}, dimensions={0} | all-to-all | bytes 1572864 | tf_op jit(solution)/shard_map/all_to_all | solution.py:177
  81.6 0.4 shard_map.77
  81.9 2.5 %collective-permute-start.2 = (f32[64,1024]{1,0:T(8,128)S(1)}, f32[64,1024]{1,0:T(8,128)S(1)}, u32[]{:S(2)}, u32[]{:S(2)}) collective-permute-start(f32[64,1024]{1,0:T(8,128)S(1)} %shard_map.77), channel_id=1, source_target_pairs={{0,1},{1,0},{2,3},{3,2},{4,5},{5,4},{6,7},{7,6},{8,9},{9,8},{10,11... | collective-permute-start | bytes 786440 | tf_op jit(solution)/shard_map/ppermute | solution.py:159
  84.4 1.2 %collective-permute-done.2 = f32[64,1024]{1,0:T(8,128)S(1)} collective-permute-done((f32[64,1024]{1,0:T(8,128)S(1)}, f32[64,1024]{1,0:T(8,128)S(1)}, u32[]{:S(2)}, u32[]{:S(2)}) %collective-permute-start.2) | collective-permute-done | bytes 262176 | tf_op jit(solution)/shard_map/ppermute | solution.py:159
  85.6 0.7 add_convert_fusion
Async XLA Ops:
  0.0 47.8 %copy-start.1 = (bf16[1,1024,896]{2,1,0:T(8,128)(2,1)S(1)}, bf16[1,1024,896]{2,1,0:T(8,128)(2,1)}, u32[]{:S(2)}) copy-start(bf16[1,1024,896]{2,1,0:T(8,128)(2,1)} %param.11) | copy-start | bytes 5505028
  40.7 9.9 %collective-permute-start = (bf16[192,2,1024]{2,1,0:T(2,128)(2,1)S(1)}, bf16[192,2,1024]{2,1,0:T(2,128)(2,1)S(1)}, u32[]{:S(2)}, u32[]{:S(2)}) collective-permute-start(bf16[192,2,1024]{2,1,0:T(2,128)(2,1)S(1)} %bitcast.13), channel_id=1, source_target_pairs={{0,1},{1,0},{2,3},{3,2},{4,5},{5,4},{6,7},{7,6},{8,9},{9,8},{10,11... | collective-permute-start | bytes 2359304 | tf_op jit(solution)/shard_map/ppermute | solution.py:159
  47.8 2.8 %copy-start = (s32[64,4]{0,1:T(4,128)S(1)}, s32[64,4]{0,1:T(4,128)}, u32[]{:S(2)}) copy-start(s32[64,4]{0,1:T(4,128)} %param.8) | copy-start | bytes 3076
  47.8 2.9 %copy-start.2 = (f32[64,4]{0,1:T(4,128)S(1)}, f32[64,4]{0,1:T(4,128)}, u32[]{:S(2)}) copy-start(f32[64,4]{0,1:T(4,128)} %param.9) | copy-start | bytes 3076
  50.4 2.9 %collective-permute-start.1 = (bf16[384,1024]{1,0:T(8,128)(2,1)S(1)}, bf16[384,1024]{1,0:T(8,128)(2,1)S(1)}, u32[]{:S(2)}, u32[]{:S(2)}) collective-permute-start(bf16[384,1024]{1,0:T(8,128)(2,1)S(1)} %get-tuple-element.16), channel_id=1, source_target_pairs={{0,1},{1,0},{2,3},{3,2},{4,5},{5,4},{6,7},{7,6},{8,9},{9,8},{10,11... | collective-permute-start | bytes 2359304 | tf_op jit(solution)/shard_map/ppermute | solution.py:159
  81.9 3.6 %collective-permute-start.2 = (f32[64,1024]{1,0:T(8,128)S(1)}, f32[64,1024]{1,0:T(8,128)S(1)}, u32[]{:S(2)}, u32[]{:S(2)}) collective-permute-start(f32[64,1024]{1,0:T(8,128)S(1)} %shard_map.77), channel_id=1, source_target_pairs={{0,1},{1,0},{2,3},{3,2},{4,5},{5,4},{6,7},{7,6},{8,9},{9,8},{10,11... | collective-permute-start | bytes 786440 | tf_op jit(solution)/shard_map/ppermute | solution.py:159

commit v7 on v6

--- a/solution.py
+++ b/solution.py
@@ -1,4 +1,5 @@
 import functools
+import math
 
 import jax
 import jax.numpy as jnp
@@ -63,8 +64,13 @@
     return jnp.where((chosen > 0) & (rel >= 0) & (rel < slots), rel, -1.0)
 
 
+def expert_at(place, core, side):
+    row = place >> (side.bit_length() - 1)
+    return jnp.where(core == 0, place, (place - row * side) * side + row)
+
+
 def prep_body(
-    lane_ref, tok_hbm, gain_hbm, rt_hbm, wu_hbm, out_ref, wu_ref, tok_ref, gain_ref, rt_ref, sems, *, experts, slots
+    lane_ref, tok_hbm, gain_hbm, rt_hbm, wu_hbm, out_ref, wu_ref, tok_ref, gain_ref, rt_ref, sems, *, experts, slots, side
 ):
     copies = start_all(((rt_hbm, rt_ref), (tok_hbm, tok_ref), (gain_hbm, gain_ref), (wu_hbm, wu_ref)), sems)
     for c in copies[:3]:
@@ -79,7 +85,7 @@
         chosen = chosen + (e_of == rt_ref[k : k + 1, :]).astype(F32)
     place = slot_of(chosen, lane_ref[0], slots).astype(BF)
     n = slots * experts
-    e_row = div_const(iota((n, experts), 0), slots)
+    e_row = expert_at(div_const(iota((n, experts), 0), slots), lane_ref[0], side)
     r = iota((n, toks), 0)
     slot = (r - div_const(r, slots) * slots).astype(F32)
     one = bf(dot(bf(iota((n, experts), 1) == e_row), place) == slot)
@@ -103,14 +109,14 @@
 
 
 def other_body(
-    lane_ref, x_ref, wg_ref, wu_ref, wd_ref, rt_ref, gt_ref, out_ref, mix_ref, hid_ref, *, slots, experts
+    lane_ref, x_ref, wg_ref, wu_ref, wd_ref, rt_ref, gt_ref, out_ref, mix_ref, hid_ref, *, slots, experts, side
 ):
-    table(lane_ref, rt_ref[...], gt_ref[...], mix_ref, slots, experts)
+    table(lane_ref, rt_ref[...], gt_ref[...], mix_ref, slots, experts, side)
     hidden_units(flat(x_ref), wg_ref, wu_ref, hid_ref)
     out_ref[...] = dot(hid_ref[...], wd_ref[...]).astype(BF)
 
 
-def table(lane_ref, rt, gt, mix_ref, slots, experts):
+def table(lane_ref, rt, gt, mix_ref, slots, experts, side):
     top, toks = rt.shape
     e_of = iota((experts, toks), 0)
     chosen = jnp.zeros((experts, toks), F32)
@@ -129,7 +135,7 @@
     r = iota((1, n), 1)
     e_r = div_const(r, slots)
     slot = (r - e_r * slots).astype(F32)
-    rep = bf(iota((experts, n), 0) == e_r)
+    rep = bf(iota((experts, n), 0) == expert_at(e_r, 1 - lane_ref[0], side))
     here = dot(place, rep) == slot
     for i, piece in enumerate((g1, g2, g3)):
         mix_ref[i * toks : (i + 1) * toks, :] = jnp.where(here, dot(piece, rep), 0.0).astype(BF)
@@ -153,6 +159,7 @@
     cap = max(2, min(toks, 3 * toks * top // experts))
     slots = -(-cap // 4) * 2
     ff = w_gate.shape[2]
+    side = math.isqrt(experts)
     items = experts * slots
     pairs = pltpu.VMEM((items // 2, 2, width), BF)
     tall = pltpu.VMEM((items, width), BF)
@@ -163,7 +170,7 @@
     rt = routes.T
 
     outgoing, wu = call(
-        functools.partial(prep_body, experts=experts, slots=slots),
+        functools.partial(prep_body, experts=experts, slots=slots, side=side),
         (pairs, pltpu.VMEM(wu.shape, BF)),
         [SMEM] + [HBM] * 4,
         [
@@ -174,10 +181,16 @@
         ],
         flops=2 * items * toks * width,
     )(lanes, *in_hbm(tokens, norm_gain.reshape(1, width), rt, wu))
-    exchange = lambda v: lax.all_to_all(
-        v.reshape(experts, slots // 2, 2, width), "ep", split_axis=0, concat_axis=0, tiled=True
-    ).reshape(v.shape)
-    mine = exchange(outgoing)
+    by_row = list(range(experts))
+    by_column = [(p % side) * side + p // side for p in by_row]
+
+    def exchange(v, first, second):
+        return lax.all_to_all(
+            v.reshape(experts, slots // 2, 2, width), ("ep", "tp"), split_axis=0, concat_axis=0, tiled=True,
+            axis_index_groups=[[2 * e for e in first], [2 * e + 1 for e in second]],
+        ).reshape(v.shape)
+
+    mine = exchange(outgoing, by_row, by_column)
     other = swap(mine)
     work = 2 * items * width * 3 * ff
     held = pltpu.VMEM((items, ff), BF)
@@ -187,10 +200,10 @@
     )(mine, wg, wu, *in_hbm(wd))
     got = swap(sent)
     kept, mix = call(
-        functools.partial(other_body, slots=slots, experts=experts),
+        functools.partial(other_body, slots=slots, experts=experts, side=side),
         (tall, pltpu.VMEM((3 * toks, items), BF)), [SMEM] + [VMEM] * 6, [held], flops=work,
     )(lanes, other, wg, wu, wd, rt, gates.T)
-    back = exchange(call(add_body, pairs, [VMEM] * 2, flops=items * width)(kept, got))
+    back = exchange(call(add_body, pairs, [VMEM] * 2, flops=items * width)(kept, got), by_column, by_row)
     part = call(
         last_body, pltpu.VMEM((toks, width), F32), [VMEM] * 2, flops=2 * 3 * toks * items * width
     )(mix, back)

time: 86.5 us -> 86.7 us (level)
  no operation moved by 1% of the time
where the time goes in v7:
time: 86.7 us; the launch traced here: 86.5 us
  blocking collectives  66.7 us (77%)
  starting transfers between devices  10 us (12%)
  Pallas kernels  7.83 us (9%)
  waiting for transfers between devices  1.17 us (1%)
    all_to_all x2, blocking collectives, exchange(): lax.all_to_all(v.reshape(experts, slots // 2, 2, width), ('ep', 'tp'), sp...  66.7 us
    ppermute x3, starting transfers between devices, per_device(): swap = lambda v: lax.ppermute(v, 'tp', [(0, 1), (1, 0)])  10 us
    pallas_call x1, Pallas kernels, per_device(): call(functools.partial(other_body, slots=slots, experts=experts, side=sid...  2.75 us
    pallas_call x1, Pallas kernels, per_device(): call(own_body, (tall, pltpu.VMEM(wd.shape, BF)), [VMEM] * 3 + [HBM], [hel...  2.66 us
    pallas_call x1, Pallas kernels, per_device(): call(functools.partial(prep_body, experts=experts, slots=slots, side=side...  1.76 us
  transfers between devices with their start and end apart: 3, of which 1 were waited for; matrix products, arithmetic and copies ran while one was open for 0% of the time, Pallas kernels for 6%

profile of v7, /device:TPU:513, one launch (start us, length us, event | category | flops | bytes accessed | tf_op | source)
XLA Modules:
  0.0 86.5 jit_solution(10599697120621621191)
XLA Ops:
  0.0 0.0 copy-start.1
  0.0 1.8 %shard_map.73 = (bf16[192,2,1024]{2,1,0:T(2,128)(2,1)S(1)}, bf16[1024,896]{1,0:T(8,128)(2,1)S(1)}) custom-call(s32[1]{0:T(128)} %bitcast.lane_ref, bf16[64,1024]{1,0:T(8,128)(2,1)} %tok_hbm.1, f32[1,1024]{1,0:T(1,128)} %bitcast.22, s32[4,64]{1,0:T(4,128)} %bitcast.16, bf16[1024,896]{1,0:T(8,128)(2,1)} %bitcast.21), custom_call_target="tpu_custom_call" | custom-call | flops 50331648 | tf_op jit(solution)/shard_map/pallas_call | solution.py:172
  1.8 38.7 %all_to_all.10 = bf16[64,3,2,1024]{3,2,1,0:T(2,128)(2,1)S(1)} all-to-all(bf16[64,3,2,1024]{3,2,1,0:T(2,128)(2,1)S(1)} %bitcast.15), channel_id=1, replica_groups={{0,2,4,6,8,10,12,14,16,18,20,22,24,26,28,30,32,34,36,38,40,42,44,46,48,..., dimensions={0} | all-to-all | bytes 1572864 | tf_op jit(solution)/shard_map/all_to_all | solution.py:188
  40.5 6.9 %collective-permute-start = (bf16[192,2,1024]{2,1,0:T(2,128)(2,1)S(1)}, bf16[192,2,1024]{2,1,0:T(2,128)(2,1)S(1)}, u32[]{:S(2)}, u32[]{:S(2)}) collective-permute-start(bf16[192,2,1024]{2,1,0:T(2,128)(2,1)S(1)} %bitcast.13), channel_id=1, source_target_pairs={{0,1},{1,0},{2,3},{3,2},{4,5},{5,4},{6,7},{7,6},{8,9},{9,8},{10,11... | collective-permute-start | bytes 2359304 | tf_op jit(solution)/shard_map/ppermute | solution.py:166
  47.4 0.0 copy-done.1
  47.4 0.0 copy-start
  47.4 0.0 copy-start.2
  47.4 2.7 %shard_map.74 = (bf16[384,1024]{1,0:T(8,128)(2,1)S(1)}, bf16[896,1024]{1,0:T(8,128)(2,1)S(1)}) custom-call(bf16[192,2,1024]{2,1,0:T(2,128)(2,1)S(1)} %bitcast.14, bf16[1024,896]{1,0:T(8,128)(2,1)S(1)} %bitcast.18, bf16[1024,896]{1,0:T(8,128)(2,1)S(1)} %get-tuple-element.12.wu_ref, bf16[896,1024]{1,0:T(8,128)(2,1)} %bitcast.23), custom_call_target="tpu_custom_call" | custom-call | flops 2113929216 | tf_op jit(solution)/shard_map/pallas_call | solution.py:197
  50.1 0.1 collective-permute-start.1
  50.3 0.0 collective-permute-done.x_ref
  50.3 0.0 copy-done
  50.3 0.0 copy-done.2
  50.3 2.7 %shard_map.75 = (bf16[384,1024]{1,0:T(8,128)(2,1)S(1)}, bf16[192,384]{1,0:T(8,128)(2,1)S(1)}) custom-call(s32[1]{0:T(128)} %bitcast.lane_ref, bf16[192,2,1024]{2,1,0:T(2,128)(2,1)S(1)} %collective-permute-done.x_ref, bf16[1024,896]{1,0:T(8,128)(2,1)S(1)} %bitcast.19, bf16[1024,896]{1,0:T(8,128)(2,1)S(1)} %get-tuple-element.12.wu_ref, ...), custom_call_target="tpu_custom_call" | custom-call | flops 2113929216 | tf_op jit(solution)/shard_map/pallas_call | solution.py:202
  53.0 0.0 collective-permute-done.1.b_ref
  53.0 0.3 shard_map.76
  53.3 28.0 %all_to_all.11 = bf16[64,3,2,1024]{3,2,1,0:T(2,128)(2,1)S(1)} all-to-all(bf16[64,3,2,1024]{3,2,1,0:T(2,128)(2,1)S(1)} %bitcast.12), channel_id=1, replica_groups={{0,16,32,48,64,80,96,112,2,18,34,50,66,82,98,114,4,20,36,52,68,84,100,1..., dimensions={0} | all-to-all | bytes 1572864 | tf_op jit(solution)/shard_map/all_to_all | solution.py:188
  81.3 0.4 shard_map.77
  81.7 2.9 %collective-permute-start.2 = (f32[64,1024]{1,0:T(8,128)S(1)}, f32[64,1024]{1,0:T(8,128)S(1)}, u32[]{:S(2)}, u32[]{:S(2)}) collective-permute-start(f32[64,1024]{1,0:T(8,128)S(1)} %shard_map.77), channel_id=1, source_target_pairs={{0,1},{1,0},{2,3},{3,2},{4,5},{5,4},{6,7},{7,6},{8,9},{9,8},{10,11... | collective-permute-start | bytes 786440 | tf_op jit(solution)/shard_map/ppermute | solution.py:166
  84.6 1.2 %collective-permute-done.2 = f32[64,1024]{1,0:T(8,128)S(1)} collective-permute-done((f32[64,1024]{1,0:T(8,128)S(1)}, f32[64,1024]{1,0:T(8,128)S(1)}, u32[]{:S(2)}, u32[]{:S(2)}) %collective-permute-start.2) | collective-permute-done | bytes 262176 | tf_op jit(solution)/shard_map/ppermute | solution.py:166
  85.8 0.7 add_convert_fusion
Async XLA Ops:
  0.0 47.4 %copy-start.1 = (bf16[1,1024,896]{2,1,0:T(8,128)(2,1)S(1)}, bf16[1,1024,896]{2,1,0:T(8,128)(2,1)}, u32[]{:S(2)}) copy-start(bf16[1,1024,896]{2,1,0:T(8,128)(2,1)} %param.11) | copy-start | bytes 5505028
  40.5 9.8 %collective-permute-start = (bf16[192,2,1024]{2,1,0:T(2,128)(2,1)S(1)}, bf16[192,2,1024]{2,1,0:T(2,128)(2,1)S(1)}, u32[]{:S(2)}, u32[]{:S(2)}) collective-permute-start(bf16[192,2,1024]{2,1,0:T(2,128)(2,1)S(1)} %bitcast.13), channel_id=1, source_target_pairs={{0,1},{1,0},{2,3},{3,2},{4,5},{5,4},{6,7},{7,6},{8,9},{9,8},{10,11... | collective-permute-start | bytes 2359304 | tf_op jit(solution)/shard_map/ppermute | solution.py:166
  47.4 2.8 %copy-start = (s32[64,4]{0,1:T(4,128)S(1)}, s32[64,4]{0,1:T(4,128)}, u32[]{:S(2)}) copy-start(s32[64,4]{0,1:T(4,128)} %param.8) | copy-start | bytes 3076
  47.4 2.8 %copy-start.2 = (f32[64,4]{0,1:T(4,128)S(1)}, f32[64,4]{0,1:T(4,128)}, u32[]{:S(2)}) copy-start(f32[64,4]{0,1:T(4,128)} %param.9) | copy-start | bytes 3076
  50.1 2.9 %collective-permute-start.1 = (bf16[384,1024]{1,0:T(8,128)(2,1)S(1)}, bf16[384,1024]{1,0:T(8,128)(2,1)S(1)}, u32[]{:S(2)}, u32[]{:S(2)}) collective-permute-start(bf16[384,1024]{1,0:T(8,128)(2,1)S(1)} %get-tuple-element.16), channel_id=1, source_target_pairs={{0,1},{1,0},{2,3},{3,2},{4,5},{5,4},{6,7},{7,6},{8,9},{9,8},{10,11... | collective-permute-start | bytes 2359304 | tf_op jit(solution)/shard_map/ppermute | solution.py:166
  81.7 4.1 %collective-permute-start.2 = (f32[64,1024]{1,0:T(8,128)S(1)}, f32[64,1024]{1,0:T(8,128)S(1)}, u32[]{:S(2)}, u32[]{:S(2)}) collective-permute-start(f32[64,1024]{1,0:T(8,128)S(1)} %shard_map.77), channel_id=1, source_target_pairs={{0,1},{1,0},{2,3},{3,2},{4,5},{5,4},{6,7},{7,6},{8,9},{9,8},{10,11... | collective-permute-start | bytes 786440 | tf_op jit(solution)/shard_map/ppermute | solution.py:166

commit v8 on v6

--- a/solution.py
+++ b/solution.py
@@ -64,10 +64,14 @@
 
 
 def prep_body(
-    lane_ref, tok_hbm, gain_hbm, rt_hbm, wu_hbm, out_ref, wu_ref, tok_ref, gain_ref, rt_ref, sems, *, experts, slots
+    lane_ref, tok_hbm, gain_hbm, rt_hbm, gt_hbm, wu_hbm,
+    out_ref, wu_ref, mix_ref,
+    tok_ref, gain_ref, rt_ref, gt_ref, sems, *, experts, slots,
 ):
-    copies = start_all(((rt_hbm, rt_ref), (tok_hbm, tok_ref), (gain_hbm, gain_ref), (wu_hbm, wu_ref)), sems)
-    for c in copies[:3]:
+    copies = start_all(
+        ((rt_hbm, rt_ref), (tok_hbm, tok_ref), (gain_hbm, gain_ref), (gt_hbm, gt_ref), (wu_hbm, wu_ref)), sems
+    )
+    for c in copies[:4]:
         c.wait()
     toks = tok_ref.shape[0]
     xf = tok_ref[...].astype(F32)
@@ -84,7 +88,8 @@
     slot = (r - div_const(r, slots) * slots).astype(F32)
     one = bf(dot(bf(iota((n, experts), 1) == e_row), place) == slot)
     out_ref[...] = dot(one, normed).astype(BF).reshape(out_ref.shape)
-    copies[3].wait()
+    table(lane_ref, rt_ref[...], gt_ref[...], mix_ref, slots, experts)
+    copies[4].wait()
 
 
 def hidden_units(rows, wg_ref, wu_ref, hid_ref):
@@ -102,10 +107,7 @@
     out_ref[...] = dot(hid_ref[...], wd_ref[...]).astype(BF)
 
 
-def other_body(
-    lane_ref, x_ref, wg_ref, wu_ref, wd_ref, rt_ref, gt_ref, out_ref, mix_ref, hid_ref, *, slots, experts
-):
-    table(lane_ref, rt_ref[...], gt_ref[...], mix_ref, slots, experts)
+def other_body(x_ref, wg_ref, wu_ref, wd_ref, out_ref, hid_ref):
     hidden_units(flat(x_ref), wg_ref, wu_ref, hid_ref)
     out_ref[...] = dot(hid_ref[...], wd_ref[...]).astype(BF)
 
@@ -160,20 +162,20 @@
     lanes = lax.axis_index("tp").astype(jnp.int32).reshape(1)
     in_hbm = lambda *vs: [pltpu.with_memory_space_constraint(v, pltpu.HBM) for v in vs]
     wg, wu, wd = w_gate[0], w_up[0], w_down[0]
-    rt = routes.T
-
-    outgoing, wu = call(
+
+    outgoing, wu, mix = call(
         functools.partial(prep_body, experts=experts, slots=slots),
-        (pairs, pltpu.VMEM(wu.shape, BF)),
-        [SMEM] + [HBM] * 4,
+        (pairs, pltpu.VMEM(wu.shape, BF), pltpu.VMEM((3 * toks, items), BF)),
+        [SMEM] + [HBM] * 5,
         [
             pltpu.VMEM((toks, width), BF),
             pltpu.VMEM((1, width), F32),
             pltpu.VMEM((top, toks), jnp.int32),
-            pltpu.SemaphoreType.DMA((4,)),
+            pltpu.VMEM((top, toks), F32),
+            pltpu.SemaphoreType.DMA((5,)),
         ],
         flops=2 * items * toks * width,
-    )(lanes, *in_hbm(tokens, norm_gain.reshape(1, width), rt, wu))
+    )(lanes, *in_hbm(tokens, norm_gain.reshape(1, width), routes.T, gates.T, wu))
     exchange = lambda v: lax.all_to_all(
         v.reshape(experts, slots // 2, 2, width), "ep", split_axis=0, concat_axis=0, tiled=True
     ).reshape(v.shape)
@@ -186,10 +188,7 @@
         [held, pltpu.SemaphoreType.DMA((1,))], flops=work,
     )(mine, wg, wu, *in_hbm(wd))
     got = swap(sent)
-    kept, mix = call(
-        functools.partial(other_body, slots=slots, experts=experts),
-        (tall, pltpu.VMEM((3 * toks, items), BF)), [SMEM] + [VMEM] * 6, [held], flops=work,
-    )(lanes, other, wg, wu, wd, rt, gates.T)
+    kept = call(other_body, tall, [VMEM] * 4, [held], flops=work)(other, wg, wu, wd)
     back = exchange(call(add_body, pairs, [VMEM] * 2, flops=items * width)(kept, got))
     part = call(
         last_body, pltpu.VMEM((toks, width), F32), [VMEM] * 2, flops=2 * 3 * toks * items * width

time: 86.5 us -> 86.3 us (level)
  no operation moved by 1% of the time
where the time goes in v8:
time: 86.3 us; the launch traced here: 86.1 us
  blocking collectives  66.8 us (77%)
  starting transfers between devices  9.72 us (11%)
  Pallas kernels  7.68 us (9%)
  waiting for transfers between devices  1.17 us (1%)
    all_to_all x2, blocking collectives, per_device(): lax.all_to_all(v.reshape(experts, slots // 2, 2, width), 'ep', split_axis...  66.8 us
    ppermute x3, starting transfers between devices, per_device(): swap = lambda v: lax.ppermute(v, 'tp', [(0, 1), (1, 0)])  9.72 us
    pallas_call x1, Pallas kernels, per_device(): call(own_body, (tall, pltpu.VMEM(wd.shape, BF)), [VMEM] * 3 + [HBM], [hel...  2.64 us
    pallas_call x1, Pallas kernels, per_device(): call(other_body, tall, [VMEM] * 4, [held], flops=work)(other, wg, wu, wd)  2.41 us
    pallas_call x1, Pallas kernels, per_device(): call(functools.partial(prep_body, experts=experts, slots=slots), (pairs,...  1.98 us
  transfers between devices with their start and end apart: 3, of which 1 were waited for; matrix products, arithmetic and copies ran while one was open for 0% of the time, Pallas kernels for 6%

profile of v8, /device:TPU:513, one launch (start us, length us, event | category | flops | bytes accessed | tf_op | source)
XLA Modules:
  0.0 86.1 jit_solution(41485467113506159)
XLA Ops:
  0.0 0.0 copy-start
  0.0 2.0 %shard_map.73 = (bf16[192,2,1024]{2,1,0:T(2,128)(2,1)S(1)}, bf16[1024,896]{1,0:T(8,128)(2,1)S(1)}, bf16[192,384]{1,0:T(8,128)(2,1)S(1)}) custom-call(s32[1]{0:T(128)} %bitcast.lane_ref, bf16[64,1024]{1,0:T(8,128)(2,1)} %tok_hbm.1, f32[1,1024]{1,0:T(1,128)} %bitcast.19, s32[4,64]{1,0:T(4,128)} %bitcast.20, f32[4,64]{1,0:T(4,128)} %bitcast.21, ...), custom_call_target="tpu_custom_call" | custom-call | flops 50331648 | tf_op jit(solution)/shard_map/pallas_call | solution.py:166
  2.0 38.9 %all_to_all.10 = bf16[64,3,2,1024]{3,2,1,0:T(2,128)(2,1)S(1)} all-to-all(bf16[64,3,2,1024]{3,2,1,0:T(2,128)(2,1)S(1)} %bitcast.15), channel_id=1, replica_groups=mesh['grp'=2,'ep'=64,'tp'=2] {'ep'}, dimensions={0} | all-to-all | bytes 1572864 | tf_op jit(solution)/shard_map/all_to_all | solution.py:179
  40.9 7.1 %collective-permute-start = (bf16[192,2,1024]{2,1,0:T(2,128)(2,1)S(1)}, bf16[192,2,1024]{2,1,0:T(2,128)(2,1)S(1)}, u32[]{:S(2)}, u32[]{:S(2)}) collective-permute-start(bf16[192,2,1024]{2,1,0:T(2,128)(2,1)S(1)} %bitcast.13), channel_id=1, source_target_pairs={{0,1},{1,0},{2,3},{3,2},{4,5},{5,4},{6,7},{7,6},{8,9},{9,8},{10,11... | collective-permute-start | bytes 2359304 | tf_op jit(solution)/shard_map/ppermute | solution.py:161
  48.0 0.0 copy-done
  48.0 2.6 %shard_map.74 = (bf16[384,1024]{1,0:T(8,128)(2,1)S(1)}, bf16[896,1024]{1,0:T(8,128)(2,1)S(1)}) custom-call(bf16[192,2,1024]{2,1,0:T(2,128)(2,1)S(1)} %bitcast.14, bf16[1024,896]{1,0:T(8,128)(2,1)S(1)} %bitcast.16, bf16[1024,896]{1,0:T(8,128)(2,1)S(1)} %get-tuple-element.12.wu_ref, bf16[896,1024]{1,0:T(8,128)(2,1)} %bitcast.22), custom_call_target="tpu_custom_call" | custom-call | flops 2113929216 | tf_op jit(solution)/shard_map/pallas_call | solution.py:186
  50.6 0.1 collective-permute-start.1
  50.8 0.0 collective-permute-done.x_ref
  50.8 2.4 %shard_map.75.a_ref = bf16[384,1024]{1,0:T(8,128)(2,1)S(1)} custom-call(bf16[192,2,1024]{2,1,0:T(2,128)(2,1)S(1)} %collective-permute-done.x_ref, bf16[1024,896]{1,0:T(8,128)(2,1)S(1)} %bitcast.17, bf16[1024,896]{1,0:T(8,128)(2,1)S(1)} %get-tuple-element.12.wu_ref, bf16[896,1024]{1,0:T(8,128)(2,1)S(1)} %get-tuple-element.13.wd_ref), custom_call_target="tpu_custom_call" | custom-call | flops 2113929216 | tf_op jit(solution)/shard_map/pallas_call | solution.py:191
  53.2 0.0 collective-permute-done.1.b_ref
  53.2 0.3 shard_map.76
  53.5 27.9 %all_to_all.11 = bf16[64,3,2,1024]{3,2,1,0:T(2,128)(2,1)S(1)} all-to-all(bf16[64,3,2,1024]{3,2,1,0:T(2,128)(2,1)S(1)} %bitcast.12), channel_id=1, replica_groups=mesh['grp'=2,'ep'=64,'tp'=2] {'ep'}, dimensions={0} | all-to-all | bytes 1572864 | tf_op jit(solution)/shard_map/all_to_all | solution.py:179
  81.4 0.4 shard_map.77
  81.7 2.5 %collective-permute-start.2 = (f32[64,1024]{1,0:T(8,128)S(1)}, f32[64,1024]{1,0:T(8,128)S(1)}, u32[]{:S(2)}, u32[]{:S(2)}) collective-permute-start(f32[64,1024]{1,0:T(8,128)S(1)} %shard_map.77), channel_id=1, source_target_pairs={{0,1},{1,0},{2,3},{3,2},{4,5},{5,4},{6,7},{7,6},{8,9},{9,8},{10,11... | collective-permute-start | bytes 786440 | tf_op jit(solution)/shard_map/ppermute | solution.py:161
  84.2 1.2 %collective-permute-done.2 = f32[64,1024]{1,0:T(8,128)S(1)} collective-permute-done((f32[64,1024]{1,0:T(8,128)S(1)}, f32[64,1024]{1,0:T(8,128)S(1)}, u32[]{:S(2)}, u32[]{:S(2)}) %collective-permute-start.2) | collective-permute-done | bytes 262176 | tf_op jit(solution)/shard_map/ppermute | solution.py:161
  85.4 0.7 add_convert_fusion
Async XLA Ops:
  0.0 48.0 %copy-start = (bf16[1,1024,896]{2,1,0:T(8,128)(2,1)S(1)}, bf16[1,1024,896]{2,1,0:T(8,128)(2,1)}, u32[]{:S(2)}) copy-start(bf16[1,1024,896]{2,1,0:T(8,128)(2,1)} %param.11) | copy-start | bytes 5505028
  40.9 9.9 %collective-permute-start = (bf16[192,2,1024]{2,1,0:T(2,128)(2,1)S(1)}, bf16[192,2,1024]{2,1,0:T(2,128)(2,1)S(1)}, u32[]{:S(2)}, u32[]{:S(2)}) collective-permute-start(bf16[192,2,1024]{2,1,0:T(2,128)(2,1)S(1)} %bitcast.13), channel_id=1, source_target_pairs={{0,1},{1,0},{2,3},{3,2},{4,5},{5,4},{6,7},{7,6},{8,9},{9,8},{10,11... | collective-permute-start | bytes 2359304 | tf_op jit(solution)/shard_map/ppermute | solution.py:161
  50.6 2.6 %collective-permute-start.1 = (bf16[384,1024]{1,0:T(8,128)(2,1)S(1)}, bf16[384,1024]{1,0:T(8,128)(2,1)S(1)}, u32[]{:S(2)}, u32[]{:S(2)}) collective-permute-start(bf16[384,1024]{1,0:T(8,128)(2,1)S(1)} %get-tuple-element.14), channel_id=1, source_target_pairs={{0,1},{1,0},{2,3},{3,2},{4,5},{5,4},{6,7},{7,6},{8,9},{9,8},{10,11... | collective-permute-start | bytes 2359304 | tf_op jit(solution)/shard_map/ppermute | solution.py:161
  81.7 3.7 %collective-permute-start.2 = (f32[64,1024]{1,0:T(8,128)S(1)}, f32[64,1024]{1,0:T(8,128)S(1)}, u32[]{:S(2)}, u32[]{:S(2)}) collective-permute-start(f32[64,1024]{1,0:T(8,128)S(1)} %shard_map.77), channel_id=1, source_target_pairs={{0,1},{1,0},{2,3},{3,2},{4,5},{5,4},{6,7},{7,6},{8,9},{9,8},{10,11... | collective-permute-start | bytes 786440 | tf_op jit(solution)/shard_map/ppermute | solution.py:161

commit v9 on v8

--- a/solution.py
+++ b/solution.py
@@ -13,6 +13,7 @@
 VMEM = pl.BlockSpec(memory_space=pltpu.VMEM)
 SMEM = pl.BlockSpec(memory_space=pltpu.SMEM)
 HBM = pl.BlockSpec(memory_space=pltpu.HBM)
+HEAD_START = 1500
 LIMIT = 16 * 1024 * 1024
 
 
@@ -137,9 +138,13 @@
         mix_ref[i * toks : (i + 1) * toks, :] = jnp.where(here, dot(piece, rep), 0.0).astype(BF)
 
 
-def add_body(a_ref, b_ref, out_ref):
+def add_body(lane_ref, a_ref, b_ref, out_ref):
     total = a_ref[...].astype(F32) + b_ref[...].astype(F32)
     out_ref[...] = total.astype(BF).reshape(out_ref.shape)
+
+    @pl.when(lane_ref[0] == 1)
+    def _():
+        pl.delay(HEAD_START)
 
 
 def last_body(mix_ref, back_ref, out_ref):
@@ -189,7 +194,7 @@
     )(mine, wg, wu, *in_hbm(wd))
     got = swap(sent)
     kept = call(other_body, tall, [VMEM] * 4, [held], flops=work)(other, wg, wu, wd)
-    back = exchange(call(add_body, pairs, [VMEM] * 2, flops=items * width)(kept, got))
+    back = exchange(call(add_body, pairs, [SMEM] + [VMEM] * 2, flops=items * width)(lanes, kept, got))
     part = call(
         last_body, pltpu.VMEM((toks, width), F32), [VMEM] * 2, flops=2 * 3 * toks * items * width
     )(mix, back)

time: 86.3 us -> 87.7 us (1.016)
  blocking collectives: 66.8 us -> 70.2 us
  starting transfers between devices: 9.72 us -> 7.37 us
    all_to_all x2, blocking collectives: 66.8 us -> 70.2 us  [per_device(): lax.all_to_all(v.reshape(experts, slots // 2, 2, width), 'ep', split_axis...]
    ppermute x3, starting transfers between devices: 9.72 us -> 7.37 us  [per_device(): swap = lambda v: lax.ppermute(v, 'tp', [(0, 1), (1, 0)])]
where the time goes in v9:
time: 87.7 us; the launch traced here: 87.5 us
  blocking collectives  70.2 us (80%)
  Pallas kernels  7.7 us (9%)
  starting transfers between devices  7.37 us (8%)
  waiting for transfers between devices  1.51 us (2%)
    all_to_all x2, blocking collectives, per_device(): lax.all_to_all(v.reshape(experts, slots // 2, 2, width), 'ep', split_axis...  70.2 us
    ppermute x3, starting transfers between devices, per_device(): swap = lambda v: lax.ppermute(v, 'tp', [(0, 1), (1, 0)])  7.37 us
    pallas_call x1, Pallas kernels, per_device(): call(own_body, (tall, pltpu.VMEM(wd.shape, BF)), [VMEM] * 3 + [HBM], [hel...  2.64 us
    pallas_call x1, Pallas kernels, per_device(): call(other_body, tall, [VMEM] * 4, [held], flops=work)(other, wg, wu, wd)  2.41 us
    pallas_call x1, Pallas kernels, per_device(): call(functools.partial(prep_body, experts=experts, slots=slots), (pairs,...  1.98 us
  transfers between devices with their start and end apart: 3, of which 1 were waited for; matrix products, arithmetic and copies ran while one was open for 0% of the time, Pallas kernels for 6%

profile of v9, /device:TPU:513, one launch (start us, length us, event | category | flops | bytes accessed | tf_op | source)
XLA Modules:
  0.0 87.5 jit_solution(6877885141670467794)
XLA Ops:
  0.0 0.0 copy-start
  0.0 2.0 %shard_map.73 = (bf16[192,2,1024]{2,1,0:T(2,128)(2,1)S(1)}, bf16[1024,896]{1,0:T(8,128)(2,1)S(1)}, bf16[192,384]{1,0:T(8,128)(2,1)S(1)}) custom-call(s32[1]{0:T(128)} %bitcast.lane_ref, bf16[64,1024]{1,0:T(8,128)(2,1)} %tok_hbm.1, f32[1,1024]{1,0:T(1,128)} %bitcast.19, s32[4,64]{1,0:T(4,128)} %bitcast.20, f32[4,64]{1,0:T(4,128)} %bitcast.21, ...), custom_call_target="tpu_custom_call" | custom-call | flops 50331648 | tf_op jit(solution)/shard_map/pallas_call | solution.py:171
  2.0 38.9 %all_to_all.10 = bf16[64,3,2,1024]{3,2,1,0:T(2,128)(2,1)S(1)} all-to-all(bf16[64,3,2,1024]{3,2,1,0:T(2,128)(2,1)S(1)} %bitcast.15), channel_id=1, replica_groups=mesh['grp'=2,'ep'=64,'tp'=2] {'ep'}, dimensions={0} | all-to-all | bytes 1572864 | tf_op jit(solution)/shard_map/all_to_all | solution.py:184
  40.9 7.1 %collective-permute-start = (bf16[192,2,1024]{2,1,0:T(2,128)(2,1)S(1)}, bf16[192,2,1024]{2,1,0:T(2,128)(2,1)S(1)}, u32[]{:S(2)}, u32[]{:S(2)}) collective-permute-start(bf16[192,2,1024]{2,1,0:T(2,128)(2,1)S(1)} %bitcast.13), channel_id=1, source_target_pairs={{0,1},{1,0},{2,3},{3,2},{4,5},{5,4},{6,7},{7,6},{8,9},{9,8},{10,11... | collective-permute-start | bytes 2359304 | tf_op jit(solution)/shard_map/ppermute | solution.py:166
  48.0 0.0 copy-done
  48.0 2.6 %shard_map.74 = (bf16[384,1024]{1,0:T(8,128)(2,1)S(1)}, bf16[896,1024]{1,0:T(8,128)(2,1)S(1)}) custom-call(bf16[192,2,1024]{2,1,0:T(2,128)(2,1)S(1)} %bitcast.14, bf16[1024,896]{1,0:T(8,128)(2,1)S(1)} %bitcast.16, bf16[1024,896]{1,0:T(8,128)(2,1)S(1)} %get-tuple-element.12.wu_ref, bf16[896,1024]{1,0:T(8,128)(2,1)} %bitcast.22), custom_call_target="tpu_custom_call" | custom-call | flops 2113929216 | tf_op jit(solution)/shard_map/pallas_call | solution.py:191
  50.6 0.1 collective-permute-start.1
  50.8 0.0 collective-permute-done.x_ref
  50.8 2.4 %shard_map.75.a_ref = bf16[384,1024]{1,0:T(8,128)(2,1)S(1)} custom-call(bf16[192,2,1024]{2,1,0:T(2,128)(2,1)S(1)} %collective-permute-done.x_ref, bf16[1024,896]{1,0:T(8,128)(2,1)S(1)} %bitcast.17, bf16[1024,896]{1,0:T(8,128)(2,1)S(1)} %get-tuple-element.12.wu_ref, bf16[896,1024]{1,0:T(8,128)(2,1)S(1)} %get-tuple-element.13.wd_ref), custom_call_target="tpu_custom_call" | custom-call | flops 2113929216 | tf_op jit(solution)/shard_map/pallas_call | solution.py:196
  53.2 0.0 collective-permute-done.1.b_ref
  53.2 0.3 shard_map.76
  53.5 31.3 %all_to_all.11 = bf16[64,3,2,1024]{3,2,1,0:T(2,128)(2,1)S(1)} all-to-all(bf16[64,3,2,1024]{3,2,1,0:T(2,128)(2,1)S(1)} %bitcast.11), channel_id=1, replica_groups=mesh['grp'=2,'ep'=64,'tp'=2] {'ep'}, dimensions={0} | all-to-all | bytes 1572864 | tf_op jit(solution)/shard_map/all_to_all | solution.py:184
  84.8 0.4 shard_map.77
  85.2 0.1 collective-permute-start.2
  85.3 1.5 %collective-permute-done.2 = f32[64,1024]{1,0:T(8,128)S(1)} collective-permute-done((f32[64,1024]{1,0:T(8,128)S(1)}, f32[64,1024]{1,0:T(8,128)S(1)}, u32[]{:S(2)}, u32[]{:S(2)}) %collective-permute-start.2) | collective-permute-done | bytes 262176 | tf_op jit(solution)/shard_map/ppermute | solution.py:166
  86.8 0.7 add_convert_fusion
Async XLA Ops:
  0.0 48.0 %copy-start = (bf16[1,1024,896]{2,1,0:T(8,128)(2,1)S(1)}, bf16[1,1024,896]{2,1,0:T(8,128)(2,1)}, u32[]{:S(2)}) copy-start(bf16[1,1024,896]{2,1,0:T(8,128)(2,1)} %param.11) | copy-start | bytes 5505028
  40.9 9.9 %collective-permute-start = (bf16[192,2,1024]{2,1,0:T(2,128)(2,1)S(1)}, bf16[192,2,1024]{2,1,0:T(2,128)(2,1)S(1)}, u32[]{:S(2)}, u32[]{:S(2)}) collective-permute-start(bf16[192,2,1024]{2,1,0:T(2,128)(2,1)S(1)} %bitcast.13), channel_id=1, source_target_pairs={{0,1},{1,0},{2,3},{3,2},{4,5},{5,4},{6,7},{7,6},{8,9},{9,8},{10,11... | collective-permute-start | bytes 2359304 | tf_op jit(solution)/shard_map/ppermute | solution.py:166
  50.6 2.6 %collective-permute-start.1 = (bf16[384,1024]{1,0:T(8,128)(2,1)S(1)}, bf16[384,1024]{1,0:T(8,128)(2,1)S(1)}, u32[]{:S(2)}, u32[]{:S(2)}) collective-permute-start(bf16[384,1024]{1,0:T(8,128)(2,1)S(1)} %get-tuple-element.14), channel_id=1, source_target_pairs={{0,1},{1,0},{2,3},{3,2},{4,5},{5,4},{6,7},{7,6},{8,9},{9,8},{10,11... | collective-permute-start | bytes 2359304 | tf_op jit(solution)/shard_map/ppermute | solution.py:166
  85.2 1.7 %collective-permute-start.2 = (f32[64,1024]{1,0:T(8,128)S(1)}, f32[64,1024]{1,0:T(8,128)S(1)}, u32[]{:S(2)}, u32[]{:S(2)}) collective-permute-start(f32[64,1024]{1,0:T(8,128)S(1)} %shard_map.77), channel_id=1, source_target_pairs={{0,1},{1,0},{2,3},{3,2},{4,5},{5,4},{6,7},{7,6},{8,9},{9,8},{10,11... | collective-permute-start | bytes 786440 | tf_op jit(solution)/shard_map/ppermute | solution.py:166

commit v10 on v8

--- a/solution.py
+++ b/solution.py
@@ -49,10 +49,10 @@
     )
 
 
-def start_all(pairs, sems):
+def start_all(pairs, sems, urgent=0):
     copies = [pltpu.make_async_copy(a, b, sems.at[i]) for i, (a, b) in enumerate(pairs)]
-    for c in copies:
-        c.start()
+    for i, c in enumerate(copies):
+        c.start(priority=int(i < urgent))
     return copies
 
 
@@ -68,15 +68,11 @@
     out_ref, wu_ref, mix_ref,
     tok_ref, gain_ref, rt_ref, gt_ref, sems, *, experts, slots,
 ):
-    copies = start_all(
-        ((rt_hbm, rt_ref), (tok_hbm, tok_ref), (gain_hbm, gain_ref), (gt_hbm, gt_ref), (wu_hbm, wu_ref)), sems
-    )
-    for c in copies[:4]:
-        c.wait()
+    pairs = ((rt_hbm, rt_ref), (gt_hbm, gt_ref), (tok_hbm, tok_ref), (gain_hbm, gain_ref), (wu_hbm, wu_ref))
+    copies = start_all(pairs, sems, urgent=4)
+    copies[0].wait()
+    copies[1].wait()
     toks = tok_ref.shape[0]
-    xf = tok_ref[...].astype(F32)
-    var = jnp.mean(xf * xf, axis=-1, keepdims=True)
-    normed = (xf * lax.rsqrt(var + EPS) * gain_ref[...]).astype(BF)
     e_of = iota((experts, toks), 0)
     chosen = jnp.zeros((experts, toks), F32)
     for k in range(rt_ref.shape[0]):
@@ -87,8 +83,13 @@
     r = iota((n, toks), 0)
     slot = (r - div_const(r, slots) * slots).astype(F32)
     one = bf(dot(bf(iota((n, experts), 1) == e_row), place) == slot)
+    table(lane_ref, rt_ref[...], gt_ref[...], mix_ref, slots, experts)
+    copies[2].wait()
+    copies[3].wait()
+    xf = tok_ref[...].astype(F32)
+    var = jnp.mean(xf * xf, axis=-1, keepdims=True)
+    normed = (xf * lax.rsqrt(var + EPS) * gain_ref[...]).astype(BF)
     out_ref[...] = dot(one, normed).astype(BF).reshape(out_ref.shape)
-    table(lane_ref, rt_ref[...], gt_ref[...], mix_ref, slots, experts)
     copies[4].wait()
 
 

time: 86.3 us -> 86.6 us (level)
  no operation moved by 1% of the time
where the time goes in v10:
time: 86.6 us; the launch traced here: 86.4 us
  blocking collectives  66.8 us (77%)
  starting transfers between devices  9.71 us (11%)
  Pallas kernels  8.01 us (9%)
  waiting for transfers between devices  1.17 us (1%)
    all_to_all x2, blocking collectives, per_device(): lax.all_to_all(v.reshape(experts, slots // 2, 2, width), 'ep', split_axis...  66.8 us
    ppermute x3, starting transfers between devices, per_device(): swap = lambda v: lax.ppermute(v, 'tp', [(0, 1), (1, 0)])  9.71 us
    pallas_call x1, Pallas kernels, per_device(): call(own_body, (tall, pltpu.VMEM(wd.shape, BF)), [VMEM] * 3 + [HBM], [hel...  2.65 us
    pallas_call x1, Pallas kernels, per_device(): call(other_body, tall, [VMEM] * 4, [held], flops=work)(other, wg, wu, wd)  2.41 us
    pallas_call x1, Pallas kernels, per_device(): call(functools.partial(prep_body, experts=experts, slots=slots), (pairs,...  2.3 us
  transfers between devices with their start and end apart: 3, of which 1 were waited for; matrix products, arithmetic and copies ran while one was open for 0% of the time, Pallas kernels for 6%

profile of v10, /device:TPU:513, one launch (start us, length us, event | category | flops | bytes accessed | tf_op | source)
XLA Modules:
  0.0 86.4 jit_solution(1018011905167872554)
XLA Ops:
  0.0 0.0 copy-start
  0.0 2.3 %shard_map.73 = (bf16[192,2,1024]{2,1,0:T(2,128)(2,1)S(1)}, bf16[1024,896]{1,0:T(8,128)(2,1)S(1)}, bf16[192,384]{1,0:T(8,128)(2,1)S(1)}) custom-call(s32[1]{0:T(128)} %bitcast.lane_ref, bf16[64,1024]{1,0:T(8,128)(2,1)} %tok_hbm.1, f32[1,1024]{1,0:T(1,128)} %bitcast.19, s32[4,64]{1,0:T(4,128)} %bitcast.20, f32[4,64]{1,0:T(4,128)} %bitcast.21, ...), custom_call_target="tpu_custom_call" | custom-call | flops 50331648 | tf_op jit(solution)/shard_map/pallas_call | solution.py:167
  2.3 38.9 %all_to_all.10 = bf16[64,3,2,1024]{3,2,1,0:T(2,128)(2,1)S(1)} all-to-all(bf16[64,3,2,1024]{3,2,1,0:T(2,128)(2,1)S(1)} %bitcast.15), channel_id=1, replica_groups=mesh['grp'=2,'ep'=64,'tp'=2] {'ep'}, dimensions={0} | all-to-all | bytes 1572864 | tf_op jit(solution)/shard_map/all_to_all | solution.py:180
  41.2 7.1 %collective-permute-start = (bf16[192,2,1024]{2,1,0:T(2,128)(2,1)S(1)}, bf16[192,2,1024]{2,1,0:T(2,128)(2,1)S(1)}, u32[]{:S(2)}, u32[]{:S(2)}) collective-permute-start(bf16[192,2,1024]{2,1,0:T(2,128)(2,1)S(1)} %bitcast.13), channel_id=1, source_target_pairs={{0,1},{1,0},{2,3},{3,2},{4,5},{5,4},{6,7},{7,6},{8,9},{9,8},{10,11... | collective-permute-start | bytes 2359304 | tf_op jit(solution)/shard_map/ppermute | solution.py:162
  48.3 0.0 copy-done
  48.3 2.6 %shard_map.74 = (bf16[384,1024]{1,0:T(8,128)(2,1)S(1)}, bf16[896,1024]{1,0:T(8,128)(2,1)S(1)}) custom-call(bf16[192,2,1024]{2,1,0:T(2,128)(2,1)S(1)} %bitcast.14, bf16[1024,896]{1,0:T(8,128)(2,1)S(1)} %bitcast.16, bf16[1024,896]{1,0:T(8,128)(2,1)S(1)} %get-tuple-element.12.wu_ref, bf16[896,1024]{1,0:T(8,128)(2,1)} %bitcast.22), custom_call_target="tpu_custom_call" | custom-call | flops 2113929216 | tf_op jit(solution)/shard_map/pallas_call | solution.py:187
  50.9 0.1 collective-permute-start.1
  51.1 0.0 collective-permute-done.x_ref
  51.1 2.4 %shard_map.75.a_ref = bf16[384,1024]{1,0:T(8,128)(2,1)S(1)} custom-call(bf16[192,2,1024]{2,1,0:T(2,128)(2,1)S(1)} %collective-permute-done.x_ref, bf16[1024,896]{1,0:T(8,128)(2,1)S(1)} %bitcast.17, bf16[1024,896]{1,0:T(8,128)(2,1)S(1)} %get-tuple-element.12.wu_ref, bf16[896,1024]{1,0:T(8,128)(2,1)S(1)} %get-tuple-element.13.wd_ref), custom_call_target="tpu_custom_call" | custom-call | flops 2113929216 | tf_op jit(solution)/shard_map/pallas_call | solution.py:192
  53.5 0.0 collective-permute-done.1.b_ref
  53.5 0.3 shard_map.76
  53.8 27.9 %all_to_all.11 = bf16[64,3,2,1024]{3,2,1,0:T(2,128)(2,1)S(1)} all-to-all(bf16[64,3,2,1024]{3,2,1,0:T(2,128)(2,1)S(1)} %bitcast.12), channel_id=1, replica_groups=mesh['grp'=2,'ep'=64,'tp'=2] {'ep'}, dimensions={0} | all-to-all | bytes 1572864 | tf_op jit(solution)/shard_map/all_to_all | solution.py:180
  81.7 0.4 shard_map.77
  82.1 2.5 %collective-permute-start.2 = (f32[64,1024]{1,0:T(8,128)S(1)}, f32[64,1024]{1,0:T(8,128)S(1)}, u32[]{:S(2)}, u32[]{:S(2)}) collective-permute-start(f32[64,1024]{1,0:T(8,128)S(1)} %shard_map.77), channel_id=1, source_target_pairs={{0,1},{1,0},{2,3},{3,2},{4,5},{5,4},{6,7},{7,6},{8,9},{9,8},{10,11... | collective-permute-start | bytes 786440 | tf_op jit(solution)/shard_map/ppermute | solution.py:162
  84.6 1.2 %collective-permute-done.2 = f32[64,1024]{1,0:T(8,128)S(1)} collective-permute-done((f32[64,1024]{1,0:T(8,128)S(1)}, f32[64,1024]{1,0:T(8,128)S(1)}, u32[]{:S(2)}, u32[]{:S(2)}) %collective-permute-start.2) | collective-permute-done | bytes 262176 | tf_op jit(solution)/shard_map/ppermute | solution.py:162
  85.7 0.7 add_convert_fusion
Async XLA Ops:
  0.0 48.3 %copy-start = (bf16[1,1024,896]{2,1,0:T(8,128)(2,1)S(1)}, bf16[1,1024,896]{2,1,0:T(8,128)(2,1)}, u32[]{:S(2)}) copy-start(bf16[1,1024,896]{2,1,0:T(8,128)(2,1)} %param.11) | copy-start | bytes 5505028
  41.2 9.9 %collective-permute-start = (bf16[192,2,1024]{2,1,0:T(2,128)(2,1)S(1)}, bf16[192,2,1024]{2,1,0:T(2,128)(2,1)S(1)}, u32[]{:S(2)}, u32[]{:S(2)}) collective-permute-start(bf16[192,2,1024]{2,1,0:T(2,128)(2,1)S(1)} %bitcast.13), channel_id=1, source_target_pairs={{0,1},{1,0},{2,3},{3,2},{4,5},{5,4},{6,7},{7,6},{8,9},{9,8},{10,11... | collective-permute-start | bytes 2359304 | tf_op jit(solution)/shard_map/ppermute | solution.py:162
  50.9 2.6 %collective-permute-start.1 = (bf16[384,1024]{1,0:T(8,128)(2,1)S(1)}, bf16[384,1024]{1,0:T(8,128)(2,1)S(1)}, u32[]{:S(2)}, u32[]{:S(2)}) collective-permute-start(bf16[384,1024]{1,0:T(8,128)(2,1)S(1)} %get-tuple-element.14), channel_id=1, source_target_pairs={{0,1},{1,0},{2,3},{3,2},{4,5},{5,4},{6,7},{7,6},{8,9},{9,8},{10,11... | collective-permute-start | bytes 2359304 | tf_op jit(solution)/shard_map/ppermute | solution.py:162
  82.1 3.7 %collective-permute-start.2 = (f32[64,1024]{1,0:T(8,128)S(1)}, f32[64,1024]{1,0:T(8,128)S(1)}, u32[]{:S(2)}, u32[]{:S(2)}) collective-permute-start(f32[64,1024]{1,0:T(8,128)S(1)} %shard_map.77), channel_id=1, source_target_pairs={{0,1},{1,0},{2,3},{3,2},{4,5},{5,4},{6,7},{7,6},{8,9},{9,8},{10,11... | collective-permute-start | bytes 786440 | tf_op jit(solution)/shard_map/ppermute | solution.py:162

commit v11 on v8

--- a/solution.py
+++ b/solution.py
@@ -145,7 +145,7 @@
 def last_body(mix_ref, back_ref, out_ref):
     toks = out_ref.shape[0]
     s = dot(mix_ref[...], flat(back_ref))
-    out_ref[...] = s[:toks] + s[toks : 2 * toks] + s[2 * toks :]
+    out_ref[...] = (s[:toks] + s[toks : 2 * toks] + s[2 * toks :]).astype(BF)
 
 
 def per_device(tokens, routes, gates, norm_gain, w_gate, w_up, w_down):
@@ -191,9 +191,9 @@
     kept = call(other_body, tall, [VMEM] * 4, [held], flops=work)(other, wg, wu, wd)
     back = exchange(call(add_body, pairs, [VMEM] * 2, flops=items * width)(kept, got))
     part = call(
-        last_body, pltpu.VMEM((toks, width), F32), [VMEM] * 2, flops=2 * 3 * toks * items * width
+        last_body, pltpu.VMEM((toks, width), BF), [VMEM] * 2, flops=2 * 3 * toks * items * width
     )(mix, back)
-    return (part + swap(part)).astype(BF)
+    return (part.astype(F32) + swap(part).astype(F32)).astype(BF)
 
 
 def solution(mesh):

time: 86.3 us -> 86.1 us (level)
  no operation moved by 1% of the time
where the time goes in v11:
time: 86.1 us; the launch traced here: 85.9 us
  blocking collectives  66.8 us (78%)
  starting transfers between devices  9.72 us (11%)
  Pallas kernels  7.68 us (9%)
  waiting for transfers between devices  0.99 us (1%)
    all_to_all x2, blocking collectives, per_device(): lax.all_to_all(v.reshape(experts, slots // 2, 2, width), 'ep', split_axis...  66.8 us
    ppermute x3, starting transfers between devices, per_device(): swap = lambda v: lax.ppermute(v, 'tp', [(0, 1), (1, 0)])  9.72 us
    pallas_call x1, Pallas kernels, per_device(): call(own_body, (tall, pltpu.VMEM(wd.shape, BF)), [VMEM] * 3 + [HBM], [hel...  2.64 us
    pallas_call x1, Pallas kernels, per_device(): call(other_body, tall, [VMEM] * 4, [held], flops=work)(other, wg, wu, wd)  2.41 us
    pallas_call x1, Pallas kernels, per_device(): call(functools.partial(prep_body, experts=experts, slots=slots), (pairs,...  1.98 us
  transfers between devices with their start and end apart: 3, of which 1 were waited for; matrix products, arithmetic and copies ran while one was open for 0% of the time, Pallas kernels for 6%

profile of v11, /device:TPU:513, one launch (start us, length us, event | category | flops | bytes accessed | tf_op | source)
XLA Modules:
  0.0 85.9 jit_solution(15160106857679554025)
XLA Ops:
  0.0 0.0 copy-start
  0.0 2.0 %shard_map.73 = (bf16[192,2,1024]{2,1,0:T(2,128)(2,1)S(1)}, bf16[1024,896]{1,0:T(8,128)(2,1)S(1)}, bf16[192,384]{1,0:T(8,128)(2,1)S(1)}) custom-call(s32[1]{0:T(128)} %bitcast.lane_ref, bf16[64,1024]{1,0:T(8,128)(2,1)} %tok_hbm.1, f32[1,1024]{1,0:T(1,128)} %bitcast.19, s32[4,64]{1,0:T(4,128)} %bitcast.20, f32[4,64]{1,0:T(4,128)} %bitcast.21, ...), custom_call_target="tpu_custom_call" | custom-call | flops 50331648 | tf_op jit(solution)/shard_map/pallas_call | solution.py:166
  2.0 38.9 %all_to_all.10 = bf16[64,3,2,1024]{3,2,1,0:T(2,128)(2,1)S(1)} all-to-all(bf16[64,3,2,1024]{3,2,1,0:T(2,128)(2,1)S(1)} %bitcast.15), channel_id=1, replica_groups=mesh['grp'=2,'ep'=64,'tp'=2] {'ep'}, dimensions={0} | all-to-all | bytes 1572864 | tf_op jit(solution)/shard_map/all_to_all | solution.py:179
  40.9 7.1 %collective-permute-start = (bf16[192,2,1024]{2,1,0:T(2,128)(2,1)S(1)}, bf16[192,2,1024]{2,1,0:T(2,128)(2,1)S(1)}, u32[]{:S(2)}, u32[]{:S(2)}) collective-permute-start(bf16[192,2,1024]{2,1,0:T(2,128)(2,1)S(1)} %bitcast.13), channel_id=1, source_target_pairs={{0,1},{1,0},{2,3},{3,2},{4,5},{5,4},{6,7},{7,6},{8,9},{9,8},{10,11... | collective-permute-start | bytes 2359304 | tf_op jit(solution)/shard_map/ppermute | solution.py:161
  48.0 0.0 copy-done
  48.0 2.6 %shard_map.74 = (bf16[384,1024]{1,0:T(8,128)(2,1)S(1)}, bf16[896,1024]{1,0:T(8,128)(2,1)S(1)}) custom-call(bf16[192,2,1024]{2,1,0:T(2,128)(2,1)S(1)} %bitcast.14, bf16[1024,896]{1,0:T(8,128)(2,1)S(1)} %bitcast.16, bf16[1024,896]{1,0:T(8,128)(2,1)S(1)} %get-tuple-element.12.wu_ref, bf16[896,1024]{1,0:T(8,128)(2,1)} %bitcast.22), custom_call_target="tpu_custom_call" | custom-call | flops 2113929216 | tf_op jit(solution)/shard_map/pallas_call | solution.py:186
  50.6 0.1 collective-permute-start.1
  50.8 0.0 collective-permute-done.x_ref
  50.8 2.4 %shard_map.75.a_ref = bf16[384,1024]{1,0:T(8,128)(2,1)S(1)} custom-call(bf16[192,2,1024]{2,1,0:T(2,128)(2,1)S(1)} %collective-permute-done.x_ref, bf16[1024,896]{1,0:T(8,128)(2,1)S(1)} %bitcast.17, bf16[1024,896]{1,0:T(8,128)(2,1)S(1)} %get-tuple-element.12.wu_ref, bf16[896,1024]{1,0:T(8,128)(2,1)S(1)} %get-tuple-element.13.wd_ref), custom_call_target="tpu_custom_call" | custom-call | flops 2113929216 | tf_op jit(solution)/shard_map/pallas_call | solution.py:191
  53.2 0.0 collective-permute-done.1.b_ref
  53.2 0.3 shard_map.76
  53.5 27.9 %all_to_all.11 = bf16[64,3,2,1024]{3,2,1,0:T(2,128)(2,1)S(1)} all-to-all(bf16[64,3,2,1024]{3,2,1,0:T(2,128)(2,1)S(1)} %bitcast.12), channel_id=1, replica_groups=mesh['grp'=2,'ep'=64,'tp'=2] {'ep'}, dimensions={0} | all-to-all | bytes 1572864 | tf_op jit(solution)/shard_map/all_to_all | solution.py:179
  81.4 0.4 shard_map.77
  81.7 2.5 %collective-permute-start.2 = (bf16[64,1024]{1,0:T(8,128)(2,1)S(1)}, bf16[64,1024]{1,0:T(8,128)(2,1)S(1)}, u32[]{:S(2)}, u32[]{:S(2)}) collective-permute-start(bf16[64,1024]{1,0:T(8,128)(2,1)S(1)} %shard_map.77), channel_id=1, source_target_pairs={{0,1},{1,0},{2,3},{3,2},{4,5},{5,4},{6,7},{7,6},{8,9},{9,8},{10,11... | collective-permute-start | bytes 393224 | tf_op jit(solution)/shard_map/ppermute | solution.py:161
  84.2 1.0 %collective-permute-done.2 = bf16[64,1024]{1,0:T(8,128)(2,1)S(1)} collective-permute-done((bf16[64,1024]{1,0:T(8,128)(2,1)S(1)}, bf16[64,1024]{1,0:T(8,128)(2,1)S(1)}, u32[]{:S(2)}, u32[]{:S(2)}) %collective-permute-start.2) | collective-permute-done | bytes 131104 | tf_op jit(solution)/shard_map/ppermute | solution.py:161
  85.2 0.7 add_convert_fusion
Async XLA Ops:
  0.0 48.0 %copy-start = (bf16[1,1024,896]{2,1,0:T(8,128)(2,1)S(1)}, bf16[1,1024,896]{2,1,0:T(8,128)(2,1)}, u32[]{:S(2)}) copy-start(bf16[1,1024,896]{2,1,0:T(8,128)(2,1)} %param.11) | copy-start | bytes 5505028
  40.9 9.9 %collective-permute-start = (bf16[192,2,1024]{2,1,0:T(2,128)(2,1)S(1)}, bf16[192,2,1024]{2,1,0:T(2,128)(2,1)S(1)}, u32[]{:S(2)}, u32[]{:S(2)}) collective-permute-start(bf16[192,2,1024]{2,1,0:T(2,128)(2,1)S(1)} %bitcast.13), channel_id=1, source_target_pairs={{0,1},{1,0},{2,3},{3,2},{4,5},{5,4},{6,7},{7,6},{8,9},{9,8},{10,11... | collective-permute-start | bytes 2359304 | tf_op jit(solution)/shard_map/ppermute | solution.py:161
  50.6 2.6 %collective-permute-start.1 = (bf16[384,1024]{1,0:T(8,128)(2,1)S(1)}, bf16[384,1024]{1,0:T(8,128)(2,1)S(1)}, u32[]{:S(2)}, u32[]{:S(2)}) collective-permute-start(bf16[384,1024]{1,0:T(8,128)(2,1)S(1)} %get-tuple-element.14), channel_id=1, source_target_pairs={{0,1},{1,0},{2,3},{3,2},{4,5},{5,4},{6,7},{7,6},{8,9},{9,8},{10,11... | collective-permute-start | bytes 2359304 | tf_op jit(solution)/shard_map/ppermute | solution.py:161
  81.7 3.5 %collective-permute-start.2 = (bf16[64,1024]{1,0:T(8,128)(2,1)S(1)}, bf16[64,1024]{1,0:T(8,128)(2,1)S(1)}, u32[]{:S(2)}, u32[]{:S(2)}) collective-permute-start(bf16[64,1024]{1,0:T(8,128)(2,1)S(1)} %shard_map.77), channel_id=1, source_target_pairs={{0,1},{1,0},{2,3},{3,2},{4,5},{5,4},{6,7},{7,6},{8,9},{9,8},{10,11... | collective-permute-start | bytes 393224 | tf_op jit(solution)/shard_map/ppermute | solution.py:161

commit v12 on v8

--- a/solution.py
+++ b/solution.py
@@ -14,6 +14,7 @@
 SMEM = pl.BlockSpec(memory_space=pltpu.SMEM)
 HBM = pl.BlockSpec(memory_space=pltpu.HBM)
 LIMIT = 16 * 1024 * 1024
+PIECES = 8
 
 
 def dot(a, b):
@@ -68,8 +69,12 @@
     out_ref, wu_ref, mix_ref,
     tok_ref, gain_ref, rt_ref, gt_ref, sems, *, experts, slots,
 ):
+    step = wu_ref.shape[0] // PIECES
+    pieces = [slice(i * step, (i + 1) * step) for i in range(PIECES)]
     copies = start_all(
-        ((rt_hbm, rt_ref), (tok_hbm, tok_ref), (gain_hbm, gain_ref), (gt_hbm, gt_ref), (wu_hbm, wu_ref)), sems
+        ((rt_hbm, rt_ref), (tok_hbm, tok_ref), (gain_hbm, gain_ref), (gt_hbm, gt_ref))
+        + tuple((wu_hbm.at[p], wu_ref.at[p]) for p in pieces),
+        sems,
     )
     for c in copies[:4]:
         c.wait()
@@ -89,7 +94,8 @@
     one = bf(dot(bf(iota((n, experts), 1) == e_row), place) == slot)
     out_ref[...] = dot(one, normed).astype(BF).reshape(out_ref.shape)
     table(lane_ref, rt_ref[...], gt_ref[...], mix_ref, slots, experts)
-    copies[4].wait()
+    for c in copies[4:]:
+        c.wait()
 
 
 def hidden_units(rows, wg_ref, wu_ref, hid_ref):
@@ -172,7 +178,7 @@
             pltpu.VMEM((1, width), F32),
             pltpu.VMEM((top, toks), jnp.int32),
             pltpu.VMEM((top, toks), F32),
-            pltpu.SemaphoreType.DMA((5,)),
+            pltpu.SemaphoreType.DMA((4 + PIECES,)),
         ],
         flops=2 * items * toks * width,
     )(lanes, *in_hbm(tokens, norm_gain.reshape(1, width), routes.T, gates.T, wu))

time: 86.3 us -> 86.4 us (level)
  no operation moved by 1% of the time
where the time goes in v12:
time: 86.4 us; the launch traced here: 86.2 us
  blocking collectives  66.8 us (77%)
  starting transfers between devices  9.72 us (11%)
  Pallas kernels  7.76 us (9%)
  waiting for transfers between devices  1.17 us (1%)
    all_to_all x2, blocking collectives, per_device(): lax.all_to_all(v.reshape(experts, slots // 2, 2, width), 'ep', split_axis...  66.8 us
    ppermute x3, starting transfers between devices, per_device(): swap = lambda v: lax.ppermute(v, 'tp', [(0, 1), (1, 0)])  9.72 us
    pallas_call x1, Pallas kernels, per_device(): call(own_body, (tall, pltpu.VMEM(wd.shape, BF)), [VMEM] * 3 + [HBM], [hel...  2.65 us
    pallas_call x1, Pallas kernels, per_device(): call(other_body, tall, [VMEM] * 4, [held], flops=work)(other, wg, wu, wd)  2.41 us
    pallas_call x1, Pallas kernels, per_device(): call(functools.partial(prep_body, experts=experts, slots=slots), (pairs,...  2.05 us
  transfers between devices with their start and end apart: 3, of which 1 were waited for; matrix products, arithmetic and copies ran while one was open for 0% of the time, Pallas kernels for 6%

profile of v12, /device:TPU:513, one launch (start us, length us, event | category | flops | bytes accessed | tf_op | source)
XLA Modules:
  0.0 86.2 jit_solution(6700426232669818108)
XLA Ops:
  0.0 0.0 copy-start
  0.0 2.1 %shard_map.73 = (bf16[192,2,1024]{2,1,0:T(2,128)(2,1)S(1)}, bf16[1024,896]{1,0:T(8,128)(2,1)S(1)}, bf16[192,384]{1,0:T(8,128)(2,1)S(1)}) custom-call(s32[1]{0:T(128)} %bitcast.lane_ref, bf16[64,1024]{1,0:T(8,128)(2,1)} %tok_hbm.1, f32[1,1024]{1,0:T(1,128)} %bitcast.19, s32[4,64]{1,0:T(4,128)} %bitcast.20, f32[4,64]{1,0:T(4,128)} %bitcast.21, ...), custom_call_target="tpu_custom_call" | custom-call | flops 50331648 | tf_op jit(solution)/shard_map/pallas_call | solution.py:172
  2.1 38.9 %all_to_all.10 = bf16[64,3,2,1024]{3,2,1,0:T(2,128)(2,1)S(1)} all-to-all(bf16[64,3,2,1024]{3,2,1,0:T(2,128)(2,1)S(1)} %bitcast.15), channel_id=1, replica_groups=mesh['grp'=2,'ep'=64,'tp'=2] {'ep'}, dimensions={0} | all-to-all | bytes 1572864 | tf_op jit(solution)/shard_map/all_to_all | solution.py:185
  41.0 7.1 %collective-permute-start = (bf16[192,2,1024]{2,1,0:T(2,128)(2,1)S(1)}, bf16[192,2,1024]{2,1,0:T(2,128)(2,1)S(1)}, u32[]{:S(2)}, u32[]{:S(2)}) collective-permute-start(bf16[192,2,1024]{2,1,0:T(2,128)(2,1)S(1)} %bitcast.13), channel_id=1, source_target_pairs={{0,1},{1,0},{2,3},{3,2},{4,5},{5,4},{6,7},{7,6},{8,9},{9,8},{10,11... | collective-permute-start | bytes 2359304 | tf_op jit(solution)/shard_map/ppermute | solution.py:167
  48.0 0.0 copy-done
  48.0 2.6 %shard_map.74 = (bf16[384,1024]{1,0:T(8,128)(2,1)S(1)}, bf16[896,1024]{1,0:T(8,128)(2,1)S(1)}) custom-call(bf16[192,2,1024]{2,1,0:T(2,128)(2,1)S(1)} %bitcast.14, bf16[1024,896]{1,0:T(8,128)(2,1)S(1)} %bitcast.16, bf16[1024,896]{1,0:T(8,128)(2,1)S(1)} %get-tuple-element.12.wu_ref, bf16[896,1024]{1,0:T(8,128)(2,1)} %bitcast.22), custom_call_target="tpu_custom_call" | custom-call | flops 2113929216 | tf_op jit(solution)/shard_map/pallas_call | solution.py:192
  50.7 0.1 collective-permute-start.1
  50.9 0.0 collective-permute-done.x_ref
  50.9 2.4 %shard_map.75.a_ref = bf16[384,1024]{1,0:T(8,128)(2,1)S(1)} custom-call(bf16[192,2,1024]{2,1,0:T(2,128)(2,1)S(1)} %collective-permute-done.x_ref, bf16[1024,896]{1,0:T(8,128)(2,1)S(1)} %bitcast.17, bf16[1024,896]{1,0:T(8,128)(2,1)S(1)} %get-tuple-element.12.wu_ref, bf16[896,1024]{1,0:T(8,128)(2,1)S(1)} %get-tuple-element.13.wd_ref), custom_call_target="tpu_custom_call" | custom-call | flops 2113929216 | tf_op jit(solution)/shard_map/pallas_call | solution.py:197
  53.3 0.0 collective-permute-done.1.b_ref
  53.3 0.3 shard_map.76
  53.6 27.9 %all_to_all.11 = bf16[64,3,2,1024]{3,2,1,0:T(2,128)(2,1)S(1)} all-to-all(bf16[64,3,2,1024]{3,2,1,0:T(2,128)(2,1)S(1)} %bitcast.12), channel_id=1, replica_groups=mesh['grp'=2,'ep'=64,'tp'=2] {'ep'}, dimensions={0} | all-to-all | bytes 1572864 | tf_op jit(solution)/shard_map/all_to_all | solution.py:185
  81.4 0.4 shard_map.77
  81.8 2.5 %collective-permute-start.2 = (f32[64,1024]{1,0:T(8,128)S(1)}, f32[64,1024]{1,0:T(8,128)S(1)}, u32[]{:S(2)}, u32[]{:S(2)}) collective-permute-start(f32[64,1024]{1,0:T(8,128)S(1)} %shard_map.77), channel_id=1, source_target_pairs={{0,1},{1,0},{2,3},{3,2},{4,5},{5,4},{6,7},{7,6},{8,9},{9,8},{10,11... | collective-permute-start | bytes 786440 | tf_op jit(solution)/shard_map/ppermute | solution.py:167
  84.3 1.2 %collective-permute-done.2 = f32[64,1024]{1,0:T(8,128)S(1)} collective-permute-done((f32[64,1024]{1,0:T(8,128)S(1)}, f32[64,1024]{1,0:T(8,128)S(1)}, u32[]{:S(2)}, u32[]{:S(2)}) %collective-permute-start.2) | collective-permute-done | bytes 262176 | tf_op jit(solution)/shard_map/ppermute | solution.py:167
  85.5 0.7 add_convert_fusion
Async XLA Ops:
  0.0 48.0 %copy-start = (bf16[1,1024,896]{2,1,0:T(8,128)(2,1)S(1)}, bf16[1,1024,896]{2,1,0:T(8,128)(2,1)}, u32[]{:S(2)}) copy-start(bf16[1,1024,896]{2,1,0:T(8,128)(2,1)} %param.11) | copy-start | bytes 5505028
  41.0 9.9 %collective-permute-start = (bf16[192,2,1024]{2,1,0:T(2,128)(2,1)S(1)}, bf16[192,2,1024]{2,1,0:T(2,128)(2,1)S(1)}, u32[]{:S(2)}, u32[]{:S(2)}) collective-permute-start(bf16[192,2,1024]{2,1,0:T(2,128)(2,1)S(1)} %bitcast.13), channel_id=1, source_target_pairs={{0,1},{1,0},{2,3},{3,2},{4,5},{5,4},{6,7},{7,6},{8,9},{9,8},{10,11... | collective-permute-start | bytes 2359304 | tf_op jit(solution)/shard_map/ppermute | solution.py:167
  50.7 2.6 %collective-permute-start.1 = (bf16[384,1024]{1,0:T(8,128)(2,1)S(1)}, bf16[384,1024]{1,0:T(8,128)(2,1)S(1)}, u32[]{:S(2)}, u32[]{:S(2)}) collective-permute-start(bf16[384,1024]{1,0:T(8,128)(2,1)S(1)} %get-tuple-element.14), channel_id=1, source_target_pairs={{0,1},{1,0},{2,3},{3,2},{4,5},{5,4},{6,7},{7,6},{8,9},{9,8},{10,11... | collective-permute-start | bytes 2359304 | tf_op jit(solution)/shard_map/ppermute | solution.py:167
  81.8 3.7 %collective-permute-start.2 = (f32[64,1024]{1,0:T(8,128)S(1)}, f32[64,1024]{1,0:T(8,128)S(1)}, u32[]{:S(2)}, u32[]{:S(2)}) collective-permute-start(f32[64,1024]{1,0:T(8,128)S(1)} %shard_map.77), channel_id=1, source_target_pairs={{0,1},{1,0},{2,3},{3,2},{4,5},{5,4},{6,7},{7,6},{8,9},{9,8},{10,11... | collective-permute-start | bytes 786440 | tf_op jit(solution)/shard_map/ppermute | solution.py:167

commit v13 on v12

--- a/solution.py
+++ b/solution.py
@@ -57,11 +57,9 @@
     return copies
 
 
-def slot_of(chosen, core, slots):
-    toks = chosen.shape[1]
-    upper = bf(iota((toks, toks), 0) < iota((toks, toks), 1))
-    rel = dot(chosen.astype(BF), upper) - (core * slots).astype(F32)
-    return jnp.where((chosen > 0) & (rel >= 0) & (rel < slots), rel, -1.0)
+def slot_of(rank, core, slots):
+    rel = rank - (core * slots).astype(F32)
+    return jnp.where((rank >= 0) & (rel >= 0) & (rel < slots), rel, -1.0)
 
 
 def prep_body(
@@ -71,12 +69,15 @@
 ):
     step = wu_ref.shape[0] // PIECES
     pieces = [slice(i * step, (i + 1) * step) for i in range(PIECES)]
+    few = tok_ref.shape[0] // 4
+    blocks = [slice(i * few, (i + 1) * few) for i in range(4)]
     copies = start_all(
-        ((rt_hbm, rt_ref), (tok_hbm, tok_ref), (gain_hbm, gain_ref), (gt_hbm, gt_ref))
+        ((rt_hbm, rt_ref), (gain_hbm, gain_ref), (gt_hbm, gt_ref))
+        + tuple((tok_hbm.at[p], tok_ref.at[p]) for p in blocks)
         + tuple((wu_hbm.at[p], wu_ref.at[p]) for p in pieces),
         sems,
     )
-    for c in copies[:4]:
+    for c in copies[:7]:
         c.wait()
     toks = tok_ref.shape[0]
     xf = tok_ref[...].astype(F32)
@@ -84,17 +85,22 @@
     normed = (xf * lax.rsqrt(var + EPS) * gain_ref[...]).astype(BF)
     e_of = iota((experts, toks), 0)
     chosen = jnp.zeros((experts, toks), F32)
+    gate = jnp.zeros((experts, toks), F32)
     for k in range(rt_ref.shape[0]):
-        chosen = chosen + (e_of == rt_ref[k : k + 1, :]).astype(F32)
-    place = slot_of(chosen, lane_ref[0], slots).astype(BF)
+        hit = e_of == rt_ref[k : k + 1, :]
+        chosen = chosen + hit.astype(F32)
+        gate = gate + jnp.where(hit, gt_ref[k : k + 1, :], 0.0)
+    upper = bf(iota((toks, toks), 0) < iota((toks, toks), 1))
+    rank = jnp.where(chosen > 0, dot(chosen.astype(BF), upper), -1.0)
+    place = slot_of(rank, lane_ref[0], slots).astype(BF)
     n = slots * experts
     e_row = div_const(iota((n, experts), 0), slots)
     r = iota((n, toks), 0)
     slot = (r - div_const(r, slots) * slots).astype(F32)
     one = bf(dot(bf(iota((n, experts), 1) == e_row), place) == slot)
     out_ref[...] = dot(one, normed).astype(BF).reshape(out_ref.shape)
-    table(lane_ref, rt_ref[...], gt_ref[...], mix_ref, slots, experts)
-    for c in copies[4:]:
+    table(slot_of(rank, 1 - lane_ref[0], slots).T.astype(BF), gate.T, mix_ref, slots)
+    for c in copies[7:]:
         c.wait()
 
 
@@ -118,17 +124,8 @@
     out_ref[...] = dot(hid_ref[...], wd_ref[...]).astype(BF)
 
 
-def table(lane_ref, rt, gt, mix_ref, slots, experts):
-    top, toks = rt.shape
-    e_of = iota((experts, toks), 0)
-    chosen = jnp.zeros((experts, toks), F32)
-    gate = jnp.zeros((experts, toks), F32)
-    for k in range(top):
-        hit = e_of == rt[k : k + 1, :]
-        chosen = chosen + hit.astype(F32)
-        gate = gate + jnp.where(hit, gt[k : k + 1, :], 0.0)
-    place = slot_of(chosen, 1 - lane_ref[0], slots).T.astype(BF)
-    gate = gate.T
+def table(place, gate, mix_ref, slots):
+    toks, experts = gate.shape
     g1 = gate.astype(BF)
     rest = gate - g1.astype(F32)
     g2 = rest.astype(BF)
@@ -138,9 +135,11 @@
     e_r = div_const(r, slots)
     slot = (r - e_r * slots).astype(F32)
     rep = bf(iota((experts, n), 0) == e_r)
-    here = dot(place, rep) == slot
-    for i, piece in enumerate((g1, g2, g3)):
-        mix_ref[i * toks : (i + 1) * toks, :] = jnp.where(here, dot(piece, rep), 0.0).astype(BF)
+    spread = dot(jnp.concatenate([place, g1, g2, g3], axis=0), rep)
+    here = spread[:toks] == slot
+    for i in range(3):
+        piece = spread[(i + 1) * toks : (i + 2) * toks]
+        mix_ref[i * toks : (i + 1) * toks, :] = jnp.where(here, piece, 0.0).astype(BF)
 
 
 def add_body(a_ref, b_ref, out_ref):
@@ -178,7 +177,7 @@
             pltpu.VMEM((1, width), F32),
             pltpu.VMEM((top, toks), jnp.int32),
             pltpu.VMEM((top, toks), F32),
-            pltpu.SemaphoreType.DMA((4 + PIECES,)),
+            pltpu.SemaphoreType.DMA((7 + PIECES,)),
         ],
         flops=2 * items * toks * width,
     )(lanes, *in_hbm(tokens, norm_gain.reshape(1, width), routes.T, gates.T, wu))

time: 86.4 us -> 86.2 us (level)
  no operation moved by 1% of the time
where the time goes in v13:
time: 86.2 us; the launch traced here: 86 us
  blocking collectives  66.8 us (77%)
  starting transfers between devices  9.72 us (11%)
  Pallas kernels  7.59 us (9%)
  waiting for transfers between devices  1.17 us (1%)
    all_to_all x2, blocking collectives, per_device(): lax.all_to_all(v.reshape(experts, slots // 2, 2, width), 'ep', split_axis...  66.8 us
    ppermute x3, starting transfers between devices, per_device(): swap = lambda v: lax.ppermute(v, 'tp', [(0, 1), (1, 0)])  9.72 us
    pallas_call x1, Pallas kernels, per_device(): call(own_body, (tall, pltpu.VMEM(wd.shape, BF)), [VMEM] * 3 + [HBM], [hel...  2.64 us
    pallas_call x1, Pallas kernels, per_device(): call(other_body, tall, [VMEM] * 4, [held], flops=work)(other, wg, wu, wd)  2.41 us
    pallas_call x1, Pallas kernels, per_device(): call(functools.partial(prep_body, experts=experts, slots=slots), (pairs,...  1.88 us
  transfers between devices with their start and end apart: 3, of which 1 were waited for; matrix products, arithmetic and copies ran while one was open for 0% of the time, Pallas kernels for 6%

profile of v13, /device:TPU:513, one launch (start us, length us, event | category | flops | bytes accessed | tf_op | source)
XLA Modules:
  0.0 86.0 jit_solution(14771395282145111428)
XLA Ops:
  0.0 0.0 copy-start
  0.0 1.9 %shard_map.73 = (bf16[192,2,1024]{2,1,0:T(2,128)(2,1)S(1)}, bf16[1024,896]{1,0:T(8,128)(2,1)S(1)}, bf16[192,384]{1,0:T(8,128)(2,1)S(1)}) custom-call(s32[1]{0:T(128)} %bitcast.lane_ref, bf16[64,1024]{1,0:T(8,128)(2,1)} %tok_hbm.1, f32[1,1024]{1,0:T(1,128)} %bitcast.19, s32[4,64]{1,0:T(4,128)} %bitcast.20, f32[4,64]{1,0:T(4,128)} %bitcast.21, ...), custom_call_target="tpu_custom_call" | custom-call | flops 50331648 | tf_op jit(solution)/shard_map/pallas_call | solution.py:171
  1.9 38.9 %all_to_all.10 = bf16[64,3,2,1024]{3,2,1,0:T(2,128)(2,1)S(1)} all-to-all(bf16[64,3,2,1024]{3,2,1,0:T(2,128)(2,1)S(1)} %bitcast.15), channel_id=1, replica_groups=mesh['grp'=2,'ep'=64,'tp'=2] {'ep'}, dimensions={0} | all-to-all | bytes 1572864 | tf_op jit(solution)/shard_map/all_to_all | solution.py:184
  40.8 7.1 %collective-permute-start = (bf16[192,2,1024]{2,1,0:T(2,128)(2,1)S(1)}, bf16[192,2,1024]{2,1,0:T(2,128)(2,1)S(1)}, u32[]{:S(2)}, u32[]{:S(2)}) collective-permute-start(bf16[192,2,1024]{2,1,0:T(2,128)(2,1)S(1)} %bitcast.13), channel_id=1, source_target_pairs={{0,1},{1,0},{2,3},{3,2},{4,5},{5,4},{6,7},{7,6},{8,9},{9,8},{10,11... | collective-permute-start | bytes 2359304 | tf_op jit(solution)/shard_map/ppermute | solution.py:166
  47.9 0.0 copy-done
  47.9 2.6 %shard_map.74 = (bf16[384,1024]{1,0:T(8,128)(2,1)S(1)}, bf16[896,1024]{1,0:T(8,128)(2,1)S(1)}) custom-call(bf16[192,2,1024]{2,1,0:T(2,128)(2,1)S(1)} %bitcast.14, bf16[1024,896]{1,0:T(8,128)(2,1)S(1)} %bitcast.16, bf16[1024,896]{1,0:T(8,128)(2,1)S(1)} %get-tuple-element.12.wu_ref, bf16[896,1024]{1,0:T(8,128)(2,1)} %bitcast.22), custom_call_target="tpu_custom_call" | custom-call | flops 2113929216 | tf_op jit(solution)/shard_map/pallas_call | solution.py:191
  50.5 0.1 collective-permute-start.1
  50.7 0.0 collective-permute-done.x_ref
  50.7 2.4 %shard_map.75.a_ref = bf16[384,1024]{1,0:T(8,128)(2,1)S(1)} custom-call(bf16[192,2,1024]{2,1,0:T(2,128)(2,1)S(1)} %collective-permute-done.x_ref, bf16[1024,896]{1,0:T(8,128)(2,1)S(1)} %bitcast.17, bf16[1024,896]{1,0:T(8,128)(2,1)S(1)} %get-tuple-element.12.wu_ref, bf16[896,1024]{1,0:T(8,128)(2,1)S(1)} %get-tuple-element.13.wd_ref), custom_call_target="tpu_custom_call" | custom-call | flops 2113929216 | tf_op jit(solution)/shard_map/pallas_call | solution.py:196
  53.1 0.0 collective-permute-done.1.b_ref
  53.1 0.3 shard_map.76
  53.4 27.9 %all_to_all.11 = bf16[64,3,2,1024]{3,2,1,0:T(2,128)(2,1)S(1)} all-to-all(bf16[64,3,2,1024]{3,2,1,0:T(2,128)(2,1)S(1)} %bitcast.12), channel_id=1, replica_groups=mesh['grp'=2,'ep'=64,'tp'=2] {'ep'}, dimensions={0} | all-to-all | bytes 1572864 | tf_op jit(solution)/shard_map/all_to_all | solution.py:184
  81.3 0.4 shard_map.77
  81.7 2.5 %collective-permute-start.2 = (f32[64,1024]{1,0:T(8,128)S(1)}, f32[64,1024]{1,0:T(8,128)S(1)}, u32[]{:S(2)}, u32[]{:S(2)}) collective-permute-start(f32[64,1024]{1,0:T(8,128)S(1)} %shard_map.77), channel_id=1, source_target_pairs={{0,1},{1,0},{2,3},{3,2},{4,5},{5,4},{6,7},{7,6},{8,9},{9,8},{10,11... | collective-permute-start | bytes 786440 | tf_op jit(solution)/shard_map/ppermute | solution.py:166
  84.1 1.2 %collective-permute-done.2 = f32[64,1024]{1,0:T(8,128)S(1)} collective-permute-done((f32[64,1024]{1,0:T(8,128)S(1)}, f32[64,1024]{1,0:T(8,128)S(1)}, u32[]{:S(2)}, u32[]{:S(2)}) %collective-permute-start.2) | collective-permute-done | bytes 262176 | tf_op jit(solution)/shard_map/ppermute | solution.py:166
  85.3 0.7 add_convert_fusion
Async XLA Ops:
  0.0 47.9 %copy-start = (bf16[1,1024,896]{2,1,0:T(8,128)(2,1)S(1)}, bf16[1,1024,896]{2,1,0:T(8,128)(2,1)}, u32[]{:S(2)}) copy-start(bf16[1,1024,896]{2,1,0:T(8,128)(2,1)} %param.11) | copy-start | bytes 5505028
  40.8 9.9 %collective-permute-start = (bf16[192,2,1024]{2,1,0:T(2,128)(2,1)S(1)}, bf16[192,2,1024]{2,1,0:T(2,128)(2,1)S(1)}, u32[]{:S(2)}, u32[]{:S(2)}) collective-permute-start(bf16[192,2,1024]{2,1,0:T(2,128)(2,1)S(1)} %bitcast.13), channel_id=1, source_target_pairs={{0,1},{1,0},{2,3},{3,2},{4,5},{5,4},{6,7},{7,6},{8,9},{9,8},{10,11... | collective-permute-start | bytes 2359304 | tf_op jit(solution)/shard_map/ppermute | solution.py:166
  50.5 2.6 %collective-permute-start.1 = (bf16[384,1024]{1,0:T(8,128)(2,1)S(1)}, bf16[384,1024]{1,0:T(8,128)(2,1)S(1)}, u32[]{:S(2)}, u32[]{:S(2)}) collective-permute-start(bf16[384,1024]{1,0:T(8,128)(2,1)S(1)} %get-tuple-element.14), channel_id=1, source_target_pairs={{0,1},{1,0},{2,3},{3,2},{4,5},{5,4},{6,7},{7,6},{8,9},{9,8},{10,11... | collective-permute-start | bytes 2359304 | tf_op jit(solution)/shard_map/ppermute | solution.py:166
  81.7 3.7 %collective-permute-start.2 = (f32[64,1024]{1,0:T(8,128)S(1)}, f32[64,1024]{1,0:T(8,128)S(1)}, u32[]{:S(2)}, u32[]{:S(2)}) collective-permute-start(f32[64,1024]{1,0:T(8,128)S(1)} %shard_map.77), channel_id=1, source_target_pairs={{0,1},{1,0},{2,3},{3,2},{4,5},{5,4},{6,7},{7,6},{8,9},{9,8},{10,11... | collective-permute-start | bytes 786440 | tf_op jit(solution)/shard_map/ppermute | solution.py:166
